TPU v7x, 32 devices: a whole 2x2x4 slice. The times are simulated.
32 devices in a mesh: ep: 4 (over y, x), tp: 8 (over z, core).
Axes of the slice: x: 2, y: 2, z: 4, core: 2. Of those that a mesh axis runs over, the one named last changes fastest.
Arguments:
- queries: bfloat16 [2048, 16, 128], P('ep', 'tp'), may hold values from -300 to 300
- keys: bfloat16 [2048, 16, 128], P('ep', 'tp'), may hold values from -4 to 4
- values: bfloat16 [2048, 16, 128], P('ep', 'tp'), may hold values from -6 to 6
- mix_weight: float32 [16], P('tp'), may hold values from 0.3 to 0.8
- sub_gain: float32 [128], replicated, may hold values from 0.1 to 1.9
- tokens: bfloat16 [1024, 2048], P('ep', 'tp'), may hold values from -6 to 6
- routes: int32 [1024, 2], P('ep'), may hold values from 0 to 7, all different within a row; in each aligned block of 256 rows (0 to 255, 256 to 511, ...) at most 96 rows name the same one
- route_weights: float32 [1024, 2], P('ep'), may hold values from 0.1 to 1
- expert_gain: float32 [2048], replicated, may hold values from 0.1 to 1.9
- gate_weight: bfloat16 [8, 2048, 4096], P('ep', None, 'tp'), may hold values from -0.375 to 0.375
- up_weight: bfloat16 [8, 2048, 4096], P('ep', None, 'tp'), may hold values from -0.375 to 0.375
- down_weight: bfloat16 [8, 4096, 2048], P('ep', 'tp'), may hold values from -0.09375 to 0.09375
Outputs:
- attn_out: bfloat16 [2048, 16, 128], P('ep', 'tp')
- moe_out: bfloat16 [1024, 2048], P('ep', 'tp')
Inputs may be any that keep to these rules, and one draw needn't show every extreme that they name: `routes`: in each aligned block of 256 rows no expert is named by more than 96 rows, and in every draw some expert is named by exactly 96 rows of some block.
All inputs are finite; a program needn't handle non-finite values.
Results may differ from a plain program's by a relative error of at most 0.018.
Values may be sent and summed in bfloat16 or wider, within the bound.
No kernel may reach another device: no remote copies, remote signals or barrier semaphores. Data moves between devices by JAX's collectives and lax.ppermute only.
A program may use at most 128 MiB of HBM per device.

v0:
```python
import math

import jax
import jax.numpy as jnp
from jax import lax
from jax.sharding import PartitionSpec as P

NEG_FILL = -1e30
SUB_EPS = 1e-05
NORM_EPS = 1e-06
CLAMP_LIMIT = 7.0
GLU_ALPHA = 1.702
OUT_SCALE = 0.8


def partner(value, axis, stride):
    mask = 2**stride
    pairs = [(source, source ^ mask) for source in range(lax.axis_size(axis))]
    return lax.ppermute(value, axis, pairs)


def score_update(running, query_four, key_block, value_block, key_start, query_pos, score_scale):
    row_max, row_sum, weighted = running
    item_count = key_block.shape[0]
    key_four = key_block.reshape(item_count, key_block.shape[1], 2, -1)
    scores = (
        jnp.einsum("qhmd,khmd->hmqk", query_four, key_four, preferred_element_type=jnp.float32)
        * score_scale
    )
    key_pos = key_start + lax.iota(jnp.int32, item_count)
    visible = key_pos[None, :] <= query_pos[:, None]
    new_max = jnp.maximum(row_max, jnp.max(jnp.where(visible, scores, NEG_FILL), axis=-1))
    weights = jnp.where(visible, jnp.exp(scores - new_max[..., None]), 0.0)
    shrink = jnp.exp(row_max - new_max)
    row_sum = row_sum * shrink + jnp.sum(weights, axis=-1)
    value_sum = jnp.einsum(
        "hmqk,khe->hmqe",
        weights.astype(jnp.bfloat16),
        value_block,
        preferred_element_type=jnp.float32,
    )
    return (new_max, row_sum, weighted * shrink[..., None] + value_sum)


def attend(queries, keys, values, mix_weight, sub_gain):
    row_count, heads_here, pair_width = queries.shape
    value_width = values.shape[2]
    groups = lax.axis_size("ep")
    bit_count = groups.bit_length() - 1
    half_rows = row_count // 2
    place = lax.axis_index("ep")
    moved = queries[half_rows:]
    for bit in range(bit_count):
        moved = partner(moved, "ep", bit)
    queries_used = jnp.concatenate([queries[:half_rows], moved], axis=0)
    query_pos = jnp.concatenate(
        [
            place * row_count + lax.iota(jnp.int32, half_rows),
            (groups - 1 - place) * row_count + half_rows + lax.iota(jnp.int32, half_rows),
        ],
        axis=0,
    )
    query_four = queries_used.reshape(row_count, heads_here, 2, pair_width // 2)
    score_scale = (pair_width // 2) ** (-0.5)
    last_pos = jnp.max(query_pos)
    initial = (
        jnp.full((heads_here, 2, row_count), NEG_FILL, jnp.float32),
        jnp.zeros((heads_here, 2, row_count), jnp.float32),
        jnp.zeros((heads_here, 2, row_count, value_width), jnp.float32),
    )
    key_piece = lax.all_gather(keys, "ep", axis=0, tiled=True)
    value_piece = lax.all_gather(values, "ep", axis=0, tiled=True)
    item_count = key_piece.shape[0]
    block_size = math.gcd(item_count, 1536)
    key_blocks = key_piece.reshape(item_count // block_size, block_size, heads_here, pair_width)
    value_blocks = value_piece.reshape(
        item_count // block_size, block_size, heads_here, value_width
    )

    def key_step(current, bundle):
        key_block, value_block, block_index = bundle
        key_start = block_index * block_size

        def update(inner):
            return score_update(
                inner, query_four, key_block, value_block, key_start, query_pos, score_scale
            )

        def keep_state(inner):
            return inner

        return (lax.cond(key_start <= last_pos, update, keep_state, current), None)

    result, _ = lax.scan(
        key_step, initial, (key_blocks, value_blocks, lax.iota(jnp.int32, item_count // block_size))
    )
    row_max, row_sum, weighted = result
    heads_out = weighted / row_sum[..., None]
    blend = heads_out[:, 0] - mix_weight[:, None, None] * heads_out[:, 1]
    scaled = blend * lax.rsqrt(jnp.mean(blend * blend, axis=-1, keepdims=True) + SUB_EPS)
    result = jnp.transpose((scaled * sub_gain * OUT_SCALE).astype(jnp.bfloat16), (1, 0, 2))
    returned = result[half_rows:]
    for bit in range(bit_count):
        returned = partner(returned, "ep", bit)
    result = jnp.concatenate([result[:half_rows], returned], axis=0)
    return result


def slot_table(routes, experts_all, capacity):
    flat_routes = routes.reshape(-1)
    onehot = (flat_routes[:, None] == lax.iota(jnp.int32, experts_all)[None, :]).astype(jnp.int32)
    slot_rank = jnp.sum((jnp.cumsum(onehot, axis=0) - 1) * onehot, axis=1)
    return flat_routes * capacity + slot_rank


def dispatch(rows_here, target, pick_count, slot_count):
    row_count = rows_here.shape[0]
    slot_owner = (
        jnp.full((slot_count,), row_count, jnp.int32)
        .at[target]
        .set(lax.iota(jnp.int32, row_count * pick_count) // pick_count)
    )
    padded = jnp.concatenate(
        [rows_here, jnp.zeros((1, rows_here.shape[1]), rows_here.dtype)], axis=0
    )
    return padded[slot_owner]


def expert_finish(gate_pre, up_pre, squares, width_total, down_weight):
    factor = lax.rsqrt(squares / width_total + NORM_EPS)[..., None]
    gate_part = jnp.minimum(gate_pre * factor, CLAMP_LIMIT)
    up_part = jnp.clip(up_pre * factor, -CLAMP_LIMIT, CLAMP_LIMIT)
    hidden = ((up_part + 1.0) * gate_part * jax.nn.sigmoid(GLU_ALPHA * gate_part)).astype(
        jnp.bfloat16
    )
    return jnp.einsum("secf,efd->secd", hidden, down_weight, preferred_element_type=jnp.float32)


def route_layer(tokens, routes, route_weights, expert_gain, gate_weight, up_weight, down_weight):
    row_count, pick_count = routes.shape
    groups = lax.axis_size("ep")
    local_experts = gate_weight.shape[0]
    experts_all = groups * local_experts
    capacity = 3 * row_count * pick_count // (2 * experts_all)
    target = slot_table(routes, experts_all, capacity)
    layout = (groups, local_experts, capacity)
    width_total = expert_gain.shape[0]
    full_rows = lax.all_gather(tokens, "tp", axis=1, tiled=True)
    outgoing = dispatch(full_rows, target, pick_count, experts_all * capacity).reshape(
        layout + (width_total,)
    )
    arrived = lax.all_to_all(outgoing, "ep", split_axis=0, concat_axis=0, tiled=True)
    floats = arrived.astype(jnp.float32)
    squares = jnp.sum(floats * floats, axis=-1)
    normed = (floats * expert_gain).astype(jnp.bfloat16)
    gate_pre = jnp.einsum("secd,edf->secf", normed, gate_weight, preferred_element_type=jnp.float32)
    up_pre = jnp.einsum("secd,edf->secf", normed, up_weight, preferred_element_type=jnp.float32)
    partial_value = expert_finish(gate_pre, up_pre, squares, width_total, down_weight)
    summed = lax.psum_scatter(
        partial_value.astype(jnp.bfloat16), "tp", scatter_dimension=3, tiled=True
    )
    returned = lax.all_to_all(summed, "ep", split_axis=0, concat_axis=0, tiled=True)
    flat_back = returned.reshape(experts_all * capacity, returned.shape[3])
    picked = flat_back[target].astype(jnp.float32).reshape(row_count, pick_count, returned.shape[3])
    return jnp.sum(picked * route_weights[..., None], axis=1).astype(jnp.bfloat16)


def shards(
    queries,
    keys,
    values,
    mix_weight,
    sub_gain,
    tokens,
    routes,
    route_weights,
    expert_gain,
    gate_weight,
    up_weight,
    down_weight,
):
    attn_out = attend(queries, keys, values, mix_weight, sub_gain)
    moe_out = route_layer(
        tokens, routes, route_weights, expert_gain, gate_weight, up_weight, down_weight
    )
    return (attn_out, moe_out)


def solution(mesh):
    return jax.shard_map(
        shards,
        mesh=mesh,
        in_specs=(
            P("ep", "tp", None),
            P("ep", "tp", None),
            P("ep", "tp", None),
            P("tp"),
            P(),
            P("ep", "tp"),
            P("ep", None),
            P("ep", None),
            P(),
            P("ep", None, "tp"),
            P("ep", None, "tp"),
            P("ep", "tp", None),
        ),
        out_specs=(P("ep", "tp", None), P("ep", "tp")),
        check_vma=False,
    )
```

profile of v0, /device:TPU:0, one launch (start us, length us, event | category | flops | bytes accessed | tf_op | source)
XLA Modules:
  0.0 175.6 jit_solution(4271129474864718489)
XLA Ops:
  12.3 2.4 %scatter_custom_fusion = s32[768]{0:T(1024)S(1)} fusion(s32[512]{0:T(512)S(1)} %bitcast.108, s32[512]{0:T(512)S(1)} %add_select_fusion, s32[]{:T(128)} %constant.91.clone.1), kind=kCustom, calls=%fused_computation.85 | custom fusion | bytes 3076 | tf_op jit(solution)/shard_map/scatter | solution.py:121
  14.8 22.2 %all-gather.8.cloned.1.call-done = bf16[256,2048]{1,0:T(8,128)(2,1)} async-done(((bf16[256,256]{1,0:T(8,128)(2,1)}), bf16[256,2048]{1,0:T(8,128)(2,1)}) %all-gather.8.cloned.1.call-update) | async-done | bytes 1048592 | tf_op jit(solution)/shard_map/all_gather | solution.py:148
  38.3 4.3 %gather_fusion = bf16[768,2048]{1,0:T(8,128)(2,1)} fusion(bf16[257,2048]{1,0:T(8,128)(2,1)S(1)} %concatenate.15, s32[1024]{0:T(1024)S(1)} %pad_clamp_fusion.1), kind=kCustom, calls=%fused_computation | custom fusion | bytes 6294528 | tf_op jit(solution)/shard_map/gather | solution.py:126
  42.6 3.8 %all-to-all-start = ((bf16[4,2,96,2048]{3,2,1,0:T(8,128)(2,1)}), bf16[4,2,96,2048]{3,2,1,0:T(8,128)(2,1)S(1)}, u32[]{:S(2)}, u32[]{:S(2)}) async-start(bf16[4,2,96,2048]{3,2,1,0:T(8,128)(2,1)} %bitcast.103), calls=%async_computation | async-start | bytes 6291456 | tf_op jit(solution)/shard_map/all_to_all | solution.py:152
  47.3 1.7 copy.85
  49.1 42.5 %all-to-all-done = bf16[4,2,96,2048]{3,2,1,0:T(8,128)(2,1)S(1)} async-done(((bf16[4,2,96,2048]{3,2,1,0:T(8,128)(2,1)}), bf16[4,2,96,2048]{3,2,1,0:T(8,128)(2,1)S(1)}, u32[]{:S(2)}, u32[]{:S(2)}) %all-to-all-start) | async-done | bytes 3145760 | tf_op jit(solution)/shard_map/all_to_all | solution.py:152
  92.6 1.7 copy-done
  94.4 1.8 %fusion.23 = f32[2,4,96,512]{3,2,1,0:T(8,128)S(1)} fusion(bf16[2,2048,512]{2,1,0:T(8,128)(2,1)S(1)} %copy-done.7, bf16[4,2,96,2048]{3,2,1,0:T(8,128)(2,1)S(1)} %get-tuple-element.217), kind=kOutput, calls=%fused_computation.32 | convolution fusion | flops 1610612736 | bytes 8912896 | tf_op jit(solution)/shard_map/secd,edf->secf/dot_general | solution.py:156
  96.2 10.0 %fusion.30 = bf16[4,2,96,2048]{3,2,0,1:T(8,128)(2,1)} fusion(bf16[2,512,2048]{2,1,0:T(8,128)(2,1)} %param.27, f32[2,4,96,512]{3,2,1,0:T(8,128)S(1)} %fusion.23, bf16[2,2048,512]{2,1,0:T(8,128)(2,1)} %param.26, bf16[4,2,96,2048]{3,2,1,0:T(8,128)(2,1)} %copy-done, f32[4,2,96]{2,0,1:T(4,128)S(1)} %fusion.60), kind=kOutput, calls=%fused_computation.37 | convolution fusion | flops 3227516928 | bytes 16256000 | tf_op jit(solution)/shard_map/secf,efd->secd/dot_general | solution.py:136
  109.5 2.9 %collective-permute-done = bf16[256,2,128]{2,1,0:T(2,128)(2,1)S(1)} collective-permute-done((bf16[256,2,128]{2,1,0:T(2,128)(2,1)S(1)}, bf16[256,2,128]{2,1,0:T(2,128)(2,1)S(1)}, u32[]{:S(2)}, u32[]{:S(2)}) %collective-permute-start) | collective-permute-done | bytes 131104 | tf_op jit(solution)/shard_map/ppermute | solution.py:19
  115.8 4.8 %collective-permute-done.1 = bf16[256,2,128]{2,1,0:T(2,128)(2,1)S(1)} collective-permute-done((bf16[256,2,128]{2,1,0:T(2,128)(2,1)S(1)}, bf16[256,2,128]{2,1,0:T(2,128)(2,1)S(1)}, u32[]{:S(2)}, u32[]{:S(2)}) %collective-permute-start.1) | collective-permute-done | bytes 131104 | tf_op jit(solution)/shard_map/ppermute | solution.py:19
  121.1 1.7 copy.86
  124.3 20.2 %while.14 = (s32[]{:T(128)}, f32[2,2,512]{2,1,0:T(2,128)S(1)}, f32[2,2,512]{2,1,0:T(2,128)S(1)}, f32[2,2,512,128]{3,2,1,0:T(8,128)S(1)}, s32[4]{0:T(128)S(1)}, /...) while((s32[]{:T(128)}, f32[2,2,512]{2,1,0:T(2,128)S(1)}, ...), condition=%wide.region_7.8_spmd, body=%wide.region_2.7_spmd.sunk | while | flops 414978560 | bytes 17176872 | solution.py:94
  125.5 3.8 %conditional.2 = ((f32[2,2,512]{2,1,0:T(2,128)S(1)}, f32[2,2,512]{2,1,0:T(2,128)S(1)}, f32[2,2,512,128]{3,2,1,0:T(8,128)S(1)})) conditional(s32[]{:T(128)} %convert_element_type.74, (f32[2,2,512]{2,1,0:T(2,128)S(1)}, f32[2,2,512]{2,1,0:T(2,128)S(1)}, f32[2,2,512,128]{3,2,1,0:T(8,128)S(1)}) %tuple.48, (s32[]{:T(128)}, s32[512]{0:T(512)S(1)}, ...), branch_computations={%region_3.3_spmd, %region_4.0_spmd} | conditional | flops 414978560 | bytes 17176620 | solution.py:92
  130.6 3.8 %conditional.2 = ((f32[2,2,512]{2,1,0:T(2,128)S(1)}, f32[2,2,512]{2,1,0:T(2,128)S(1)}, f32[2,2,512,128]{3,2,1,0:T(8,128)S(1)})) conditional(s32[]{:T(128)} %convert_element_type.74, (f32[2,2,512]{2,1,0:T(2,128)S(1)}, f32[2,2,512]{2,1,0:T(2,128)S(1)}, f32[2,2,512,128]{3,2,1,0:T(8,128)S(1)}) %tuple.48, (s32[]{:T(128)}, s32[512]{0:T(512)S(1)}, ...), branch_computations={%region_3.3_spmd, %region_4.0_spmd} | conditional | flops 414978560 | bytes 17176620 | solution.py:92
  135.7 3.8 %conditional.2 = ((f32[2,2,512]{2,1,0:T(2,128)S(1)}, f32[2,2,512]{2,1,0:T(2,128)S(1)}, f32[2,2,512,128]{3,2,1,0:T(8,128)S(1)})) conditional(s32[]{:T(128)} %convert_element_type.74, (f32[2,2,512]{2,1,0:T(2,128)S(1)}, f32[2,2,512]{2,1,0:T(2,128)S(1)}, f32[2,2,512,128]{3,2,1,0:T(8,128)S(1)}) %tuple.48, (s32[]{:T(128)}, s32[512]{0:T(512)S(1)}, ...), branch_computations={%region_3.3_spmd, %region_4.0_spmd} | conditional | flops 414978560 | bytes 17176620 | solution.py:92
  137.8 1.6 fusion.11
  140.7 3.8 %conditional.2 = ((f32[2,2,512]{2,1,0:T(2,128)S(1)}, f32[2,2,512]{2,1,0:T(2,128)S(1)}, f32[2,2,512,128]{3,2,1,0:T(8,128)S(1)})) conditional(s32[]{:T(128)} %convert_element_type.74, (f32[2,2,512]{2,1,0:T(2,128)S(1)}, f32[2,2,512]{2,1,0:T(2,128)S(1)}, f32[2,2,512,128]{3,2,1,0:T(8,128)S(1)}) %tuple.48, (s32[]{:T(128)}, s32[512]{0:T(512)S(1)}, ...), branch_computations={%region_3.3_spmd, %region_4.0_spmd} | conditional | flops 414978560 | bytes 17176620 | solution.py:92
  144.8 3.0 %copy_divide_fusion = f32[2,2,512,128]{3,0,2,1:T(2,128)S(1)} fusion(f32[2,2,512,128]{3,2,1,0:T(8,128)S(1)} %get-tuple-element.138, f32[2,2,512]{0,2,1:T(8,128)S(1)} %copy.88), kind=kLoop, calls=%fused_computation.48 | loop fusion | flops 262144 | bytes 2105344 | tf_op jit(solution)/shard_map/div | solution.py:98
  149.8 1.8 %copy.98 = bf16[4,2,96,256]{3,2,1,0:T(8,128)(2,1)} copy(bf16[4,2,96,256]{3,2,0,1:T(8,128)(2,1)} %reduce-scatter.2.cloned.1.call-done) | data formatting | bytes 786432 | tf_op jit(solution)/shard_map/reduce_scatter | solution.py:159
  151.5 3.5 %all-to-all-start.1 = ((bf16[4,2,96,256]{3,2,1,0:T(8,128)(2,1)}), bf16[4,2,96,256]{3,2,1,0:T(8,128)(2,1)S(1)}, u32[]{:S(2)}, u32[]{:S(2)}) async-start(bf16[4,2,96,256]{3,2,1,0:T(8,128)(2,1)} %copy.98), calls=%async_computation.2 | async-start | bytes 786432 | tf_op jit(solution)/shard_map/all_to_all | solution.py:162
  155.0 2.2 %collective-permute-start.3 = (bf16[256,2,128]{2,1,0:T(2,128)(2,1)S(1)}, bf16[256,2,128]{2,1,0:T(2,128)(2,1)S(1)}, u32[]{:S(2)}, u32[]{:S(2)}) collective-permute-start(bf16[256,2,128]{2,1,0:T(2,128)(2,1)S(1)} %collective-permute-done.2), channel_id=1, source_target_pairs={{0,16},{8,24},{16,0},{24,8},{1,17},{9,25},{17,1},{25,9},{2,18},{10... | collective-permute-start | bytes 393224 | tf_op jit(solution)/shard_map/ppermute | solution.py:19
  157.4 6.2 %collective-permute-done.3 = bf16[256,2,128]{2,1,0:T(2,128)(2,1)S(1)} collective-permute-done((bf16[256,2,128]{2,1,0:T(2,128)(2,1)S(1)}, bf16[256,2,128]{2,1,0:T(2,128)(2,1)S(1)}, u32[]{:S(2)}, u32[]{:S(2)}) %collective-permute-start.3) | collective-permute-done | bytes 131104 | tf_op jit(solution)/shard_map/ppermute | solution.py:19
  164.6 1.9 %gather_fusion.1 = bf16[512,256]{1,0:T(8,128)(2,1)S(1)} fusion(bf16[768,256]{1,0:T(8,128)(2,1)S(1)} %bitcast.102, s32[1024]{0:T(1024)S(1)} %pad_clamp_fusion), kind=kCustom, calls=%fused_computation.1 | custom fusion | bytes 526336 | tf_op jit(solution)/shard_map/gather | solution.py:164
  (111 shorter events, 35.5 us)
Async XLA Ops:
  8.0 29.0 %all-gather.8.cloned.1.call-start = ((), (), s32[]{:S(2)}) async-start(), calls=%async_computation.5 | async-start | bytes 1179648 | tf_op jit(solution)/shard_map/all_gather | solution.py:148
  42.6 3.9 %copy-start.1 = (bf16[512,2,128]{2,1,0:T(2,128)(2,1)S(1)}, bf16[512,2,128]{2,1,0:T(2,128)(2,1)}, u32[]{:S(2)}) copy-start(bf16[512,2,128]{2,1,0:T(2,128)(2,1)} %param.17) | copy-start | bytes 786436
  42.6 49.0 %copy-start.3 = (f32[2048]{0:T(1024)S(1)}, f32[2048]{0:T(1024)}, u32[]{:S(2)}) copy-start(f32[2048]{0:T(1024)} %param.24) | copy-start | bytes 24580
  42.6 49.0 %all-to-all-start = ((bf16[4,2,96,2048]{3,2,1,0:T(8,128)(2,1)}), bf16[4,2,96,2048]{3,2,1,0:T(8,128)(2,1)S(1)}, u32[]{:S(2)}, u32[]{:S(2)}) async-start(bf16[4,2,96,2048]{3,2,1,0:T(8,128)(2,1)} %bitcast.103), calls=%async_computation | async-start | bytes 6291456 | tf_op jit(solution)/shard_map/all_to_all | solution.py:152
  46.5 74.7 %all-gather.4.cloned.1.call-start = ((), (), s32[]{:S(2)}) async-start(), calls=%async_computation.3 | async-start | bytes 1310720 | tf_op jit(solution)/shard_map/all_gather | solution.py:71
  47.3 75.6 %all-gather.6.cloned.1.call-start = ((), (), s32[]{:S(2)}) async-start(), calls=%async_computation.4 | async-start | bytes 1310720 | tf_op jit(solution)/shard_map/all_gather | solution.py:72
  49.1 100.7 %reduce-scatter.2.cloned.1.call-start = ((), (), s32[]{:S(2)}) async-start(), calls=%async_computation.6 | async-start | bytes 3538944 | tf_op jit(solution)/shard_map/reduce_scatter | solution.py:159
  91.6 2.8 %copy-start.7 = (bf16[2,2048,512]{2,1,0:T(8,128)(2,1)S(1)}, bf16[2,2048,512]{2,1,0:T(8,128)(2,1)}, u32[]{:S(2)}) copy-start(bf16[2,2048,512]{2,1,0:T(8,128)(2,1)} %param.25) | copy-start | bytes 12582916
  92.6 1.7 copy-start
  106.2 0.9 copy-start.2
  107.4 5.0 %collective-permute-start = (bf16[256,2,128]{2,1,0:T(2,128)(2,1)S(1)}, bf16[256,2,128]{2,1,0:T(2,128)(2,1)S(1)}, u32[]{:S(2)}, u32[]{:S(2)}) collective-permute-start(bf16[256,2,128]{2,1,0:T(2,128)(2,1)S(1)} %get-tuple-element.221), channel_id=1, source_target_pairs={{0,8},{8,0},{16,24},{24,16},{1,9},{9,1},{17,25},{25,17},{2,10},{10... | collective-permute-start | bytes 393224 | tf_op jit(solution)/shard_map/ppermute | solution.py:19
  112.4 8.2 %collective-permute-start.1 = (bf16[256,2,128]{2,1,0:T(2,128)(2,1)S(1)}, bf16[256,2,128]{2,1,0:T(2,128)(2,1)S(1)}, u32[]{:S(2)}, u32[]{:S(2)}) collective-permute-start(bf16[256,2,128]{2,1,0:T(2,128)(2,1)S(1)} %collective-permute-done), channel_id=1, source_target_pairs={{0,16},{8,24},{16,0},{24,8},{1,17},{9,25},{17,1},{25,9},{2,18},{10... | collective-permute-start | bytes 393224 | tf_op jit(solution)/shard_map/ppermute | solution.py:19
  144.5 3.3 %copy-start.6 = (f32[2]{0:T(128)S(1)}, f32[2]{0:T(128)}, u32[]{:S(2)}) copy-start(f32[2]{0:T(128)} %param.19) | copy-start | bytes 28
  144.5 4.2 %copy-start.5 = (f32[128]{0:T(128)S(1)}, f32[128]{0:T(128)}, u32[]{:S(2)}) copy-start(f32[128]{0:T(128)} %param.20) | copy-start | bytes 1540
  147.8 9.4 %copy-start.4 = (f32[256,2]{0,1:T(2,128)S(1)}, f32[256,2]{0,1:T(2,128)}, u32[]{:S(2)}) copy-start(f32[256,2]{0,1:T(2,128)} %param.23) | copy-start | bytes 6148
  149.6 5.4 %collective-permute-start.2 = (bf16[256,2,128]{2,1,0:T(2,128)(2,1)S(1)}, bf16[256,2,128]{2,1,0:T(2,128)(2,1)S(1)}, u32[]{:S(2)}, u32[]{:S(2)}) collective-permute-start(bf16[256,2,128]{2,1,0:T(2,128)(2,1)S(1)} %get-tuple-element.219), channel_id=1, source_target_pairs={{0,8},{8,0},{16,24},{24,16},{1,9},{9,1},{17,25},{25,17},{2,10},{10... | collective-permute-start | bytes 393224 | tf_op jit(solution)/shard_map/ppermute | solution.py:19
  151.5 13.1 %all-to-all-start.1 = ((bf16[4,2,96,256]{3,2,1,0:T(8,128)(2,1)}), bf16[4,2,96,256]{3,2,1,0:T(8,128)(2,1)S(1)}, u32[]{:S(2)}, u32[]{:S(2)}) async-start(bf16[4,2,96,256]{3,2,1,0:T(8,128)(2,1)} %copy.98), calls=%async_computation.2 | async-start | bytes 786432 | tf_op jit(solution)/shard_map/all_to_all | solution.py:162
  155.0 8.5 %collective-permute-start.3 = (bf16[256,2,128]{2,1,0:T(2,128)(2,1)S(1)}, bf16[256,2,128]{2,1,0:T(2,128)(2,1)S(1)}, u32[]{:S(2)}, u32[]{:S(2)}) collective-permute-start(bf16[256,2,128]{2,1,0:T(2,128)(2,1)S(1)} %collective-permute-done.2), channel_id=1, source_target_pairs={{0,16},{8,24},{16,0},{24,8},{1,17},{9,25},{17,1},{25,9},{2,18},{10... | collective-permute-start | bytes 393224 | tf_op jit(solution)/shard_map/ppermute | solution.py:19
Sparse Core Ops, SparseCore 0:
  10.4 26.5 all-gather.7
  106.4 39.1 reduce-scatter.1
Sparse Core Ops, SparseCore 1:
  49.4 40.8 all-gather.3
  91.9 29.8 all-gather.5
where the time goes:
time: 176 us
  waiting for transfers between devices  79.4 us (45%)
  local copies, waits for them, and re-layouts  25.2 us (14%)
  matrix products  22 us (12%)
  between operations  17.1 us (10%)
  other arithmetic  16.4 us (9%)
  starting transfers between devices  12.6 us (7%)
  loops' own time  2.99 us (2%)
    all_to_all x1, waiting for transfers between devices, route_layer(): lax.all_to_all(outgoing, 'ep', split_axis=0, concat_axis=0, tiled=True)  42.5 us
    all_gather x1, waiting for transfers between devices, route_layer(): full_rows = lax.all_gather(tokens, 'tp', axis=1, tiled=True)  22.2 us
    ppermute x4, waiting for transfers between devices, partner(): return lax.ppermute(value, axis, pairs)  13.9 us
    dot_general x1, matrix products, expert_finish(): jnp.einsum('secf,efd->secd', hidden, down_weight, preferred_element_type=...  10 us
    dot_general x4, matrix products, score_update(): jnp.einsum('hmqk,khe->hmqe', weights.astype(jnp.bfloat16), value_block, p...  6.48 us
    unnamed x20, local copies, waits for them, and re-layouts  6.1 us
    ppermute x4, starting transfers between devices, partner(): return lax.ppermute(value, axis, pairs)  5.18 us
    gather x1, local copies, waits for them, and re-layouts, dispatch(): return padded[slot_owner]  4.27 us
  transfers between devices with their start and end apart: 10, of which 5 were waited for; matrix products, arithmetic and copies ran while one was open for 29% of the time, Pallas kernels for 0%

commit v1 on v0

v1 whole, which is shorter than its diff:
```python
import functools

import jax
import jax.numpy as jnp
from jax import lax
from jax.experimental import pallas as pl
from jax.experimental.pallas import tpu as pltpu
from jax.sharding import PartitionSpec as P

NEG_FILL = -1e30
SUB_EPS = 1e-05
NORM_EPS = 1e-06
CLAMP_LIMIT = 7.0
GLU_ALPHA = 1.702
OUT_SCALE = 0.8
LOG2E = 1.4426950408889634
CORES = 2

VMEM = pltpu.VMEM
SMEM = pltpu.SMEM


def whole():
    return pl.BlockSpec(memory_space=VMEM)


def scalars():
    return pl.BlockSpec(memory_space=SMEM)


def core_groups(size):
    return [[CORES * level + core for level in range(size // CORES)] for core in range(CORES)]


def swap_core(value):
    pairs = [(source, source ^ 1) for source in range(lax.axis_size("tp"))]
    return lax.ppermute(value, "tp", pairs)


def exchange_levels(value):
    groups = core_groups(lax.axis_size("tp"))
    return lax.all_to_all(
        value, "tp", split_axis=0, concat_axis=0, axis_index_groups=groups, tiled=True
    )


def exchange_groups(value):
    return lax.all_to_all(value, "ep", split_axis=0, concat_axis=0, tiled=True)


def attention_kernel(spot_ref, mix_ref, bundle_ref, gain_ref, out_ref, scores, *, rows, scale):
    blocks, _, width = bundle_ref.shape
    share = out_ref.shape[1]
    splits = rows // share
    head, part = spot_ref[0], spot_ref[1]
    mix = mix_ref[head]
    half = width // 2
    lane = lax.broadcasted_iota(jnp.int32, (share, width), 1)
    row = lax.broadcasted_iota(jnp.int32, (share, rows), 0)
    column = lax.broadcasted_iota(jnp.int32, (share, rows), 1)
    contract = (((1,), (1,)), ((), ()))
    factor = scale * LOG2E
    for block in range(blocks):
        place = part if block % 2 == 0 else splits - 1 - part
        visible = column <= row + place * share
        queries = bundle_ref[block, 2 * rows :, :]
        sums = []
        for side in range(2):
            own = (lane < half) if side == 0 else (lane >= half)
            query = jnp.where(own, queries, jnp.zeros_like(queries))
            top = jnp.full((share, 1), NEG_FILL, jnp.float32)
            for other in range(block + 1):
                score = lax.dot_general(
                    query,
                    bundle_ref[other, :rows, :],
                    contract,
                    preferred_element_type=jnp.float32,
                )
                if other == block:
                    score = jnp.where(visible, score, NEG_FILL)
                scores[side, :, other * rows : (other + 1) * rows] = score
                top = jnp.maximum(top, jnp.max(score, axis=-1, keepdims=True))
            total = jnp.zeros((share, 1), jnp.float32)
            weighted = jnp.zeros((share, width), jnp.float32)
            for other in range(block + 1):
                score = scores[side, :, other * rows : (other + 1) * rows]
                weight = jnp.exp2((score - top) * factor)
                total += jnp.sum(weight, axis=-1, keepdims=True)
                weighted += jnp.dot(
                    weight.astype(jnp.bfloat16),
                    bundle_ref[other, rows : 2 * rows, :],
                    preferred_element_type=jnp.float32,
                )
            sums.append(weighted / total)
        blend = sums[0] - mix * sums[1]
        mean = jnp.mean(blend * blend, axis=-1, keepdims=True)
        scaled = blend * lax.rsqrt(mean + SUB_EPS)
        out_ref[block] = (scaled * gain_ref[...] * OUT_SCALE).astype(out_ref.dtype)


def attend_pack(queries, keys, values):
    rows, heads, width = queries.shape
    groups = lax.axis_size("ep")
    splits = groups // heads
    share = rows // splits
    odd = lax.axis_index("ep") % 2 == 1
    by_head = [jnp.transpose(value, (1, 0, 2)) for value in (queries, keys, values)]
    shares = by_head[0].reshape(heads, splits, share, width)
    shares = jnp.where(odd, shares[:, ::-1], shares)
    wide = (heads, splits, rows, width)
    bundle = jnp.concatenate(
        [
            jnp.broadcast_to(by_head[1][:, None], wide),
            jnp.broadcast_to(by_head[2][:, None], wide),
            shares,
        ],
        axis=2,
    )
    return bundle.reshape(groups, 2 * rows + share, width)


def attend_compute(bundle, mix_weight, sub_gain, rows):
    groups, tall, width = bundle.shape
    share = tall - 2 * rows
    splits = rows // share
    place = lax.axis_index("ep")
    spot = jnp.stack([place // splits, place % splits]).astype(jnp.int32)
    pairs = groups * (groups + 1) // 2 * share * rows * 2
    return pl.pallas_call(
        functools.partial(attention_kernel, rows=rows, scale=(width // 2) ** -0.5),
        out_shape=jax.ShapeDtypeStruct((groups, share, width), jnp.bfloat16),
        in_specs=[scalars(), scalars(), whole(), whole()],
        out_specs=whole(),
        scratch_shapes=[pltpu.VMEM((2, share, groups * rows), jnp.float32)],
        cost_estimate=pl.CostEstimate(
            flops=pairs * 4 * width, bytes_accessed=bundle.size * 2, transcendentals=pairs
        ),
        name="attention",
    )(spot, mix_weight, bundle, sub_gain[None, :])


def attend_unpack(returned, heads):
    groups, share, width = returned.shape
    splits = groups // heads
    odd = lax.axis_index("ep") % 2 == 1
    shares = returned.reshape(heads, splits, share, width)
    shares = jnp.where(odd, shares[:, ::-1], shares)
    return jnp.transpose(shares.reshape(heads, splits * share, width), (1, 0, 2))


def dispatch_kernel(routes_ref, rows_ref, *out_refs, capacity, pieces, experts):
    levels, rows, width = rows_ref.shape
    picks = routes_ref.shape[0]
    tall = max(experts, 16)
    expert = lax.broadcasted_iota(jnp.int32, (tall, rows), 0)
    named = jnp.zeros((tall, rows), jnp.bool_)
    for pick in range(picks):
        named = named | (routes_ref[pick : pick + 1, :] == expert)
    earlier = (
        lax.broadcasted_iota(jnp.int32, (rows, rows), 0)
        < lax.broadcasted_iota(jnp.int32, (rows, rows), 1)
    ).astype(jnp.float32)
    rank = jnp.dot(
        named.astype(jnp.float32).astype(jnp.bfloat16),
        earlier.astype(jnp.bfloat16),
        preferred_element_type=jnp.float32,
    )
    slots = (experts // pieces) * capacity
    slot = lax.broadcasted_iota(jnp.int32, (slots, rows), 0)
    for piece in range(pieces):
        chosen = jnp.zeros((slots, rows), jnp.bool_)
        for pick in range(picks):
            route = routes_ref[pick : pick + 1, :]
            mine = jnp.sum(jnp.where(expert == route, rank, 0.0), axis=0, keepdims=True)
            target = lax.div(route, pieces) * capacity + mine.astype(jnp.int32)
            target = jnp.where(lax.rem(route, pieces) == piece, target, -1)
            chosen = chosen | (slot == target)
        onehot = chosen.astype(jnp.float32).astype(jnp.bfloat16)
        for level in range(levels):
            out_refs[piece][:, level * width : (level + 1) * width] = jnp.dot(
                onehot, rows_ref[level], preferred_element_type=jnp.float32
            ).astype(jnp.bfloat16)


def dispatch(routes, by_level, capacity, pieces, experts):
    levels, rows, width = by_level.shape
    slots = experts // pieces * capacity
    return pl.pallas_call(
        functools.partial(dispatch_kernel, capacity=capacity, pieces=pieces, experts=experts),
        out_shape=[jax.ShapeDtypeStruct((slots, levels * width), jnp.bfloat16)] * pieces,
        in_specs=[whole(), whole()],
        out_specs=[whole()] * pieces,
        cost_estimate=pl.CostEstimate(
            flops=2 * slots * pieces * rows * levels * width,
            bytes_accessed=4 * slots * pieces * levels * width,
            transcendentals=0,
        ),
        name="dispatch",
    )(routes.T, by_level)


def expert_kernel(
    core_ref, own_ref, other_ref, gain_ref, gate_ref, up_ref, down_ref,
    kept_ref, sent_ref, normed, factor, hidden, *, width,
):
    step = pl.program_id(0)
    core = core_ref[0]
    levels = own_ref.shape[1] // width
    total_width = levels * CORES * width
    tile = gate_ref.shape[2]

    def column(level, side):
        start = (CORES * level + (core if side == 0 else 1 - core)) * width
        return pl.ds(pl.multiple_of(start, width), width)

    @pl.when(step == 0)
    def _():
        squares = jnp.zeros((own_ref.shape[0], 1), jnp.float32)
        for side, ref in ((0, own_ref), (1, other_ref)):
            for level in range(levels):
                floats = ref[:, level * width : (level + 1) * width].astype(jnp.float32)
                squares += jnp.sum(floats * floats, axis=-1, keepdims=True)
                place = column(level, side)
                normed[:, place] = (floats * gain_ref[:, place]).astype(jnp.bfloat16)
        factor[...] = lax.rsqrt(squares / total_width + NORM_EPS)

    gate = jnp.dot(normed[...], gate_ref[0], preferred_element_type=jnp.float32)
    up = jnp.dot(normed[...], up_ref[0], preferred_element_type=jnp.float32)
    gate = jnp.minimum(gate * factor[...], CLAMP_LIMIT)
    up = jnp.clip(up * factor[...], -CLAMP_LIMIT, CLAMP_LIMIT)
    value = ((up + 1.0) * gate * jax.nn.sigmoid(GLU_ALPHA * gate)).astype(jnp.bfloat16)
    hidden[:, pl.ds(pl.multiple_of(step * tile, tile), tile)] = value

    @pl.when(step == pl.num_programs(0) - 1)
    def _():
        for side, ref in ((1, sent_ref), (0, kept_ref)):
            for level in range(levels):
                ref[:, level * width : (level + 1) * width] = jnp.dot(
                    hidden[...],
                    down_ref[0, :, column(level, side)],
                    preferred_element_type=jnp.float32,
                ).astype(jnp.bfloat16)


def run_expert(piece, own, other, gain, gate_weight, up_weight, down_weight, width):
    slots, half = own.shape
    _, total_width, ff = gate_weight.shape
    tile = ff // 2 if ff % 512 == 0 else ff
    core = (lax.axis_index("tp") % CORES).astype(jnp.int32)[None]
    return pl.pallas_call(
        functools.partial(expert_kernel, width=width),
        out_shape=[jax.ShapeDtypeStruct((slots, half), jnp.bfloat16)] * 2,
        grid=(ff // tile,),
        in_specs=[
            scalars(),
            pl.BlockSpec((slots, half), lambda i: (0, 0)),
            pl.BlockSpec((slots, half), lambda i: (0, 0)),
            pl.BlockSpec((1, total_width), lambda i: (0, 0)),
            pl.BlockSpec((1, total_width, tile), lambda i: (piece, 0, i)),
            pl.BlockSpec((1, total_width, tile), lambda i: (piece, 0, i)),
            pl.BlockSpec((1, ff, total_width), lambda i: (piece, 0, 0)),
        ],
        out_specs=[pl.BlockSpec((slots, half), lambda i: (0, 0))] * 2,
        scratch_shapes=[
            pltpu.VMEM((slots, total_width), jnp.bfloat16),
            pltpu.VMEM((slots, 1), jnp.float32),
            pltpu.VMEM((slots, ff), jnp.bfloat16),
        ],
        compiler_params=pltpu.CompilerParams(
            dimension_semantics=("arbitrary",), vmem_limit_bytes=32 * 1024 * 1024
        ),
        cost_estimate=pl.CostEstimate(
            flops=6 * slots * total_width * ff,
            bytes_accessed=6 * total_width * ff + 8 * slots * half,
            transcendentals=slots * ff,
        ),
        name=f"expert_{piece}",
    )(core, own, other, gain[None, :], gate_weight, up_weight, down_weight)


def combine_kernel(routes_ref, weights_ref, *refs, capacity, pieces, experts):
    piece_refs, out_ref = refs[:pieces], refs[pieces]
    levels, rows, width = out_ref.shape
    picks = routes_ref.shape[1]
    wide = max(experts, 128)
    expert = lax.broadcasted_iota(jnp.int32, (rows, wide), 1)
    named = jnp.zeros((rows, wide), jnp.bool_)
    for pick in range(picks):
        named = named | (routes_ref[:, pick : pick + 1] == expert)
    earlier = (
        lax.broadcasted_iota(jnp.int32, (rows, rows), 1)
        < lax.broadcasted_iota(jnp.int32, (rows, rows), 0)
    ).astype(jnp.float32)
    rank = jnp.dot(
        earlier.astype(jnp.bfloat16),
        named.astype(jnp.float32).astype(jnp.bfloat16),
        preferred_element_type=jnp.float32,
    )
    slots = (experts // pieces) * capacity
    slot = lax.broadcasted_iota(jnp.int32, (rows, slots), 1)
    chosen = []
    for pick in range(picks):
        route = routes_ref[:, pick : pick + 1]
        mine = jnp.sum(jnp.where(expert == route, rank, 0.0), axis=1, keepdims=True)
        target = lax.div(route, pieces) * capacity + mine.astype(jnp.int32)
        for piece in range(pieces):
            here = jnp.where(lax.rem(route, pieces) == piece, target, -1)
            chosen.append((slot == here).astype(jnp.float32).astype(jnp.bfloat16))
    for level in range(levels):
        columns = slice(level * width, (level + 1) * width)
        total = jnp.zeros((rows, width), jnp.float32)
        for pick in range(picks):
            picked = jnp.zeros((rows, width), jnp.float32)
            for piece in range(pieces):
                picked += jnp.dot(
                    chosen[pick * pieces + piece],
                    piece_refs[piece][:, columns],
                    preferred_element_type=jnp.float32,
                )
            total += picked * weights_ref[:, pick : pick + 1]
        out_ref[level] = total.astype(jnp.bfloat16)


def combine(routes, route_weights, returned, capacity, levels, experts):
    rows, picks = routes.shape
    pieces = len(returned)
    slots, half = returned[0].shape
    return pl.pallas_call(
        functools.partial(combine_kernel, capacity=capacity, pieces=pieces, experts=experts),
        out_shape=jax.ShapeDtypeStruct((levels, rows, half // levels), jnp.bfloat16),
        in_specs=[whole()] * (2 + pieces),
        out_specs=whole(),
        cost_estimate=pl.CostEstimate(
            flops=2 * picks * pieces * slots * rows * half,
            bytes_accessed=2 * pieces * slots * half + 2 * rows * half,
            transcendentals=0,
        ),
        name="combine",
    )(routes, route_weights, *returned)


def shards(
    queries, keys, values, mix_weight, sub_gain, tokens, routes, route_weights,
    expert_gain, gate_weight, up_weight, down_weight,
):
    rows2, width = tokens.shape
    picks = routes.shape[1]
    groups, levels = lax.axis_size("ep"), lax.axis_size("tp") // CORES
    pieces = gate_weight.shape[0]
    experts = groups * pieces
    capacity = 3 * rows2 * picks // (2 * experts)

    by_level = exchange_levels(jnp.broadcast_to(tokens[None], (levels, rows2, width)))
    bundle = exchange_groups(attend_pack(queries, keys, values))
    outgoing = dispatch(routes, by_level, capacity, pieces, experts)
    slots, half = outgoing[0].shape
    layout = (groups, slots // groups, half)
    arrived = [exchange_groups(value.reshape(layout)).reshape(slots, half) for value in outgoing]
    attended = attend_compute(bundle, mix_weight, sub_gain, queries.shape[0])
    attended = exchange_groups(attended)
    returned = []
    for piece in range(pieces):
        own = arrived[piece]
        other = swap_core(own)
        kept, sent = run_expert(
            piece, own, other, expert_gain, gate_weight, up_weight, down_weight, width
        )
        partner = swap_core(sent)
        total = (kept.astype(jnp.float32) + partner.astype(jnp.float32)).astype(jnp.bfloat16)
        returned.append(exchange_groups(total.reshape(layout)).reshape(slots, half))
    combined = combine(routes, route_weights, returned, capacity, levels, experts)
    parts = exchange_levels(combined)
    moe_out = jnp.sum(parts.astype(jnp.float32), axis=0).astype(jnp.bfloat16)
    attn_out = attend_unpack(attended, queries.shape[1])
    return (attn_out, moe_out)


def solution(mesh):
    return jax.shard_map(
        shards,
        mesh=mesh,
        in_specs=(
            P("ep", "tp", None),
            P("ep", "tp", None),
            P("ep", "tp", None),
            P("tp"),
            P(),
            P("ep", "tp"),
            P("ep", None),
            P("ep", None),
            P(),
            P("ep", None, "tp"),
            P("ep", None, "tp"),
            P("ep", "tp", None),
        ),
        out_specs=(P("ep", "tp", None), P("ep", "tp")),
        check_vma=False,
    )
```

time: 176 us -> 145 us (0.82)
  waiting for transfers between devices: 79.4 us -> 35.9 us
  blocking collectives: 0 us -> 34.9 us
  Pallas kernels: 0 us -> 23.4 us
  matrix products: 22 us -> 0 us
  between operations: 17.1 us -> 0.84 us
  starting transfers between devices: 12.6 us -> 23 us
  other arithmetic: 16.4 us -> 6.12 us
  local copies, waits for them, and re-layouts: 25.2 us -> 19.2 us
  loops' own time: 2.99 us -> 0 us
    all_to_all x0 -> x2, blocking collectives: none -> 34.9 us  [the longest x1 20.7 us: exchange_levels(): lax.all_to_all(value, 'tp', split_axis=0, concat_axis=0, axis_index_group...]
    pallas_call x0 -> x5, Pallas kernels: none -> 23.4 us  [the longest x2 9.61 us: run_expert(): pl.pallas_call(functools.partial(expert_kernel, width=width), out_shape=[...]
    all_gather x3 -> x0, waiting for transfers between devices: 22.3 us -> none  [the longest x1 22.2 us: route_layer(): full_rows = lax.all_gather(tokens, 'tp', axis=1, tiled=True)]
    dot_general x10 -> x0, matrix products: 22 us -> none  [the longest x1 10 us: expert_finish(): jnp.einsum('secf,efd->secd', hidden, down_weight, preferred_element_type=...]
    all_to_all x2 -> x6, starting transfers between devices: 7.29 us -> 22.4 us  [the longest x5 18.3 us: exchange_groups(): return lax.all_to_all(value, 'ep', split_axis=0, concat_axis=0, tiled=True)]
    ppermute x4, waiting for transfers between devices: 13.9 us -> 0.01 us  [swap_core(): return lax.ppermute(value, 'tp', pairs)]
    unnamed x20 -> x32, local copies, waits for them, and re-layouts: 6.1 us -> 14.7 us
    all_to_all x2 -> x6, waiting for transfers between devices: 42.5 us -> 35.9 us  [the longest x5 23.2 us: exchange_groups(): return lax.all_to_all(value, 'ep', split_axis=0, concat_axis=0, tiled=True)]
  transfers between devices with their start and end apart: 10 -> 10, of which waited for: 5 -> 5; matrix products, arithmetic and copies ran while one was open for 29% -> 7% of each run, Pallas kernels for 0% -> 14%
where the time goes in v1:
time: 145 us; the launch traced here: 143 us
  waiting for transfers between devices  35.9 us (25%)
  blocking collectives  34.9 us (24%)
  Pallas kernels  23.4 us (16%)
  starting transfers between devices  23 us (16%)
  local copies, waits for them, and re-layouts  19.2 us (13%)
  other arithmetic  6.12 us (4%)
    all_to_all x5, waiting for transfers between devices, exchange_groups(): return lax.all_to_all(value, 'ep', split_axis=0, concat_axis=0, tiled=True)  23.2 us
    all_to_all x1, blocking collectives, exchange_levels(): lax.all_to_all(value, 'tp', split_axis=0, concat_axis=0, axis_index_group...  20.7 us
    all_to_all x5, starting transfers between devices, exchange_groups(): return lax.all_to_all(value, 'ep', split_axis=0, concat_axis=0, tiled=True)  18.3 us
    unnamed x32, local copies, waits for them, and re-layouts  14.7 us
    all_to_all x1, blocking collectives, exchange_groups(): return lax.all_to_all(value, 'ep', split_axis=0, concat_axis=0, tiled=True)  14.1 us
    all_to_all x1, waiting for transfers between devices, exchange_levels(): lax.all_to_all(value, 'tp', split_axis=0, concat_axis=0, axis_index_group...  12.7 us
    pallas_call x2, Pallas kernels, run_expert(): pl.pallas_call(functools.partial(expert_kernel, width=width), out_shape=[...  9.61 us
    pallas_call x1, Pallas kernels, attend_compute(): pl.pallas_call(functools.partial(attention_kernel, rows=rows, scale=(widt...  6.92 us
  transfers between devices with their start and end apart: 10, of which 5 were waited for; matrix products, arithmetic and copies ran while one was open for 7% of the time, Pallas kernels for 14%

profile of v1, /device:TPU:0, one launch (start us, length us, event | category | flops | bytes accessed | tf_op | source)
XLA Modules:
  0.0 143.5 jit_solution(4799323875367851711)
XLA Ops:
  1.6 20.7 %all_to_all.40.rows_ref = bf16[4,256,256]{2,1,0:T(8,128)(2,1)} all-to-all(bf16[4,256,256]{2,1,0:T(8,128)(2,1)S(1)} %broadcast_in_dim.16), channel_id=1, replica_groups={{0,2,4,6},{1,3,5,7},{8,10,12,14},{9,11,13,15},{16,18,20,22},{17,19,21,2..., dimensions={0} | all-to-all | bytes 1048576 | tf_op jit(solution)/shard_map/all_to_all | solution.py:42
  22.3 2.8 %dispatch.1 = (bf16[384,1024]{1,0:T(8,128)(2,1)}, bf16[384,1024]{1,0:T(8,128)(2,1)}) custom-call(s32[2,256]{1,0:T(2,128)} %bitcast.38, bf16[4,256,256]{2,1,0:T(8,128)(2,1)} %all_to_all.40.rows_ref), custom_call_target="tpu_custom_call" | custom-call | flops 402653184 | bytes 3145728 | tf_op jit(solution)/shard_map/dispatch/pallas_call | solution.py:188
  25.1 14.1 %all_to_all.41 = bf16[4,96,1024]{2,1,0:T(8,128)(2,1)S(1)} all-to-all(bf16[4,96,1024]{2,1,0:T(8,128)(2,1)} %bitcast.33), channel_id=1, replica_groups=mesh['ep'=4,'tp'=8] {'ep'}, dimensions={0} | all-to-all | bytes 1572864 | tf_op jit(solution)/shard_map/all_to_all | solution.py:48
  39.2 3.6 %all-to-all-start.3 = ((bf16[4,96,1024]{2,1,0:T(8,128)(2,1)}), bf16[4,96,1024]{2,1,0:T(8,128)(2,1)S(1)}, u32[]{:S(2)}, u32[]{:S(2)}) async-start(bf16[4,96,1024]{2,1,0:T(8,128)(2,1)} %bitcast.13), calls=%async_computation.3 | async-start | bytes 1572864 | tf_op jit(solution)/shard_map/all_to_all | solution.py:48
  43.0 8.2 %all-to-all-done.3 = bf16[4,96,1024]{2,1,0:T(8,128)(2,1)S(1)} async-done(((bf16[4,96,1024]{2,1,0:T(8,128)(2,1)}), bf16[4,96,1024]{2,1,0:T(8,128)(2,1)S(1)}, u32[]{:S(2)}, u32[]{:S(2)}) %all-to-all-start.3) | async-done | bytes 786464 | tf_op jit(solution)/shard_map/all_to_all | solution.py:48
  53.7 2.2 %copy-done = bf16[2,2048,512]{2,1,0:T(8,128)(2,1)S(1)} copy-done((bf16[2,2048,512]{2,1,0:T(8,128)(2,1)S(1)}, bf16[2,2048,512]{2,1,0:T(8,128)(2,1)}, u32[]{:S(2)}) %copy-start) | copy-done | bytes 4194328
  55.9 2.2 %copy-done.2 = bf16[2,2048,512]{2,1,0:T(8,128)(2,1)S(1)} copy-done((bf16[2,2048,512]{2,1,0:T(8,128)(2,1)S(1)}, bf16[2,2048,512]{2,1,0:T(8,128)(2,1)}, u32[]{:S(2)}) %copy-start.2) | copy-done | bytes 4194328
  58.1 2.2 %copy-done.4 = bf16[2,512,2048]{2,1,0:T(8,128)(2,1)S(1)} copy-done((bf16[2,512,2048]{2,1,0:T(8,128)(2,1)S(1)}, bf16[2,512,2048]{2,1,0:T(8,128)(2,1)}, u32[]{:S(2)}) %copy-start.4) | copy-done | bytes 4194328
  60.3 4.8 %expert_1.1 = (bf16[384,1024]{1,0:T(8,128)(2,1)S(1)}, bf16[384,1024]{1,0:T(8,128)(2,1)}) custom-call(s32[1]{0:T(128)} %bitcast.11.core_ref, bf16[384,1024]{1,0:T(8,128)(2,1)S(1)} %bitcast.27, bf16[384,1024]{1,0:T(8,128)(2,1)S(1)} %collective-permute-done.2.other_ref, f32[1,2048]{1,0:T(1,128)S(1)} %bitcast.28, bf16[2,2048,512]{2,1,0:T(8,128)(2,1)S(1)} %copy-done, ...), custom_call_target="tpu_custom_call" | custom-call | flops 2415919104 | bytes 9437184 | tf_op jit(solution)/shard_map/expert_1/pallas_call | solution.py:250
  66.9 4.3 %all-to-all-start = ((bf16[4,1280,128]{2,1,0:T(8,128)(2,1)}), bf16[4,1280,128]{2,1,0:T(8,128)(2,1)}, u32[]{:S(2)}, u32[]{:S(2)}) async-start(bf16[4,1280,128]{2,1,0:T(8,128)(2,1)} %bitcast.6), calls=%async_computation | async-start | bytes 2621440 | tf_op jit(solution)/shard_map/all_to_all | solution.py:48
  73.4 2.2 %copy-done.3 = bf16[2,2048,512]{2,1,0:T(8,128)(2,1)S(1)} copy-done((bf16[2,2048,512]{2,1,0:T(8,128)(2,1)S(1)}, bf16[2,2048,512]{2,1,0:T(8,128)(2,1)}, u32[]{:S(2)}) %copy-start.3) | copy-done | bytes 4194328
  75.6 2.2 %copy-done.5 = bf16[2,512,2048]{2,1,0:T(8,128)(2,1)S(1)} copy-done((bf16[2,512,2048]{2,1,0:T(8,128)(2,1)S(1)}, bf16[2,512,2048]{2,1,0:T(8,128)(2,1)}, u32[]{:S(2)}) %copy-start.5) | copy-done | bytes 4194328
  77.8 4.9 %expert_0.1 = (bf16[384,1024]{1,0:T(8,128)(2,1)S(1)}, bf16[384,1024]{1,0:T(8,128)(2,1)S(1)}) custom-call(s32[1]{0:T(128)} %bitcast.11.core_ref, bf16[384,1024]{1,0:T(8,128)(2,1)S(1)} %bitcast.25, bf16[384,1024]{1,0:T(8,128)(2,1)} %collective-permute-done.other_ref, f32[1,2048]{1,0:T(1,128)S(1)} %bitcast.29, bf16[2,2048,512]{2,1,0:T(8,128)(2,1)S(1)} %copy-done.1, ...), custom_call_target="tpu_custom_call" | custom-call | flops 2415919104 | bytes 9437184 | tf_op jit(solution)/shard_map/expert_0/pallas_call | solution.py:250
  82.7 2.3 %add_convert_fusion = bf16[384,1024]{1,0:T(8,128)(2,1)} fusion(bf16[384,1024]{1,0:T(8,128)(2,1)} %collective-permute-done.3, bf16[384,1024]{1,0:T(8,128)(2,1)S(1)} %get-tuple-element.12), kind=kLoop, calls=%fused_computation | loop fusion | flops 1572864 | bytes 2359296 | tf_op jit(solution)/shard_map/convert_element_type | solution.py:369
  85.1 3.1 %all-to-all-done.bundle_ref = bf16[4,1280,128]{2,1,0:T(8,128)(2,1)} async-done(((bf16[4,1280,128]{2,1,0:T(8,128)(2,1)}), bf16[4,1280,128]{2,1,0:T(8,128)(2,1)}, u32[]{:S(2)}, u32[]{:S(2)}) %all-to-all-start) | async-done | bytes 1310752 | tf_op jit(solution)/shard_map/all_to_all | solution.py:48
  88.1 3.5 %all-to-all-start.6 = ((bf16[4,96,1024]{2,1,0:T(8,128)(2,1)}), bf16[4,96,1024]{2,1,0:T(8,128)(2,1)S(1)}, u32[]{:S(2)}, u32[]{:S(2)}) async-start(bf16[4,96,1024]{2,1,0:T(8,128)(2,1)} %bitcast.20), calls=%async_computation.6 | async-start | bytes 1572864 | tf_op jit(solution)/shard_map/all_to_all | solution.py:48
  92.8 9.2 %all-to-all-done.6 = bf16[4,96,1024]{2,1,0:T(8,128)(2,1)S(1)} async-done(((bf16[4,96,1024]{2,1,0:T(8,128)(2,1)}), bf16[4,96,1024]{2,1,0:T(8,128)(2,1)S(1)}, u32[]{:S(2)}, u32[]{:S(2)}) %all-to-all-start.6) | async-done | bytes 786464 | tf_op jit(solution)/shard_map/all_to_all | solution.py:48
  102.0 3.5 %all-to-all-start.4 = ((bf16[4,96,1024]{2,1,0:T(8,128)(2,1)}), bf16[4,96,1024]{2,1,0:T(8,128)(2,1)S(1)}, u32[]{:S(2)}, u32[]{:S(2)}) async-start(bf16[4,96,1024]{2,1,0:T(8,128)(2,1)} %bitcast.16), calls=%async_computation.4 | async-start | bytes 1572864 | tf_op jit(solution)/shard_map/all_to_all | solution.py:48
  106.1 6.9 %attention.1 = bf16[4,256,128]{2,1,0:T(8,128)(2,1)} custom-call(s32[2]{0:T(128)} %pad_add_fusion.spot_ref, f32[2]{0:T(128)} %mix_ref.1, bf16[4,1280,128]{2,1,0:T(8,128)(2,1)} %all-to-all-done.bundle_ref, f32[1,128]{1,0:T(1,128)} %bitcast.39), custom_call_target="tpu_custom_call" | custom-call | flops 1342177280 | bytes 1310720 | tf_op jit(solution)/shard_map/attention/pallas_call | solution.py:129
  113.1 2.8 %all-to-all-done.4 = bf16[4,96,1024]{2,1,0:T(8,128)(2,1)S(1)} async-done(((bf16[4,96,1024]{2,1,0:T(8,128)(2,1)}), bf16[4,96,1024]{2,1,0:T(8,128)(2,1)S(1)}, u32[]{:S(2)}, u32[]{:S(2)}) %all-to-all-start.4) | async-done | bytes 786464 | tf_op jit(solution)/shard_map/all_to_all | solution.py:48
  115.8 3.4 %all-to-all-start.1 = ((bf16[4,256,128]{2,1,0:T(8,128)(2,1)}), bf16[4,256,128]{2,1,0:T(8,128)(2,1)S(1)}, u32[]{:S(2)}, u32[]{:S(2)}) async-start(bf16[4,256,128]{2,1,0:T(8,128)(2,1)} %attention.1), calls=%async_computation.1 | async-start | bytes 524288 | tf_op jit(solution)/shard_map/all_to_all | solution.py:48
  120.8 4.1 %combine.1 = bf16[4,256,256]{2,1,0:T(8,128)(2,1)} custom-call(s32[256,2]{1,0:T(8,128)} %copy.19.routes_ref, f32[256,2]{1,0:T(8,128)} %copy.20.weights_ref, bf16[384,1024]{1,0:T(8,128)(2,1)} %bitcast.32, bf16[384,1024]{1,0:T(8,128)(2,1)} %bitcast.31), custom_call_target="tpu_custom_call" | custom-call | flops 805306368 | bytes 2097152 | tf_op jit(solution)/shard_map/combine/pallas_call | solution.py:328
  124.9 4.0 %all-to-all-start.7 = ((bf16[4,256,256]{2,1,0:T(8,128)(2,1)}), bf16[4,256,256]{2,1,0:T(8,128)(2,1)S(1)}, u32[]{:S(2)}, u32[]{:S(2)}) async-start(bf16[4,256,256]{2,1,0:T(8,128)(2,1)} %combine.1), calls=%async_computation.7 | async-start | bytes 1048576 | tf_op jit(solution)/shard_map/all_to_all | solution.py:42
  130.0 12.7 %all-to-all-done.7 = bf16[4,256,256]{2,1,0:T(8,128)(2,1)S(1)} async-done(((bf16[4,256,256]{2,1,0:T(8,128)(2,1)}), bf16[4,256,256]{2,1,0:T(8,128)(2,1)S(1)}, u32[]{:S(2)}, u32[]{:S(2)}) %all-to-all-start.7) | async-done | bytes 524320 | tf_op jit(solution)/shard_map/all_to_all | solution.py:42
  (49 shorter events, 12.8 us)
Async XLA Ops:
  25.1 17.9 %copy-start.11 = (bf16[512,2,128]{2,1,0:T(2,128)(2,1)S(1)}, bf16[512,2,128]{2,1,0:T(2,128)(2,1)}, u32[]{:S(2)}) copy-start(bf16[512,2,128]{2,1,0:T(2,128)(2,1)} %param.12) | copy-start | bytes 786436
  39.2 12.1 %copy-start.12 = (bf16[512,2,128]{2,1,0:T(2,128)(2,1)S(1)}, bf16[512,2,128]{2,1,0:T(2,128)(2,1)}, u32[]{:S(2)}) copy-start(bf16[512,2,128]{2,1,0:T(2,128)(2,1)} %param.13) | copy-start | bytes 786436
  39.2 14.5 %copy-start.6 = (f32[2048]{0:T(1024)S(1)}, f32[2048]{0:T(1024)}, u32[]{:S(2)}) copy-start(f32[2048]{0:T(1024)} %param.20) | copy-start | bytes 24580
  39.2 12.0 %all-to-all-start.3 = ((bf16[4,96,1024]{2,1,0:T(8,128)(2,1)}), bf16[4,96,1024]{2,1,0:T(8,128)(2,1)S(1)}, u32[]{:S(2)}, u32[]{:S(2)}) async-start(bf16[4,96,1024]{2,1,0:T(8,128)(2,1)} %bitcast.13), calls=%async_computation.3 | async-start | bytes 1572864 | tf_op jit(solution)/shard_map/all_to_all | solution.py:48
  42.8 10.9 %collective-permute-start.2 = (bf16[384,1024]{1,0:T(8,128)(2,1)S(1)}, bf16[384,1024]{1,0:T(8,128)(2,1)S(1)}, u32[]{:S(2)}, u32[]{:S(2)}) collective-permute-start(bf16[384,1024]{1,0:T(8,128)(2,1)S(1)} %bitcast.26), channel_id=1, source_target_pairs={{0,1},{1,0},{2,3},{3,2},{4,5},{5,4},{6,7},{7,6},{8,9},{9,8},{10,11... | collective-permute-start | bytes 2359304 | tf_op jit(solution)/shard_map/ppermute | solution.py:37
  51.2 20.0 %collective-permute-start = (bf16[384,1024]{1,0:T(8,128)(2,1)S(1)}, bf16[384,1024]{1,0:T(8,128)(2,1)}, u32[]{:S(2)}, u32[]{:S(2)}) collective-permute-start(bf16[384,1024]{1,0:T(8,128)(2,1)S(1)} %bitcast.24), channel_id=1, source_target_pairs={{0,1},{1,0},{2,3},{3,2},{4,5},{5,4},{6,7},{7,6},{8,9},{9,8},{10,11... | collective-permute-start | bytes 2359304 | tf_op jit(solution)/shard_map/ppermute | solution.py:37
  53.7 2.2 %copy-start = (bf16[2,2048,512]{2,1,0:T(8,128)(2,1)S(1)}, bf16[2,2048,512]{2,1,0:T(8,128)(2,1)}, u32[]{:S(2)}) copy-start(bf16[2,2048,512]{2,1,0:T(8,128)(2,1)} %gate_ref.3) | copy-start | bytes 12582916
  55.9 2.2 %copy-start.2 = (bf16[2,2048,512]{2,1,0:T(8,128)(2,1)S(1)}, bf16[2,2048,512]{2,1,0:T(8,128)(2,1)}, u32[]{:S(2)}) copy-start(bf16[2,2048,512]{2,1,0:T(8,128)(2,1)} %up_ref.3) | copy-start | bytes 12582916
  60.3 5.3 %copy-start.8 = (bf16[2,512,128]{2,1,0:T(8,128)(2,1)S(1)}, bf16[2,512,128]{2,1,0:T(8,128)(2,1)}, u32[]{:S(2)}) copy-start(bf16[2,512,128]{2,1,0:T(8,128)(2,1)} %copy.14) | copy-start | bytes 786436
  60.3 5.4 %copy-start.7 = (bf16[2,512,128]{2,1,0:T(8,128)(2,1)S(1)}, bf16[2,512,128]{2,1,0:T(8,128)(2,1)}, u32[]{:S(2)}) copy-start(bf16[2,512,128]{2,1,0:T(8,128)(2,1)} %copy.15) | copy-start | bytes 786436
  65.1 17.7 %collective-permute-start.3 = (bf16[384,1024]{1,0:T(8,128)(2,1)}, bf16[384,1024]{1,0:T(8,128)(2,1)}, u32[]{:S(2)}, u32[]{:S(2)}) collective-permute-start(bf16[384,1024]{1,0:T(8,128)(2,1)} %get-tuple-element.13), channel_id=1, source_target_pairs={{0,1},{1,0},{2,3},{3,2},{4,5},{5,4},{6,7},{7,6},{8,9},{9,8},{10,11... | collective-permute-start | bytes 2359304 | tf_op jit(solution)/shard_map/ppermute | solution.py:37
  66.9 21.3 %all-to-all-start = ((bf16[4,1280,128]{2,1,0:T(8,128)(2,1)}), bf16[4,1280,128]{2,1,0:T(8,128)(2,1)}, u32[]{:S(2)}, u32[]{:S(2)}) async-start(bf16[4,1280,128]{2,1,0:T(8,128)(2,1)} %bitcast.6), calls=%async_computation | async-start | bytes 2621440 | tf_op jit(solution)/shard_map/all_to_all | solution.py:48
  71.2 2.2 %copy-start.1 = (bf16[2,2048,512]{2,1,0:T(8,128)(2,1)S(1)}, bf16[2,2048,512]{2,1,0:T(8,128)(2,1)}, u32[]{:S(2)}) copy-start(bf16[2,2048,512]{2,1,0:T(8,128)(2,1)} %gate_ref.3) | copy-start | bytes 12582916
  73.4 2.2 %copy-start.3 = (bf16[2,2048,512]{2,1,0:T(8,128)(2,1)S(1)}, bf16[2,2048,512]{2,1,0:T(8,128)(2,1)}, u32[]{:S(2)}) copy-start(bf16[2,2048,512]{2,1,0:T(8,128)(2,1)} %up_ref.3) | copy-start | bytes 12582916
  75.6 2.2 %copy-start.5 = (bf16[2,512,2048]{2,1,0:T(8,128)(2,1)S(1)}, bf16[2,512,2048]{2,1,0:T(8,128)(2,1)}, u32[]{:S(2)}) copy-start(bf16[2,512,2048]{2,1,0:T(8,128)(2,1)} %down_ref.3) | copy-start | bytes 12582916
  82.6 9.0 %collective-permute-start.1 = (bf16[384,1024]{1,0:T(8,128)(2,1)S(1)}, bf16[384,1024]{1,0:T(8,128)(2,1)S(1)}, u32[]{:S(2)}, u32[]{:S(2)}) collective-permute-start(bf16[384,1024]{1,0:T(8,128)(2,1)S(1)} %get-tuple-element.10), channel_id=1, source_target_pairs={{0,1},{1,0},{2,3},{3,2},{4,5},{5,4},{6,7},{7,6},{8,9},{9,8},{10,11... | collective-permute-start | bytes 2359304 | tf_op jit(solution)/shard_map/ppermute | solution.py:37
  88.1 13.9 %all-to-all-start.6 = ((bf16[4,96,1024]{2,1,0:T(8,128)(2,1)}), bf16[4,96,1024]{2,1,0:T(8,128)(2,1)S(1)}, u32[]{:S(2)}, u32[]{:S(2)}) async-start(bf16[4,96,1024]{2,1,0:T(8,128)(2,1)} %bitcast.20), calls=%async_computation.6 | async-start | bytes 1572864 | tf_op jit(solution)/shard_map/all_to_all | solution.py:48
  102.0 11.0 %copy-start.9 = (bf16[4,96,1024]{2,1,0:T(8,128)(2,1)}, bf16[4,96,1024]{2,1,0:T(8,128)(2,1)S(1)}, u32[]{:S(2)}) copy-start(bf16[4,96,1024]{2,1,0:T(8,128)(2,1)S(1)} %all-to-all-done.6) | copy-start | bytes 2359300
  102.0 13.8 %all-to-all-start.4 = ((bf16[4,96,1024]{2,1,0:T(8,128)(2,1)}), bf16[4,96,1024]{2,1,0:T(8,128)(2,1)S(1)}, u32[]{:S(2)}, u32[]{:S(2)}) async-start(bf16[4,96,1024]{2,1,0:T(8,128)(2,1)} %bitcast.16), calls=%async_computation.4 | async-start | bytes 1572864 | tf_op jit(solution)/shard_map/all_to_all | solution.py:48
  106.1 13.1 %copy-start.13 = (s32[256,2]{0,1:T(2,128)S(1)}, s32[256,2]{0,1:T(2,128)}, u32[]{:S(2)}) copy-start(s32[256,2]{0,1:T(2,128)} %param.18) | copy-start | bytes 6148
  106.1 13.9 %copy-start.14 = (f32[256,2]{0,1:T(2,128)S(1)}, f32[256,2]{0,1:T(2,128)}, u32[]{:S(2)}) copy-start(f32[256,2]{0,1:T(2,128)} %param.19) | copy-start | bytes 6148
  115.8 5.0 %copy-start.10 = (bf16[4,96,1024]{2,1,0:T(8,128)(2,1)}, bf16[4,96,1024]{2,1,0:T(8,128)(2,1)S(1)}, u32[]{:S(2)}) copy-start(bf16[4,96,1024]{2,1,0:T(8,128)(2,1)S(1)} %all-to-all-done.4) | copy-start | bytes 2359300
  115.8 9.1 %all-to-all-start.1 = ((bf16[4,256,128]{2,1,0:T(8,128)(2,1)}), bf16[4,256,128]{2,1,0:T(8,128)(2,1)S(1)}, u32[]{:S(2)}, u32[]{:S(2)}) async-start(bf16[4,256,128]{2,1,0:T(8,128)(2,1)} %attention.1), calls=%async_computation.1 | async-start | bytes 524288 | tf_op jit(solution)/shard_map/all_to_all | solution.py:48
  124.9 17.8 %all-to-all-start.7 = ((bf16[4,256,256]{2,1,0:T(8,128)(2,1)}), bf16[4,256,256]{2,1,0:T(8,128)(2,1)S(1)}, u32[]{:S(2)}, u32[]{:S(2)}) async-start(bf16[4,256,256]{2,1,0:T(8,128)(2,1)} %combine.1), calls=%async_computation.7 | async-start | bytes 1048576 | tf_op jit(solution)/shard_map/all_to_all | solution.py:42
  (1 other events, 2.2 us)

commit v2 on v0

v2 whole, which is shorter than its diff:
```python
import functools

import jax
import jax.numpy as jnp
from jax import lax
from jax.experimental import pallas as pl
from jax.experimental.pallas import tpu as pltpu
from jax.sharding import PartitionSpec as P


NEG_FILL = -1e30
SUB_EPS = 1e-05
NORM_EPS = 1e-06
CLAMP_LIMIT = 7.0
GLU_ALPHA = 1.702
OUT_SCALE = 0.8
LOG2E = 1.4426950408889634
CORES = 2
BF16 = jnp.bfloat16
F32 = jnp.float32


def whole():
    return pl.BlockSpec(memory_space=pltpu.VMEM)


def far():
    return pl.BlockSpec(memory_space=pl.ANY)


def weights():
    return pl.BlockSpec(memory_space=pltpu.HBM)


def scalars():
    return pl.BlockSpec(memory_space=pltpu.SMEM)


def shape_of(*sizes, dtype=BF16):
    return jax.ShapeDtypeStruct(sizes, dtype)


def grant(mebibytes, groups=4):
    size = min(60, mebibytes * max(1, groups // 4))
    return pltpu.CompilerParams(vmem_limit_bytes=size * 1024 * 1024)


def cost(flops, data, transcendentals=0):
    return pl.CostEstimate(
        flops=int(flops), bytes_accessed=int(data), transcendentals=int(transcendentals)
    )


def flip(value, axis, mask):
    pairs = [(source, source ^ mask) for source in range(lax.axis_size(axis))]
    return lax.ppermute(value, axis, pairs)


def levels_flip(value, mask):
    return flip(value, "tp", CORES * mask)


def cores_flip(value):
    return flip(value, "tp", 1)


def exchange(values):
    out = [values[0]]
    for mask in range(1, len(values)):
        out.append(flip(values[mask], "ep", mask))
    return out


def share_at(part, block, splits):
    return jnp.where(block % 2 == 0, part, splits - 1 - part)


def pack_kernel(place_ref, queries_ref, keys_ref, values_ref, *out_refs):
    place = place_ref[0]
    heads, rows, _ = keys_ref.shape
    splits = len(out_refs) // heads
    share = rows // splits
    for mask, out_ref in enumerate(out_refs):
        target = jnp.bitwise_xor(place, mask)
        head = lax.div(target, splits)
        start = share_at(lax.rem(target, splits), place, splits) * share
        out_ref[:rows] = keys_ref[head]
        out_ref[rows : 2 * rows] = values_ref[head]
        out_ref[2 * rows :] = queries_ref[head, pl.ds(pl.multiple_of(start, share), share)]


def pack(place, queries, keys, values, groups):
    rows, heads, width = queries.shape
    tall = 2 * rows + rows * heads // groups
    return pl.pallas_call(
        pack_kernel,
        out_shape=[shape_of(tall, width)] * groups,
        in_specs=[scalars(), whole(), whole(), whole()],
        out_specs=[whole()] * groups,
        cost_estimate=cost(2**21, 2 * groups * tall * width),
        compiler_params=grant(8),
        name="pack",
    )(place, *[jnp.transpose(value, (1, 0, 2)) for value in (queries, keys, values)])


def attention_kernel(place_ref, mix_ref, *refs, groups, rows, heads, scale):
    bundle_refs, gain_ref = refs[:groups], refs[groups]
    out_refs = refs[groups + 1 : 2 * groups + 1]
    bundle, outputs, scores, arrivals = refs[2 * groups + 1 :]
    place = place_ref[0]
    copies = []
    for mask in range(groups):
        copies.append(
            pltpu.make_async_copy(
                bundle_refs[mask], bundle.at[jnp.bitwise_xor(place, mask)], arrivals.at[mask]
            )
        )
    for copy in copies:
        copy.start()
    share, width = out_refs[0].shape
    splits = groups // heads
    mix = mix_ref[lax.div(place, splits)]
    part = lax.rem(place, splits)
    half = width // 2
    lane = lax.broadcasted_iota(jnp.int32, (share, width), 1)
    row = lax.broadcasted_iota(jnp.int32, (share, rows), 0)
    column = lax.broadcasted_iota(jnp.int32, (share, rows), 1)
    contract = (((1,), (1,)), ((), ()))
    factor = scale * LOG2E
    for copy in copies:
        copy.wait()
    for block in range(groups):
        visible = column <= row + (part if block % 2 == 0 else splits - 1 - part) * share
        queries = bundle[block, 2 * rows :, :]
        sums = []
        for side in range(2):
            own = (lane < half) if side == 0 else (lane >= half)
            query = jnp.where(own, queries, jnp.zeros_like(queries))
            top = jnp.full((share, 1), NEG_FILL, F32)
            for other in range(block + 1):
                score = lax.dot_general(
                    query, bundle[other, :rows, :], contract, preferred_element_type=F32
                )
                if other == block:
                    score = jnp.where(visible, score, NEG_FILL)
                scores[side, :, other * rows : (other + 1) * rows] = score
                top = jnp.maximum(top, jnp.max(score, axis=-1, keepdims=True))
            total = jnp.zeros((share, 1), F32)
            weighted = jnp.zeros((share, width), F32)
            for other in range(block + 1):
                score = scores[side, :, other * rows : (other + 1) * rows]
                weight = jnp.exp2((score - top) * factor)
                total += jnp.sum(weight, axis=-1, keepdims=True)
                weighted += jnp.dot(
                    weight.astype(BF16),
                    bundle[other, rows : 2 * rows, :],
                    preferred_element_type=F32,
                )
            sums.append(weighted / total)
        blend = sums[0] - mix * sums[1]
        mean = jnp.mean(blend * blend, axis=-1, keepdims=True)
        scaled = blend * lax.rsqrt(mean + SUB_EPS)
        outputs[block] = (scaled * gain_ref[...] * OUT_SCALE).astype(BF16)
    for mask in range(groups):
        out_refs[mask][...] = outputs[jnp.bitwise_xor(place, mask)]


def attention(place, bundles, mix_weight, sub_gain, rows):
    groups, heads = len(bundles), mix_weight.shape[0]
    tall, width = bundles[0].shape
    share = tall - 2 * rows
    pairs = groups * (groups + 1) // 2 * share * rows * 2
    return pl.pallas_call(
        functools.partial(
            attention_kernel, groups=groups, rows=rows, heads=heads, scale=(width // 2) ** -0.5
        ),
        out_shape=[shape_of(share, width)] * groups,
        in_specs=[scalars(), scalars()] + [far()] * groups + [whole()],
        out_specs=[whole()] * groups,
        scratch_shapes=[
            pltpu.VMEM((groups, tall, width), BF16),
            pltpu.VMEM((groups, share, width), BF16),
            pltpu.VMEM((2, share, groups * rows), F32),
            pltpu.SemaphoreType.DMA((groups,)),
        ],
        cost_estimate=cost(pairs * 4 * width, 2 * groups * tall * width, pairs),
        compiler_params=grant(16, groups),
        name="attention",
    )(place, mix_weight, *bundles, sub_gain[None, :])


def unpack_kernel(place_ref, *refs):
    part_refs, out_ref = refs[:-1], refs[-1]
    place = place_ref[0]
    groups, share = len(part_refs), part_refs[0].shape[0]
    splits = groups // out_ref.shape[0]
    for mask, ref in enumerate(part_refs):
        source = jnp.bitwise_xor(place, mask)
        start = share_at(lax.rem(source, splits), place, splits) * share
        out_ref[lax.div(source, splits), pl.ds(pl.multiple_of(start, share), share)] = ref[...]


def unpack(place, parts, heads):
    groups = len(parts)
    share, width = parts[0].shape
    rows = share * groups // heads
    by_head = pl.pallas_call(
        unpack_kernel,
        out_shape=shape_of(heads, rows, width),
        in_specs=[scalars()] + [whole()] * groups,
        out_specs=whole(),
        cost_estimate=cost(2**20, 4 * heads * rows * width),
        compiler_params=grant(4),
        name="unpack",
    )(place, *parts)
    return jnp.transpose(by_head, (1, 0, 2))


def ranks(named, strictly, axis):
    table = named.astype(F32).astype(BF16)
    earlier = strictly.astype(F32).astype(BF16)
    pair = (table, earlier) if axis == 1 else (earlier, table)
    return jnp.dot(*pair, preferred_element_type=F32)


def dispatch_kernel(place_ref, routes_ref, *refs, capacity, pieces, experts, groups):
    level_refs, out_refs = refs[:-groups], refs[-groups:]
    place = place_ref[0]
    rows, width = level_refs[0].shape
    picks = routes_ref.shape[0]
    tall = max(experts, 16)
    expert = lax.broadcasted_iota(jnp.int32, (tall, rows), 0)
    named = jnp.zeros((tall, rows), jnp.bool_)
    for pick in range(picks):
        named = named | (routes_ref[pick : pick + 1, :] == expert)
    first = lax.broadcasted_iota(jnp.int32, (rows, rows), 0)
    second = lax.broadcasted_iota(jnp.int32, (rows, rows), 1)
    rank = ranks(named, first < second, 1)
    targets = []
    for pick in range(picks):
        route = routes_ref[pick : pick + 1, :]
        mine = jnp.sum(jnp.where(expert == route, rank, 0.0), axis=0, keepdims=True)
        targets.append(route * capacity + mine.astype(jnp.int32))
    slots = pieces * capacity
    slot = lax.broadcasted_iota(jnp.int32, (slots, rows), 0)
    for mask in range(groups):
        here = slot + jnp.bitwise_xor(place, mask) * slots
        chosen = jnp.zeros((slots, rows), jnp.bool_)
        for pick in range(picks):
            chosen = chosen | (here == targets[pick])
        onehot = chosen.astype(F32).astype(BF16)
        for level, ref in enumerate(level_refs):
            out_refs[mask][:, level * width : (level + 1) * width] = jnp.dot(
                onehot, ref[...], preferred_element_type=F32
            ).astype(BF16)


def dispatch(place, routes, by_level, capacity, pieces, experts, groups):
    rows, width = by_level[0].shape
    slots, wide = pieces * capacity, len(by_level) * width
    return pl.pallas_call(
        functools.partial(
            dispatch_kernel, capacity=capacity, pieces=pieces, experts=experts, groups=groups
        ),
        out_shape=[shape_of(slots, wide)] * groups,
        in_specs=[scalars(), whole()] + [whole()] * len(by_level),
        out_specs=[whole()] * groups,
        cost_estimate=cost(2 * groups * slots * rows * wide, 4 * groups * slots * wide),
        compiler_params=grant(8),
        name="dispatch",
    )(place, routes.T, *by_level)


def block_start(spot_ref, level, side, width):
    core = spot_ref[2] if side == 0 else 1 - spot_ref[2]
    return (CORES * jnp.bitwise_xor(spot_ref[1], level) + core) * width


def hidden_kernel(spot_ref, *refs, count, groups, capacity, width):
    slot_refs, (gain_ref, gate_hbm, up_hbm, hidden_ref) = refs[:count], refs[count : count + 4]
    normed, gate_vmem, up_vmem, arrivals = refs[count + 4 :]
    pieces, total_width, _ = gate_hbm.shape
    tile = gate_vmem.shape[2]
    steps = gate_vmem.shape[0] // pieces
    chunks = count // groups // 2
    span = slot_refs[0].shape[1] // width
    copies = []
    for index in range(pieces * steps):
        columns = pl.ds(index % steps * tile, tile)
        for kind, (source, target) in enumerate(((gate_hbm, gate_vmem), (up_hbm, up_vmem))):
            copies.append(
                pltpu.make_async_copy(
                    source.at[index // steps, :, columns],
                    target.at[index],
                    arrivals.at[2 * index + kind],
                )
            )
    for copy in copies:
        copy.start()
    factors = [[None] * groups for _ in range(pieces)]
    for group in range(groups):
        squares = jnp.zeros((pieces * capacity, 1), F32)
        for side in range(CORES):
            for chunk in range(chunks):
                ref = slot_refs[(side * chunks + chunk) * groups + group]
                for inner in range(span):
                    floats = ref[:, inner * width : (inner + 1) * width].astype(F32)
                    squares += jnp.sum(floats * floats, axis=-1, keepdims=True)
                    start = block_start(spot_ref, chunk * span + inner, side, width)
                    place = pl.ds(pl.multiple_of(start, width), width)
                    value = (floats * gain_ref[:, place]).astype(BF16)
                    for piece in range(pieces):
                        normed[piece, group * capacity : (group + 1) * capacity, place] = value[
                            piece * capacity : (piece + 1) * capacity
                        ]
        factor = lax.rsqrt(squares / total_width + NORM_EPS)
        for piece in range(pieces):
            factors[piece][group] = factor[piece * capacity : (piece + 1) * capacity]
    for piece in range(pieces):
        factor = jnp.concatenate(factors[piece], axis=0)
        for step in range(steps):
            index = piece * steps + step
            copies[2 * index].wait()
            gate = jnp.dot(normed[piece], gate_vmem[index], preferred_element_type=F32)
            copies[2 * index + 1].wait()
            up = jnp.dot(normed[piece], up_vmem[index], preferred_element_type=F32)
            gate = jnp.minimum(gate * factor, CLAMP_LIMIT)
            up = jnp.clip(up * factor, -CLAMP_LIMIT, CLAMP_LIMIT)
            hidden_ref[piece, :, step * tile : (step + 1) * tile] = (
                (up + 1.0) * gate * jax.nn.sigmoid(GLU_ALPHA * gate)
            ).astype(BF16)


def hidden_units(spot, own, other, gain, gate_weight, up_weight, groups, capacity, width):
    pieces, total_width, ff = gate_weight.shape
    tile = 256 if ff % 256 == 0 else ff
    steps = ff // tile
    tables = [table for side in (own, other) for chunk in side for table in chunk]
    rows = groups * capacity
    return pl.pallas_call(
        functools.partial(
            hidden_kernel, count=len(tables), groups=groups, capacity=capacity, width=width
        ),
        out_shape=shape_of(pieces, rows, ff),
        in_specs=[scalars()] + [whole()] * (len(tables) + 1) + [weights()] * 2,
        out_specs=whole(),
        scratch_shapes=[
            pltpu.VMEM((pieces, rows, total_width), BF16),
            pltpu.VMEM((pieces * steps, total_width, tile), BF16),
            pltpu.VMEM((pieces * steps, total_width, tile), BF16),
            pltpu.SemaphoreType.DMA((2 * pieces * steps,)),
        ],
        cost_estimate=cost(
            4 * pieces * rows * total_width * ff,
            4 * pieces * total_width * (ff + rows),
            pieces * rows * ff,
        ),
        compiler_params=grant(24),
        name="hidden",
    )(spot, *tables, gain[None, :], gate_weight, up_weight)


def down_kernel(
    spot_ref, hidden_ref, down_hbm, sent_ref, kept_ref, down_vmem, arrivals,
    *, groups, capacity, width, start,
):
    pieces = hidden_ref.shape[0]
    part = sent_ref.shape[1]
    copies = []
    blocks = arrivals.shape[0] // (pieces * CORES)
    piece_width = part // blocks
    for side in (1, 0):
        for piece in range(pieces):
            for level in range(blocks):
                offset = block_start(spot_ref, level, side, width) + start
                index = (side * pieces + piece) * blocks + level
                copies.append(
                    pltpu.make_async_copy(
                        down_hbm.at[
                            piece, :, pl.ds(pl.multiple_of(offset, piece_width), piece_width)
                        ],
                        down_vmem.at[
                            side * pieces + piece,
                            :,
                            pl.ds(level * piece_width, piece_width),
                        ],
                        arrivals.at[index],
                    )
                )
    for copy in copies:
        copy.start()
    taken = 0
    for side, ref in ((1, sent_ref), (0, kept_ref)):
        for piece in range(pieces):
            for copy in copies[taken : taken + blocks]:
                copy.wait()
            taken += blocks
            value = jnp.dot(
                hidden_ref[piece],
                down_vmem[side * pieces + piece],
                preferred_element_type=F32,
            ).astype(BF16)
            for group in range(groups):
                row = (group * pieces + piece) * capacity
                ref[row : row + capacity] = value[group * capacity : (group + 1) * capacity]


def down(spot, hidden, down_weight, groups, capacity, width, levels, start, piece_width):
    pieces, rows, ff = hidden.shape
    part = levels * piece_width
    return pl.pallas_call(
        functools.partial(
            down_kernel, groups=groups, capacity=capacity, width=width, start=start
        ),
        out_shape=[shape_of(pieces * rows, part)] * 2,
        in_specs=[scalars(), whole(), weights()],
        out_specs=[whole()] * 2,
        scratch_shapes=[
            pltpu.VMEM((CORES * pieces, ff, part), BF16),
            pltpu.SemaphoreType.DMA((CORES * pieces * levels,)),
        ],
        cost_estimate=cost(
            2 * CORES * pieces * rows * ff * part, 2 * CORES * pieces * part * (ff + rows)
        ),
        compiler_params=grant(10),
        name="down",
    )(spot, hidden, down_weight)


def add_kernel(kept_ref, partner_ref, *out_refs):
    rows = out_refs[0].shape[0]
    for group, ref in enumerate(out_refs):
        place = slice(group * rows, (group + 1) * rows)
        ref[...] = (kept_ref[place].astype(F32) + partner_ref[place].astype(F32)).astype(BF16)


def add_cores(kept, partner, groups):
    rows, width = kept.shape
    return pl.pallas_call(
        add_kernel,
        out_shape=[shape_of(rows // groups, width)] * groups,
        in_specs=[whole()] * 2,
        out_specs=[whole()] * groups,
        cost_estimate=cost(2**21, 6 * rows * width),
        compiler_params=grant(6),
        name="add_cores",
    )(kept, partner)


def plan_kernel(place_ref, routes_ref, out_ref, *, capacity, pieces, experts):
    rows, picks = routes_ref.shape
    slots = out_ref.shape[2]
    groups = out_ref.shape[0] // picks
    wide = max(experts, 128)
    expert = lax.broadcasted_iota(jnp.int32, (rows, wide), 1)
    named = jnp.zeros((rows, wide), jnp.bool_)
    for pick in range(picks):
        named = named | (routes_ref[:, pick : pick + 1] == expert)
    first = lax.broadcasted_iota(jnp.int32, (rows, rows), 0)
    second = lax.broadcasted_iota(jnp.int32, (rows, rows), 1)
    rank = ranks(named, second < first, 0)
    slot = lax.broadcasted_iota(jnp.int32, (rows, slots), 1)
    for pick in range(picks):
        route = routes_ref[:, pick : pick + 1]
        mine = jnp.sum(jnp.where(expert == route, rank, 0.0), axis=1, keepdims=True)
        target = route * capacity + mine.astype(jnp.int32)
        for mask in range(groups):
            here = slot + jnp.bitwise_xor(place_ref[0], mask) * slots
            out_ref[pick * groups + mask] = (here == target).astype(F32).astype(BF16)


def plan(place, routes, capacity, pieces, experts, groups):
    rows, picks = routes.shape
    slots = pieces * capacity
    return pl.pallas_call(
        functools.partial(plan_kernel, capacity=capacity, pieces=pieces, experts=experts),
        out_shape=shape_of(picks * groups, rows, slots),
        in_specs=[scalars(), whole()],
        out_specs=whole(),
        cost_estimate=cost(2**25, 2 * picks * groups * rows * slots),
        compiler_params=grant(6),
        name="plan",
    )(place, routes)


def gather_kernel(chosen_ref, weights_ref, *refs, groups):
    table_refs, out_refs = refs[:groups], refs[groups:]
    picks = chosen_ref.shape[0] // groups
    width = out_refs[0].shape[1]
    total = None
    for pick in range(picks):
        picked = None
        for group in range(groups):
            part = jnp.dot(
                chosen_ref[pick * groups + group],
                table_refs[group][...],
                preferred_element_type=F32,
            )
            picked = part if picked is None else picked + part
        picked = picked * weights_ref[:, pick : pick + 1]
        total = picked if total is None else total + picked
    for level, ref in enumerate(out_refs):
        ref[...] = total[:, level * width : (level + 1) * width].astype(BF16)


def gather(chosen, route_weights, tables, levels):
    groups = len(tables)
    rows, picks = route_weights.shape
    slots, width = tables[0].shape
    return pl.pallas_call(
        functools.partial(gather_kernel, groups=groups),
        out_shape=[shape_of(rows, width // levels)] * levels,
        in_specs=[whole()] * (2 + groups),
        out_specs=[whole()] * levels,
        cost_estimate=cost(
            2 * picks * groups * slots * rows * width,
            2 * groups * slots * (width + picks * rows) + 2 * rows * width,
        ),
        compiler_params=grant(8),
        name="gather",
    )(chosen, route_weights, *tables)


def final_kernel(*refs, parts):
    out_ref = refs[-1]
    count = (len(refs) - 1) // parts
    width = out_ref.shape[1] // parts
    for part in range(parts):
        total = refs[part * count][...].astype(F32)
        for level in range(1, count):
            total += refs[part * count + level][...].astype(F32)
        out_ref[:, part * width : (part + 1) * width] = total.astype(BF16)


def final(parts):
    rows, width = parts[0][0].shape
    flat = [value for part in parts for value in part]
    return pl.pallas_call(
        functools.partial(final_kernel, parts=len(parts)),
        out_shape=shape_of(rows, width * len(parts)),
        in_specs=[whole()] * len(flat),
        out_specs=whole(),
        cost_estimate=cost(2**20, 2 * len(flat) * rows * width),
        compiler_params=grant(4),
        name="final",
    )(*flat)


def shards(
    queries, keys, values, mix_weight, sub_gain, tokens, routes, route_weights,
    expert_gain, gate_weight, up_weight, down_weight,
):
    rows2, width = tokens.shape
    picks = routes.shape[1]
    groups, levels = lax.axis_size("ep"), lax.axis_size("tp") // CORES
    pieces = gate_weight.shape[0]
    experts = groups * pieces
    capacity = 3 * rows2 * picks // (2 * experts)
    parts = parts_of(width)
    tp_index = lax.axis_index("tp")
    spot = jnp.stack([lax.axis_index("ep"), tp_index // CORES, tp_index % CORES])
    place = spot = spot.astype(jnp.int32)

    by_level = [tokens]
    for mask in range(1, levels):
        by_level.append(levels_flip(tokens, mask))
    bundles = pack(place, queries, keys, values, groups)
    bundles = exchange(bundles)
    chosen = plan(place, routes, capacity, pieces, experts, groups)
    own, other = [], []
    for chunk in range(2):
        some = by_level[chunk * levels // 2 : (chunk + 1) * levels // 2]
        tables = dispatch(place, routes, some, capacity, pieces, experts, groups)
        own.append(exchange(tables))
    for chunk in range(2):
        swapped = []
        for table in own[chunk]:
            swapped.append(cores_flip(table))
        other.append(swapped)
    hidden = hidden_units(
        spot, own, other, expert_gain, gate_weight, up_weight, groups, capacity, width
    )
    results = []
    for part in range(parts):
        sent, kept = down(
            spot, hidden, down_weight, groups, capacity, width, levels,
            part * (width // parts), width // parts,
        )
        partner = cores_flip(sent)
        tables = add_cores(kept, partner, groups)
        tables = exchange(tables)
        combined = gather(chosen, route_weights, tables, levels)
        arrived = [combined[0]]
        for mask in range(1, levels):
            arrived.append(levels_flip(combined[mask], mask))
        results.append(arrived)
    attended = attention(place, bundles, mix_weight, sub_gain, queries.shape[0])
    attended = exchange(attended)
    moe_out = final(results)
    attn_out = unpack(place, attended, queries.shape[1])
    return (attn_out, moe_out)


def parts_of(width):
    return 2 if width % 256 == 0 else 1


def solution(mesh):
    return jax.shard_map(
        shards,
        mesh=mesh,
        in_specs=(
            P("ep", "tp", None),
            P("ep", "tp", None),
            P("ep", "tp", None),
            P("tp"),
            P(),
            P("ep", "tp"),
            P("ep", None),
            P("ep", None),
            P(),
            P("ep", None, "tp"),
            P("ep", None, "tp"),
            P("ep", "tp", None),
        ),
        out_specs=(P("ep", "tp", None), P("ep", "tp")),
        check_vma=False,
    )
```

time: 176 us -> 115 us (0.65)
  waiting for transfers between devices: 79.4 us -> 28.9 us
  starting transfers between devices: 12.6 us -> 46.6 us
  Pallas kernels: 0 us -> 30 us
  matrix products: 22 us -> 0 us
  local copies, waits for them, and re-layouts: 25.2 us -> 8.05 us
  other arithmetic: 16.4 us -> 0.08 us
  between operations: 17.1 us -> 0.92 us
  loops' own time: 2.99 us -> 0 us
    all_to_all x2 -> x0, waiting for transfers between devices: 42.5 us -> none  [the longest x1 42.5 us: route_layer(): lax.all_to_all(outgoing, 'ep', split_axis=0, concat_axis=0, tiled=True)]
    ppermute x4 -> x37, starting transfers between devices: 5.18 us -> 46.6 us  [flip(): return lax.ppermute(value, axis, pairs)]
    pallas_call x0 -> x14, Pallas kernels: none -> 30 us  [the longest x1 10.1 us: hidden_units(): pl.pallas_call(functools.partial(hidden_kernel, count=len(tables), groups...]
    all_gather x3 -> x0, waiting for transfers between devices: 22.3 us -> none  [the longest x1 22.2 us: route_layer(): full_rows = lax.all_gather(tokens, 'tp', axis=1, tiled=True)]
    dot_general x10 -> x0, matrix products: 22 us -> none  [the longest x1 10 us: expert_finish(): jnp.einsum('secf,efd->secd', hidden, down_weight, preferred_element_type=...]
    ppermute x4 -> x37, waiting for transfers between devices: 13.9 us -> 28.9 us  [flip(): return lax.ppermute(value, axis, pairs)]
    all_to_all x2 -> x0, starting transfers between devices: 7.29 us -> none  [the longest x1 3.83 us: route_layer(): lax.all_to_all(outgoing, 'ep', split_axis=0, concat_axis=0, tiled=True)]
    reduce_sum x8 -> x0, other arithmetic: 6.89 us -> none  [the longest x4 3.63 us: score_update(): row_sum = row_sum * shrink + jnp.sum(weights, axis=-1)]
  transfers between devices with their start and end apart: 10 -> 37, of which waited for: 5 -> 14; matrix products, arithmetic and copies ran while one was open for 29% -> 1% of each run, Pallas kernels for 0% -> 14%
where the time goes in v2:
time: 115 us
  starting transfers between devices  46.6 us (41%)
  Pallas kernels  30 us (26%)
  waiting for transfers between devices  28.9 us (25%)
  local copies, waits for them, and re-layouts  8.05 us (7%)
    ppermute x37, starting transfers between devices, flip(): return lax.ppermute(value, axis, pairs)  46.6 us
    ppermute x37, waiting for transfers between devices, flip(): return lax.ppermute(value, axis, pairs)  28.9 us
    pallas_call x1, Pallas kernels, hidden_units(): pl.pallas_call(functools.partial(hidden_kernel, count=len(tables), groups...  10.1 us
    unnamed x30, local copies, waits for them, and re-layouts  7.98 us
    pallas_call x1, Pallas kernels, attention(): pl.pallas_call(functools.partial(attention_kernel, groups=groups, rows=ro...  6.11 us
    pallas_call x2, Pallas kernels, down(): pl.pallas_call(functools.partial(down_kernel, groups=groups, capacity=cap...  5.55 us
  transfers between devices with their start and end apart: 37, of which 14 were waited for; matrix products, arithmetic and copies ran while one was open for 1% of the time, Pallas kernels for 14%

profile of v2, /device:TPU:0, one launch (start us, length us, event | category | flops | bytes accessed | tf_op | source)
XLA Modules:
  0.0 114.6 jit_solution(17186392360850148978)
XLA Ops:
  0.6 4.1 %collective-permute-start.10 = (bf16[256,256]{1,0:T(8,128)(2,1)}, bf16[256,256]{1,0:T(8,128)(2,1)S(1)}, u32[]{:S(2)}, u32[]{:S(2)}) collective-permute-start(bf16[256,256]{1,0:T(8,128)(2,1)} %refs_0_.1), channel_id=1, source_target_pairs={{0,4},{1,5},{2,6},{3,7},{4,0},{5,1},{6,2},{7,3},{8,12},{9,13},{10,... | collective-permute-start | bytes 393224 | tf_op jit(solution)/shard_map/ppermute | solution.py:56
  6.4 8.6 %collective-permute-done.10.refs_0_ = bf16[256,256]{1,0:T(8,128)(2,1)S(1)} collective-permute-done((bf16[256,256]{1,0:T(8,128)(2,1)}, bf16[256,256]{1,0:T(8,128)(2,1)S(1)}, u32[]{:S(2)}, u32[]{:S(2)}) %collective-permute-start.10) | collective-permute-done | bytes 131104 | tf_op jit(solution)/shard_map/ppermute | solution.py:56
  16.8 1.9 %collective-permute-start.12 = (bf16[192,512]{1,0:T(8,128)(2,1)S(1)}, bf16[192,512]{1,0:T(8,128)(2,1)S(1)}, u32[]{:S(2)}, u32[]{:S(2)}) collective-permute-start(bf16[192,512]{1,0:T(8,128)(2,1)S(1)} %get-tuple-element.51), channel_id=1, source_target_pairs={{0,8},{8,0},{16,24},{24,16},{1,9},{9,1},{17,25},{25,17},{2,10},{10... | collective-permute-start | bytes 589832 | tf_op jit(solution)/shard_map/ppermute | solution.py:56
  18.6 1.5 %collective-permute-start.13 = (bf16[192,512]{1,0:T(8,128)(2,1)S(1)}, bf16[192,512]{1,0:T(8,128)(2,1)S(1)}, u32[]{:S(2)}, u32[]{:S(2)}) collective-permute-start(bf16[192,512]{1,0:T(8,128)(2,1)S(1)} %get-tuple-element.52), channel_id=1, source_target_pairs={{0,16},{8,24},{16,0},{24,8},{1,17},{9,25},{17,1},{25,9},{2,18},{10... | collective-permute-start | bytes 589832 | tf_op jit(solution)/shard_map/ppermute | solution.py:56
  22.3 1.9 %collective-permute-start.7 = (bf16[192,512]{1,0:T(8,128)(2,1)S(1)}, bf16[192,512]{1,0:T(8,128)(2,1)S(1)}, u32[]{:S(2)}, u32[]{:S(2)}) collective-permute-start(bf16[192,512]{1,0:T(8,128)(2,1)S(1)} %get-tuple-element.47), channel_id=1, source_target_pairs={{0,8},{8,0},{16,24},{24,16},{1,9},{9,1},{17,25},{25,17},{2,10},{10... | collective-permute-start | bytes 589832 | tf_op jit(solution)/shard_map/ppermute | solution.py:56
  24.2 1.5 %collective-permute-start.8 = (bf16[192,512]{1,0:T(8,128)(2,1)S(1)}, bf16[192,512]{1,0:T(8,128)(2,1)S(1)}, u32[]{:S(2)}, u32[]{:S(2)}) collective-permute-start(bf16[192,512]{1,0:T(8,128)(2,1)S(1)} %get-tuple-element.48), channel_id=1, source_target_pairs={{0,16},{8,24},{16,0},{24,8},{1,17},{9,25},{17,1},{25,9},{2,18},{10... | collective-permute-start | bytes 589832 | tf_op jit(solution)/shard_map/ppermute | solution.py:56
  25.7 1.7 %collective-permute-start.9 = (bf16[192,512]{1,0:T(8,128)(2,1)S(1)}, bf16[192,512]{1,0:T(8,128)(2,1)S(1)}, u32[]{:S(2)}, u32[]{:S(2)}) collective-permute-start(bf16[192,512]{1,0:T(8,128)(2,1)S(1)} %get-tuple-element.49), channel_id=1, source_target_pairs={{0,24},{8,16},{16,8},{24,0},{1,25},{9,17},{17,9},{25,1},{2,26},{10... | collective-permute-start | bytes 589832 | tf_op jit(solution)/shard_map/ppermute | solution.py:56
  27.8 2.4 %collective-permute-done.14.refs_7_ = bf16[192,512]{1,0:T(8,128)(2,1)S(1)} collective-permute-done((bf16[192,512]{1,0:T(8,128)(2,1)S(1)}, bf16[192,512]{1,0:T(8,128)(2,1)S(1)}, u32[]{:S(2)}, u32[]{:S(2)}) %collective-permute-start.14) | collective-permute-done | bytes 196640 | tf_op jit(solution)/shard_map/ppermute | solution.py:56
  30.2 2.4 %collective-permute-done.7.refs_1_ = bf16[192,512]{1,0:T(8,128)(2,1)S(1)} collective-permute-done((bf16[192,512]{1,0:T(8,128)(2,1)S(1)}, bf16[192,512]{1,0:T(8,128)(2,1)S(1)}, u32[]{:S(2)}, u32[]{:S(2)}) %collective-permute-start.7) | collective-permute-done | bytes 196640 | tf_op jit(solution)/shard_map/ppermute | solution.py:56
  32.6 3.3 %collective-permute-done.8.refs_2_ = bf16[192,512]{1,0:T(8,128)(2,1)S(1)} collective-permute-done((bf16[192,512]{1,0:T(8,128)(2,1)S(1)}, bf16[192,512]{1,0:T(8,128)(2,1)S(1)}, u32[]{:S(2)}, u32[]{:S(2)}) %collective-permute-start.8) | collective-permute-done | bytes 196640 | tf_op jit(solution)/shard_map/ppermute | solution.py:56
  38.5 2.2 %copy-done.1 = bf16[2,2048,512]{2,1,0:T(8,128)(2,1)S(1)} copy-done((bf16[2,2048,512]{2,1,0:T(8,128)(2,1)S(1)}, bf16[2,2048,512]{2,1,0:T(8,128)(2,1)}, u32[]{:S(2)}) %copy-start.1) | copy-done | bytes 4194328
  40.6 2.2 %copy-done.2 = bf16[2,2048,512]{2,1,0:T(8,128)(2,1)S(1)} copy-done((bf16[2,2048,512]{2,1,0:T(8,128)(2,1)S(1)}, bf16[2,2048,512]{2,1,0:T(8,128)(2,1)}, u32[]{:S(2)}) %copy-start.2) | copy-done | bytes 4194328
  43.5 10.1 %hidden.1.hidden_ref = bf16[2,384,512]{2,1,0:T(8,128)(2,1)S(1)} custom-call(s32[3]{0:T(128)S(1)} %pad_add_fusion.place_ref.spot_ref, bf16[192,512]{1,0:T(8,128)(2,1)S(1)} %get-tuple-element.46.refs_0_, bf16[192,512]{1,0:T(8,128)(2,1)S(1)} %collective-permute-done.7.refs_1_, bf16[192,512]{1,0:T(8,128)(2,1)S(1)} %collective-permute-done.8.refs_2_, ...), custom_call_target="tpu_custom_call" | custom-call | flops 3221225472 | bytes 14680064 | tf_op jit(solution)/shard_map/hidden/pallas_call | solution.py:340
  53.7 2.8 %down.3 = (bf16[768,512]{1,0:T(8,128)(2,1)S(1)}, bf16[768,512]{1,0:T(8,128)(2,1)S(1)}) custom-call(s32[3]{0:T(128)S(1)} %pad_add_fusion.place_ref.spot_ref, bf16[2,384,512]{2,1,0:T(8,128)(2,1)S(1)} %hidden.1.hidden_ref, bf16[2,512,2048]{2,1,0:T(8,128)(2,1)S(1)} %copy-done), custom_call_target="tpu_custom_call" | custom-call | flops 805306368 | bytes 3670016 | tf_op jit(solution)/shard_map/down/pallas_call | solution.py:411
  56.8 2.8 %down.2 = (bf16[768,512]{1,0:T(8,128)(2,1)S(1)}, bf16[768,512]{1,0:T(8,128)(2,1)S(1)}) custom-call(s32[3]{0:T(128)S(1)} %pad_add_fusion.place_ref.spot_ref, bf16[2,384,512]{2,1,0:T(8,128)(2,1)S(1)} %hidden.1.hidden_ref, bf16[2,512,2048]{2,1,0:T(8,128)(2,1)S(1)} %copy-done), custom_call_target="tpu_custom_call" | custom-call | flops 805306368 | bytes 3670016 | tf_op jit(solution)/shard_map/down/pallas_call | solution.py:411
  62.6 1.7 %collective-permute-start.2 = (bf16[1280,128]{1,0:T(8,128)(2,1)S(1)}, bf16[1280,128]{1,0:T(8,128)(2,1)S(1)}, u32[]{:S(2)}, u32[]{:S(2)}) collective-permute-start(bf16[1280,128]{1,0:T(8,128)(2,1)S(1)} %get-tuple-element.41), channel_id=1, source_target_pairs={{0,24},{8,16},{16,8},{24,0},{1,25},{9,17},{17,9},{25,1},{2,26},{10... | collective-permute-start | bytes 983048 | tf_op jit(solution)/shard_map/ppermute | solution.py:56
  65.8 5.6 %collective-permute-done.refs_1_ = bf16[1280,128]{1,0:T(8,128)(2,1)S(1)} collective-permute-done((bf16[1280,128]{1,0:T(8,128)(2,1)S(1)}, bf16[1280,128]{1,0:T(8,128)(2,1)S(1)}, u32[]{:S(2)}, u32[]{:S(2)}) %collective-permute-start) | collective-permute-done | bytes 327712 | tf_op jit(solution)/shard_map/ppermute | solution.py:56
  74.4 5.4 %collective-permute-start.24 = (bf16[192,512]{1,0:T(8,128)(2,1)}, bf16[192,512]{1,0:T(8,128)(2,1)S(1)}, u32[]{:S(2)}, u32[]{:S(2)}) collective-permute-start(bf16[192,512]{1,0:T(8,128)(2,1)} %get-tuple-element.57), channel_id=1, source_target_pairs={{0,8},{8,0},{16,24},{24,16},{1,9},{9,1},{17,25},{25,17},{2,10},{10... | collective-permute-start | bytes 589832 | tf_op jit(solution)/shard_map/ppermute | solution.py:56
  85.4 6.1 %attention.1 = (bf16[256,128]{1,0:T(8,128)(2,1)S(1)}, bf16[256,128]{1,0:T(8,128)(2,1)S(1)}, bf16[256,128]{1,0:T(8,128)(2,1)S(1)}, bf16[256,128]{1,0:T(8,128)(2,1)S(1)}) custom-call(s32[3]{0:T(128)S(1)} %pad_add_fusion.place_ref.spot_ref, f32[2]{0:T(128)S(1)} %copy-done.7, bf16[1280,128]{1,0:T(8,128)(2,1)S(1)} %get-tuple-element.38.refs_0_, ...), custom_call_target="tpu_custom_call" | custom-call | flops 1342177280 | bytes 1310720 | tf_op jit(solution)/shard_map/attention/pallas_call | solution.py:173
  91.5 1.5 %collective-permute-start.3 = (bf16[256,128]{1,0:T(8,128)(2,1)S(1)}, bf16[256,128]{1,0:T(8,128)(2,1)S(1)}, u32[]{:S(2)}, u32[]{:S(2)}) collective-permute-start(bf16[256,128]{1,0:T(8,128)(2,1)S(1)} %get-tuple-element.43), channel_id=1, source_target_pairs={{0,8},{8,0},{16,24},{24,16},{1,9},{9,1},{17,25},{25,17},{2,10},{10... | collective-permute-start | bytes 196616 | tf_op jit(solution)/shard_map/ppermute | solution.py:56
  95.8 4.6 %collective-permute-start.34 = (bf16[256,128]{1,0:T(8,128)(2,1)S(1)}, bf16[256,128]{1,0:T(8,128)(2,1)S(1)}, u32[]{:S(2)}, u32[]{:S(2)}) collective-permute-start(bf16[256,128]{1,0:T(8,128)(2,1)S(1)} %get-tuple-element.71), channel_id=1, source_target_pairs={{0,2},{1,3},{2,0},{3,1},{4,6},{5,7},{6,4},{7,5},{8,10},{9,11},{10,... | collective-permute-start | bytes 196616 | tf_op jit(solution)/shard_map/ppermute | solution.py:56
  100.5 2.0 %collective-permute-start.35 = (bf16[256,128]{1,0:T(8,128)(2,1)S(1)}, bf16[256,128]{1,0:T(8,128)(2,1)S(1)}, u32[]{:S(2)}, u32[]{:S(2)}) collective-permute-start(bf16[256,128]{1,0:T(8,128)(2,1)S(1)} %get-tuple-element.72), channel_id=1, source_target_pairs={{0,4},{1,5},{2,6},{3,7},{4,0},{5,1},{6,2},{7,3},{8,12},{9,13},{10,... | collective-permute-start | bytes 196616 | tf_op jit(solution)/shard_map/ppermute | solution.py:56
  105.2 2.5 %collective-permute-start.28 = (bf16[256,128]{1,0:T(8,128)(2,1)S(1)}, bf16[256,128]{1,0:T(8,128)(2,1)S(1)}, u32[]{:S(2)}, u32[]{:S(2)}) collective-permute-start(bf16[256,128]{1,0:T(8,128)(2,1)S(1)} %get-tuple-element.62), channel_id=1, source_target_pairs={{0,4},{1,5},{2,6},{3,7},{4,0},{5,1},{6,2},{7,3},{8,12},{9,13},{10,... | collective-permute-start | bytes 196616 | tf_op jit(solution)/shard_map/ppermute | solution.py:56
  110.5 2.5 %collective-permute-done.28.refs_2_ = bf16[256,128]{1,0:T(8,128)(2,1)S(1)} collective-permute-done((bf16[256,128]{1,0:T(8,128)(2,1)S(1)}, bf16[256,128]{1,0:T(8,128)(2,1)S(1)}, u32[]{:S(2)}, u32[]{:S(2)}) %collective-permute-start.28) | collective-permute-done | bytes 65568 | tf_op jit(solution)/shard_map/ppermute | solution.py:56
  (96 shorter events, 32.4 us)
Async XLA Ops:
  0.6 14.4 %collective-permute-start.10 = (bf16[256,256]{1,0:T(8,128)(2,1)}, bf16[256,256]{1,0:T(8,128)(2,1)S(1)}, u32[]{:S(2)}, u32[]{:S(2)}) collective-permute-start(bf16[256,256]{1,0:T(8,128)(2,1)} %refs_0_.1), channel_id=1, source_target_pairs={{0,4},{1,5},{2,6},{3,7},{4,0},{5,1},{6,2},{7,3},{8,12},{9,13},{10,... | collective-permute-start | bytes 393224 | tf_op jit(solution)/shard_map/ppermute | solution.py:56
  4.8 10.2 %collective-permute-start.11 = (bf16[256,256]{1,0:T(8,128)(2,1)}, bf16[256,256]{1,0:T(8,128)(2,1)S(1)}, u32[]{:S(2)}, u32[]{:S(2)}) collective-permute-start(bf16[256,256]{1,0:T(8,128)(2,1)} %refs_0_.1), channel_id=1, source_target_pairs={{0,6},{1,7},{2,4},{3,5},{4,2},{5,3},{6,0},{7,1},{8,14},{9,15},{10,... | collective-permute-start | bytes 393224 | tf_op jit(solution)/shard_map/ppermute | solution.py:56
  6.1 14.2 %collective-permute-start.6 = (bf16[256,256]{1,0:T(8,128)(2,1)}, bf16[256,256]{1,0:T(8,128)(2,1)S(1)}, u32[]{:S(2)}, u32[]{:S(2)}) collective-permute-start(bf16[256,256]{1,0:T(8,128)(2,1)} %refs_0_.1), channel_id=1, source_target_pairs={{0,2},{1,3},{2,0},{3,1},{4,6},{5,7},{6,4},{7,5},{8,10},{9,11},{10,... | collective-permute-start | bytes 393224 | tf_op jit(solution)/shard_map/ppermute | solution.py:56
  16.8 8.9 %collective-permute-start.12 = (bf16[192,512]{1,0:T(8,128)(2,1)S(1)}, bf16[192,512]{1,0:T(8,128)(2,1)S(1)}, u32[]{:S(2)}, u32[]{:S(2)}) collective-permute-start(bf16[192,512]{1,0:T(8,128)(2,1)S(1)} %get-tuple-element.51), channel_id=1, source_target_pairs={{0,8},{8,0},{16,24},{24,16},{1,9},{9,1},{17,25},{25,17},{2,10},{10... | collective-permute-start | bytes 589832 | tf_op jit(solution)/shard_map/ppermute | solution.py:56
  18.6 9.2 %collective-permute-start.13 = (bf16[192,512]{1,0:T(8,128)(2,1)S(1)}, bf16[192,512]{1,0:T(8,128)(2,1)S(1)}, u32[]{:S(2)}, u32[]{:S(2)}) collective-permute-start(bf16[192,512]{1,0:T(8,128)(2,1)S(1)} %get-tuple-element.52), channel_id=1, source_target_pairs={{0,16},{8,24},{16,0},{24,8},{1,17},{9,25},{17,1},{25,9},{2,18},{10... | collective-permute-start | bytes 589832 | tf_op jit(solution)/shard_map/ppermute | solution.py:56
  20.1 10.0 %collective-permute-start.14 = (bf16[192,512]{1,0:T(8,128)(2,1)S(1)}, bf16[192,512]{1,0:T(8,128)(2,1)S(1)}, u32[]{:S(2)}, u32[]{:S(2)}) collective-permute-start(bf16[192,512]{1,0:T(8,128)(2,1)S(1)} %get-tuple-element.53), channel_id=1, source_target_pairs={{0,24},{8,16},{16,8},{24,0},{1,25},{9,17},{17,9},{25,1},{2,26},{10... | collective-permute-start | bytes 589832 | tf_op jit(solution)/shard_map/ppermute | solution.py:56
  22.3 10.3 %collective-permute-start.7 = (bf16[192,512]{1,0:T(8,128)(2,1)S(1)}, bf16[192,512]{1,0:T(8,128)(2,1)S(1)}, u32[]{:S(2)}, u32[]{:S(2)}) collective-permute-start(bf16[192,512]{1,0:T(8,128)(2,1)S(1)} %get-tuple-element.47), channel_id=1, source_target_pairs={{0,8},{8,0},{16,24},{24,16},{1,9},{9,1},{17,25},{25,17},{2,10},{10... | collective-permute-start | bytes 589832 | tf_op jit(solution)/shard_map/ppermute | solution.py:56
  24.2 11.7 %collective-permute-start.8 = (bf16[192,512]{1,0:T(8,128)(2,1)S(1)}, bf16[192,512]{1,0:T(8,128)(2,1)S(1)}, u32[]{:S(2)}, u32[]{:S(2)}) collective-permute-start(bf16[192,512]{1,0:T(8,128)(2,1)S(1)} %get-tuple-element.48), channel_id=1, source_target_pairs={{0,16},{8,24},{16,0},{24,8},{1,17},{9,25},{17,1},{25,9},{2,18},{10... | collective-permute-start | bytes 589832 | tf_op jit(solution)/shard_map/ppermute | solution.py:56
  25.7 10.2 %collective-permute-start.9 = (bf16[192,512]{1,0:T(8,128)(2,1)S(1)}, bf16[192,512]{1,0:T(8,128)(2,1)S(1)}, u32[]{:S(2)}, u32[]{:S(2)}) collective-permute-start(bf16[192,512]{1,0:T(8,128)(2,1)S(1)} %get-tuple-element.49), channel_id=1, source_target_pairs={{0,24},{8,16},{16,8},{24,0},{1,25},{9,17},{17,9},{25,1},{2,26},{10... | collective-permute-start | bytes 589832 | tf_op jit(solution)/shard_map/ppermute | solution.py:56
  59.6 13.0 %collective-permute-start.23 = (bf16[768,512]{1,0:T(8,128)(2,1)S(1)}, bf16[768,512]{1,0:T(8,128)(2,1)S(1)}, u32[]{:S(2)}, u32[]{:S(2)}) collective-permute-start(bf16[768,512]{1,0:T(8,128)(2,1)S(1)} %get-tuple-element.55), channel_id=1, source_target_pairs={{0,1},{1,0},{2,3},{3,2},{4,5},{5,4},{6,7},{7,6},{8,9},{9,8},{10,11... | collective-permute-start | bytes 2359304 | tf_op jit(solution)/shard_map/ppermute | solution.py:56
  60.8 10.6 %collective-permute-start = (bf16[1280,128]{1,0:T(8,128)(2,1)S(1)}, bf16[1280,128]{1,0:T(8,128)(2,1)S(1)}, u32[]{:S(2)}, u32[]{:S(2)}) collective-permute-start(bf16[1280,128]{1,0:T(8,128)(2,1)S(1)} %get-tuple-element.39), channel_id=1, source_target_pairs={{0,8},{8,0},{16,24},{24,16},{1,9},{9,1},{17,25},{25,17},{2,10},{10... | collective-permute-start | bytes 983048 | tf_op jit(solution)/shard_map/ppermute | solution.py:56
  61.5 12.9 %collective-permute-start.1 = (bf16[1280,128]{1,0:T(8,128)(2,1)S(1)}, bf16[1280,128]{1,0:T(8,128)(2,1)S(1)}, u32[]{:S(2)}, u32[]{:S(2)}) collective-permute-start(bf16[1280,128]{1,0:T(8,128)(2,1)S(1)} %get-tuple-element.40), channel_id=1, source_target_pairs={{0,16},{8,24},{16,0},{24,8},{1,17},{9,25},{17,1},{25,9},{2,18},{10... | collective-permute-start | bytes 983048 | tf_op jit(solution)/shard_map/ppermute | solution.py:56
  62.6 17.2 %collective-permute-start.2 = (bf16[1280,128]{1,0:T(8,128)(2,1)S(1)}, bf16[1280,128]{1,0:T(8,128)(2,1)S(1)}, u32[]{:S(2)}, u32[]{:S(2)}) collective-permute-start(bf16[1280,128]{1,0:T(8,128)(2,1)S(1)} %get-tuple-element.41), channel_id=1, source_target_pairs={{0,24},{8,16},{16,8},{24,0},{1,25},{9,17},{17,9},{25,1},{2,26},{10... | collective-permute-start | bytes 983048 | tf_op jit(solution)/shard_map/ppermute | solution.py:56
  65.1 17.6 %collective-permute-start.31 = (bf16[192,512]{1,0:T(8,128)(2,1)S(1)}, bf16[192,512]{1,0:T(8,128)(2,1)S(1)}, u32[]{:S(2)}, u32[]{:S(2)}) collective-permute-start(bf16[192,512]{1,0:T(8,128)(2,1)S(1)} %get-tuple-element.67), channel_id=1, source_target_pairs={{0,8},{8,0},{16,24},{24,16},{1,9},{9,1},{17,25},{25,17},{2,10},{10... | collective-permute-start | bytes 589832 | tf_op jit(solution)/shard_map/ppermute | solution.py:56
  71.4 20.1 %collective-permute-start.32 = (bf16[192,512]{1,0:T(8,128)(2,1)}, bf16[192,512]{1,0:T(8,128)(2,1)S(1)}, u32[]{:S(2)}, u32[]{:S(2)}) collective-permute-start(bf16[192,512]{1,0:T(8,128)(2,1)} %get-tuple-element.68), channel_id=1, source_target_pairs={{0,16},{8,24},{16,0},{24,8},{1,17},{9,25},{17,1},{25,9},{2,18},{10... | collective-permute-start | bytes 589832 | tf_op jit(solution)/shard_map/ppermute | solution.py:56
  72.6 20.4 %collective-permute-start.33 = (bf16[192,512]{1,0:T(8,128)(2,1)S(1)}, bf16[192,512]{1,0:T(8,128)(2,1)S(1)}, u32[]{:S(2)}, u32[]{:S(2)}) collective-permute-start(bf16[192,512]{1,0:T(8,128)(2,1)S(1)} %get-tuple-element.69), channel_id=1, source_target_pairs={{0,24},{8,16},{16,8},{24,0},{1,25},{9,17},{17,9},{25,1},{2,26},{10... | collective-permute-start | bytes 589832 | tf_op jit(solution)/shard_map/ppermute | solution.py:56
  74.4 20.1 %collective-permute-start.24 = (bf16[192,512]{1,0:T(8,128)(2,1)}, bf16[192,512]{1,0:T(8,128)(2,1)S(1)}, u32[]{:S(2)}, u32[]{:S(2)}) collective-permute-start(bf16[192,512]{1,0:T(8,128)(2,1)} %get-tuple-element.57), channel_id=1, source_target_pairs={{0,8},{8,0},{16,24},{24,16},{1,9},{9,1},{17,25},{25,17},{2,10},{10... | collective-permute-start | bytes 589832 | tf_op jit(solution)/shard_map/ppermute | solution.py:56
  79.9 16.0 %collective-permute-start.25 = (bf16[192,512]{1,0:T(8,128)(2,1)}, bf16[192,512]{1,0:T(8,128)(2,1)S(1)}, u32[]{:S(2)}, u32[]{:S(2)}) collective-permute-start(bf16[192,512]{1,0:T(8,128)(2,1)} %get-tuple-element.58), channel_id=1, source_target_pairs={{0,16},{8,24},{16,0},{24,8},{1,17},{9,25},{17,1},{25,9},{2,18},{10... | collective-permute-start | bytes 589832 | tf_op jit(solution)/shard_map/ppermute | solution.py:56
  82.7 17.8 %collective-permute-start.26 = (bf16[192,512]{1,0:T(8,128)(2,1)S(1)}, bf16[192,512]{1,0:T(8,128)(2,1)S(1)}, u32[]{:S(2)}, u32[]{:S(2)}) collective-permute-start(bf16[192,512]{1,0:T(8,128)(2,1)S(1)} %get-tuple-element.59), channel_id=1, source_target_pairs={{0,24},{8,16},{16,8},{24,0},{1,25},{9,17},{17,9},{25,1},{2,26},{10... | collective-permute-start | bytes 589832 | tf_op jit(solution)/shard_map/ppermute | solution.py:56
  91.5 11.7 %collective-permute-start.3 = (bf16[256,128]{1,0:T(8,128)(2,1)S(1)}, bf16[256,128]{1,0:T(8,128)(2,1)S(1)}, u32[]{:S(2)}, u32[]{:S(2)}) collective-permute-start(bf16[256,128]{1,0:T(8,128)(2,1)S(1)} %get-tuple-element.43), channel_id=1, source_target_pairs={{0,8},{8,0},{16,24},{24,16},{1,9},{9,1},{17,25},{25,17},{2,10},{10... | collective-permute-start | bytes 196616 | tf_op jit(solution)/shard_map/ppermute | solution.py:56
  93.0 11.5 %collective-permute-start.4 = (bf16[256,128]{1,0:T(8,128)(2,1)S(1)}, bf16[256,128]{1,0:T(8,128)(2,1)S(1)}, u32[]{:S(2)}, u32[]{:S(2)}) collective-permute-start(bf16[256,128]{1,0:T(8,128)(2,1)S(1)} %get-tuple-element.44), channel_id=1, source_target_pairs={{0,16},{8,24},{16,0},{24,8},{1,17},{9,25},{17,1},{25,9},{2,18},{10... | collective-permute-start | bytes 196616 | tf_op jit(solution)/shard_map/ppermute | solution.py:56
  94.6 10.6 %collective-permute-start.5 = (bf16[256,128]{1,0:T(8,128)(2,1)S(1)}, bf16[256,128]{1,0:T(8,128)(2,1)S(1)}, u32[]{:S(2)}, u32[]{:S(2)}) collective-permute-start(bf16[256,128]{1,0:T(8,128)(2,1)S(1)} %get-tuple-element.45), channel_id=1, source_target_pairs={{0,24},{8,16},{16,8},{24,0},{1,25},{9,17},{17,9},{25,1},{2,26},{10... | collective-permute-start | bytes 196616 | tf_op jit(solution)/shard_map/ppermute | solution.py:56
  95.8 11.9 %collective-permute-start.34 = (bf16[256,128]{1,0:T(8,128)(2,1)S(1)}, bf16[256,128]{1,0:T(8,128)(2,1)S(1)}, u32[]{:S(2)}, u32[]{:S(2)}) collective-permute-start(bf16[256,128]{1,0:T(8,128)(2,1)S(1)} %get-tuple-element.71), channel_id=1, source_target_pairs={{0,2},{1,3},{2,0},{3,1},{4,6},{5,7},{6,4},{7,5},{8,10},{9,11},{10,... | collective-permute-start | bytes 196616 | tf_op jit(solution)/shard_map/ppermute | solution.py:56
  100.5 10.0 %collective-permute-start.35 = (bf16[256,128]{1,0:T(8,128)(2,1)S(1)}, bf16[256,128]{1,0:T(8,128)(2,1)S(1)}, u32[]{:S(2)}, u32[]{:S(2)}) collective-permute-start(bf16[256,128]{1,0:T(8,128)(2,1)S(1)} %get-tuple-element.72), channel_id=1, source_target_pairs={{0,4},{1,5},{2,6},{3,7},{4,0},{5,1},{6,2},{7,3},{8,12},{9,13},{10,... | collective-permute-start | bytes 196616 | tf_op jit(solution)/shard_map/ppermute | solution.py:56
  (26 other events, 204.4 us)

commit v3 on v2

--- a/solution.py
+++ b/solution.py
@@ -16,6 +16,7 @@
 OUT_SCALE = 0.8
 LOG2E = 1.4426950408889634
 CORES = 2
+FETCH_GRANT = 44
 BF16 = jnp.bfloat16
 F32 = jnp.float32
 
@@ -26,10 +27,6 @@
 
 def far():
     return pl.BlockSpec(memory_space=pl.ANY)
-
-
-def weights():
-    return pl.BlockSpec(memory_space=pltpu.HBM)
 
 
 def scalars():
@@ -129,14 +126,14 @@
     factor = scale * LOG2E
     for copy in copies:
         copy.wait()
+    tops = [None, None]
     for block in range(groups):
         visible = column <= row + (part if block % 2 == 0 else splits - 1 - part) * share
         queries = bundle[block, 2 * rows :, :]
-        sums = []
+        empty = jnp.zeros_like(queries)
         for side in range(2):
-            own = (lane < half) if side == 0 else (lane >= half)
-            query = jnp.where(own, queries, jnp.zeros_like(queries))
-            top = jnp.full((share, 1), NEG_FILL, F32)
+            query = jnp.where((lane < half) if side == 0 else (lane >= half), queries, empty)
+            top = jnp.full((share, width), NEG_FILL, F32)
             for other in range(block + 1):
                 score = lax.dot_general(
                     query, bundle[other, :rows, :], contract, preferred_element_type=F32
@@ -144,19 +141,25 @@
                 if other == block:
                     score = jnp.where(visible, score, NEG_FILL)
                 scores[side, :, other * rows : (other + 1) * rows] = score
-                top = jnp.maximum(top, jnp.max(score, axis=-1, keepdims=True))
-            total = jnp.zeros((share, 1), F32)
+                for start in range(0, rows, width):
+                    top = jnp.maximum(top, score[:, start : start + width])
+            tops[side] = jnp.max(top, axis=-1, keepdims=True)
+        sums = []
+        for side in range(2):
+            top = tops[side]
+            total = jnp.zeros((share, width), F32)
             weighted = jnp.zeros((share, width), F32)
             for other in range(block + 1):
                 score = scores[side, :, other * rows : (other + 1) * rows]
                 weight = jnp.exp2((score - top) * factor)
-                total += jnp.sum(weight, axis=-1, keepdims=True)
+                for start in range(0, rows, width):
+                    total += weight[:, start : start + width]
                 weighted += jnp.dot(
                     weight.astype(BF16),
                     bundle[other, rows : 2 * rows, :],
                     preferred_element_type=F32,
                 )
-            sums.append(weighted / total)
+            sums.append(weighted / jnp.sum(total, axis=-1, keepdims=True))
         blend = sums[0] - mix * sums[1]
         mean = jnp.mean(blend * blend, axis=-1, keepdims=True)
         scaled = blend * lax.rsqrt(mean + SUB_EPS)
@@ -268,7 +271,7 @@
         cost_estimate=cost(2 * groups * slots * rows * wide, 4 * groups * slots * wide),
         compiler_params=grant(8),
         name="dispatch",
-    )(place, routes.T, *by_level)
+    )(place, routes, *by_level)
 
 
 def block_start(spot_ref, level, side, width):
@@ -276,27 +279,41 @@
     return (CORES * jnp.bitwise_xor(spot_ref[1], level) + core) * width
 
 
-def hidden_kernel(spot_ref, *refs, count, groups, capacity, width):
-    slot_refs, (gain_ref, gate_hbm, up_hbm, hidden_ref) = refs[:count], refs[count : count + 4]
-    normed, gate_vmem, up_vmem, arrivals = refs[count + 4 :]
-    pieces, total_width, _ = gate_hbm.shape
-    tile = gate_vmem.shape[2]
-    steps = gate_vmem.shape[0] // pieces
-    chunks = count // groups // 2
-    span = slot_refs[0].shape[1] // width
+def fetch_kernel(*refs):
+    count = (len(refs) - 1) // 2
+    arrivals = refs[-1]
     copies = []
-    for index in range(pieces * steps):
-        columns = pl.ds(index % steps * tile, tile)
-        for kind, (source, target) in enumerate(((gate_hbm, gate_vmem), (up_hbm, up_vmem))):
+    for source, target in zip(refs[:count], refs[count : 2 * count]):
+        parts = [()] if len(source.shape) < 3 else [(piece,) for piece in range(source.shape[0])]
+        for part in parts:
             copies.append(
-                pltpu.make_async_copy(
-                    source.at[index // steps, :, columns],
-                    target.at[index],
-                    arrivals.at[2 * index + kind],
-                )
+                pltpu.make_async_copy(source.at[part], target.at[part], arrivals.at[len(copies)])
             )
     for copy in copies:
         copy.start()
+    for copy in copies:
+        copy.wait()
+
+
+def fetch(*arrays, mebibytes):
+    return pl.pallas_call(
+        fetch_kernel,
+        out_shape=[shape_of(*array.shape, dtype=array.dtype) for array in arrays],
+        in_specs=[far()] * len(arrays),
+        out_specs=[whole()] * len(arrays),
+        scratch_shapes=[pltpu.SemaphoreType.DMA((2 * len(arrays),))],
+        cost_estimate=cost(2**20, sum(4 * array.size for array in arrays)),
+        compiler_params=grant(mebibytes),
+    )(*arrays)
+
+
+def hidden_kernel(spot_ref, *refs, count, groups, capacity, width):
+    slot_refs = refs[:count]
+    gain_ref, gate_ref, up_ref, hidden_ref, normed = refs[count:]
+    pieces, total_width, ff = gate_ref.shape
+    tile = 256 if ff % 256 == 0 else ff
+    chunks = count // groups // 2
+    span = slot_refs[0].shape[1] // width
     factors = [[None] * groups for _ in range(pieces)]
     for group in range(groups):
         squares = jnp.zeros((pieces * capacity, 1), F32)
@@ -318,23 +335,19 @@
             factors[piece][group] = factor[piece * capacity : (piece + 1) * capacity]
     for piece in range(pieces):
         factor = jnp.concatenate(factors[piece], axis=0)
-        for step in range(steps):
-            index = piece * steps + step
-            copies[2 * index].wait()
-            gate = jnp.dot(normed[piece], gate_vmem[index], preferred_element_type=F32)
-            copies[2 * index + 1].wait()
-            up = jnp.dot(normed[piece], up_vmem[index], preferred_element_type=F32)
+        for start in range(0, ff, tile):
+            columns = slice(start, start + tile)
+            gate = jnp.dot(normed[piece], gate_ref[piece, :, columns], preferred_element_type=F32)
+            up = jnp.dot(normed[piece], up_ref[piece, :, columns], preferred_element_type=F32)
             gate = jnp.minimum(gate * factor, CLAMP_LIMIT)
             up = jnp.clip(up * factor, -CLAMP_LIMIT, CLAMP_LIMIT)
-            hidden_ref[piece, :, step * tile : (step + 1) * tile] = (
+            hidden_ref[piece, :, columns] = (
                 (up + 1.0) * gate * jax.nn.sigmoid(GLU_ALPHA * gate)
             ).astype(BF16)
 
 
 def hidden_units(spot, own, other, gain, gate_weight, up_weight, groups, capacity, width):
     pieces, total_width, ff = gate_weight.shape
-    tile = 256 if ff % 256 == 0 else ff
-    steps = ff // tile
     tables = [table for side in (own, other) for chunk in side for table in chunk]
     rows = groups * capacity
     return pl.pallas_call(
@@ -342,87 +355,51 @@
             hidden_kernel, count=len(tables), groups=groups, capacity=capacity, width=width
         ),
         out_shape=shape_of(pieces, rows, ff),
-        in_specs=[scalars()] + [whole()] * (len(tables) + 1) + [weights()] * 2,
+        in_specs=[scalars()] + [whole()] * (len(tables) + 3),
         out_specs=whole(),
-        scratch_shapes=[
-            pltpu.VMEM((pieces, rows, total_width), BF16),
-            pltpu.VMEM((pieces * steps, total_width, tile), BF16),
-            pltpu.VMEM((pieces * steps, total_width, tile), BF16),
-            pltpu.SemaphoreType.DMA((2 * pieces * steps,)),
-        ],
+        scratch_shapes=[pltpu.VMEM((pieces, rows, total_width), BF16)],
         cost_estimate=cost(
             4 * pieces * rows * total_width * ff,
             4 * pieces * total_width * (ff + rows),
             pieces * rows * ff,
         ),
-        compiler_params=grant(24),
+        compiler_params=grant(20),
         name="hidden",
     )(spot, *tables, gain[None, :], gate_weight, up_weight)
 
 
 def down_kernel(
-    spot_ref, hidden_ref, down_hbm, sent_ref, kept_ref, down_vmem, arrivals,
-    *, groups, capacity, width, start,
+    spot_ref, hidden_ref, down_ref, sent_ref, kept_ref, *, groups, capacity, width, first
 ):
     pieces = hidden_ref.shape[0]
-    part = sent_ref.shape[1]
-    copies = []
-    blocks = arrivals.shape[0] // (pieces * CORES)
-    piece_width = part // blocks
-    for side in (1, 0):
-        for piece in range(pieces):
-            for level in range(blocks):
-                offset = block_start(spot_ref, level, side, width) + start
-                index = (side * pieces + piece) * blocks + level
-                copies.append(
-                    pltpu.make_async_copy(
-                        down_hbm.at[
-                            piece, :, pl.ds(pl.multiple_of(offset, piece_width), piece_width)
-                        ],
-                        down_vmem.at[
-                            side * pieces + piece,
-                            :,
-                            pl.ds(level * piece_width, piece_width),
-                        ],
-                        arrivals.at[index],
-                    )
-                )
-    for copy in copies:
-        copy.start()
-    taken = 0
     for side, ref in ((1, sent_ref), (0, kept_ref)):
         for piece in range(pieces):
-            for copy in copies[taken : taken + blocks]:
-                copy.wait()
-            taken += blocks
-            value = jnp.dot(
-                hidden_ref[piece],
-                down_vmem[side * pieces + piece],
-                preferred_element_type=F32,
-            ).astype(BF16)
-            for group in range(groups):
-                row = (group * pieces + piece) * capacity
-                ref[row : row + capacity] = value[group * capacity : (group + 1) * capacity]
-
-
-def down(spot, hidden, down_weight, groups, capacity, width, levels, start, piece_width):
+            for inner in range(ref.shape[1] // width):
+                start = block_start(spot_ref, first + inner, side, width)
+                value = jnp.dot(
+                    hidden_ref[piece],
+                    down_ref[piece, :, pl.ds(pl.multiple_of(start, width), width)],
+                    preferred_element_type=F32,
+                ).astype(BF16)
+                for group in range(groups):
+                    row = (group * pieces + piece) * capacity
+                    ref[row : row + capacity, inner * width : (inner + 1) * width] = value[
+                        group * capacity : (group + 1) * capacity
+                    ]
+
+
+def down(spot, hidden, down_weight, groups, capacity, width, first, span):
     pieces, rows, ff = hidden.shape
-    part = levels * piece_width
-    return pl.pallas_call(
-        functools.partial(
-            down_kernel, groups=groups, capacity=capacity, width=width, start=start
-        ),
+    part = span * width
+    return pl.pallas_call(
+        functools.partial(down_kernel, groups=groups, capacity=capacity, width=width, first=first),
         out_shape=[shape_of(pieces * rows, part)] * 2,
-        in_specs=[scalars(), whole(), weights()],
+        in_specs=[scalars(), whole(), whole()],
         out_specs=[whole()] * 2,
-        scratch_shapes=[
-            pltpu.VMEM((CORES * pieces, ff, part), BF16),
-            pltpu.SemaphoreType.DMA((CORES * pieces * levels,)),
-        ],
         cost_estimate=cost(
             2 * CORES * pieces * rows * ff * part, 2 * CORES * pieces * part * (ff + rows)
         ),
-        compiler_params=grant(10),
+        compiler_params=grant(12),
         name="down",
     )(spot, hidden, down_weight)
 
@@ -447,40 +424,97 @@
     )(kept, partner)
 
 
-def plan_kernel(place_ref, routes_ref, out_ref, *, capacity, pieces, experts):
-    rows, picks = routes_ref.shape
+def part_kernel(kept_ref, partner_ref, mine_ref, *out_refs):
+    width = mine_ref.shape[1]
+    for level, ref in enumerate((mine_ref,) + out_refs):
+        place = slice(level * width, (level + 1) * width)
+        total = kept_ref[:, place].astype(F32) + partner_ref[:, place].astype(F32)
+        ref[...] = total.astype(ref.dtype)
+
+
+def part_levels(kept, partner, levels):
+    rows, width = kept.shape
+    own = width // levels
+    return pl.pallas_call(
+        part_kernel,
+        out_shape=[shape_of(rows, own, dtype=F32)] + [shape_of(rows, own)] * (levels - 1),
+        in_specs=[whole()] * 2,
+        out_specs=[whole()] * levels,
+        cost_estimate=cost(2**21, 6 * rows * width),
+        compiler_params=grant(6),
+        name="part_levels",
+    )(kept, partner)
+
+
+def sum_kernel(*refs, groups):
+    value_refs, out_refs = refs[:-groups], refs[-groups:]
+    rows = out_refs[0].shape[0]
+    for group, ref in enumerate(out_refs):
+        place = slice(group * rows, (group + 1) * rows)
+        total = value_refs[0][place]
+        for value_ref in value_refs[1:]:
+            total += value_ref[place].astype(F32)
+        ref[...] = total.astype(BF16)
+
+
+def sum_levels(values, groups):
+    rows, width = values[0].shape
+    return pl.pallas_call(
+        functools.partial(sum_kernel, groups=groups),
+        out_shape=[shape_of(rows // groups, width)] * groups,
+        in_specs=[whole()] * len(values),
+        out_specs=[whole()] * groups,
+        cost_estimate=cost(2**21, 6 * rows * width),
+        compiler_params=grant(6),
+        name="sum_levels",
+    )(*values)
+
+
+def plan_kernel(
+    place_ref, routes_ref, weights_ref, out_ref, scale_ref, *, capacity, pieces, experts
+):
+    picks, rows = routes_ref.shape
     slots = out_ref.shape[2]
     groups = out_ref.shape[0] // picks
     wide = max(experts, 128)
+    first = lax.broadcasted_iota(jnp.int32, (rows, rows), 0)
+    second = lax.broadcasted_iota(jnp.int32, (rows, rows), 1)
+
+    def column(row):
+        return jnp.sum(jnp.where(first == second, row, 0.0), axis=1, keepdims=True)
+
     expert = lax.broadcasted_iota(jnp.int32, (rows, wide), 1)
     named = jnp.zeros((rows, wide), jnp.bool_)
+    scale = jnp.zeros((rows, scale_ref.shape[1]), F32)
+    lane = lax.broadcasted_iota(jnp.int32, scale.shape, 1)
+    routes = []
     for pick in range(picks):
-        named = named | (routes_ref[:, pick : pick + 1] == expert)
-    first = lax.broadcasted_iota(jnp.int32, (rows, rows), 0)
-    second = lax.broadcasted_iota(jnp.int32, (rows, rows), 1)
+        routes.append(column(routes_ref[pick : pick + 1, :].astype(F32)).astype(jnp.int32))
+        named = named | (routes[pick] == expert)
+        scale = jnp.where(lane == pick, column(weights_ref[pick : pick + 1, :]), scale)
+    scale_ref[...] = scale
     rank = ranks(named, second < first, 0)
     slot = lax.broadcasted_iota(jnp.int32, (rows, slots), 1)
     for pick in range(picks):
-        route = routes_ref[:, pick : pick + 1]
-        mine = jnp.sum(jnp.where(expert == route, rank, 0.0), axis=1, keepdims=True)
-        target = route * capacity + mine.astype(jnp.int32)
+        mine = jnp.sum(jnp.where(expert == routes[pick], rank, 0.0), axis=1, keepdims=True)
+        target = routes[pick] * capacity + mine.astype(jnp.int32)
         for mask in range(groups):
             here = slot + jnp.bitwise_xor(place_ref[0], mask) * slots
             out_ref[pick * groups + mask] = (here == target).astype(F32).astype(BF16)
 
 
-def plan(place, routes, capacity, pieces, experts, groups):
-    rows, picks = routes.shape
+def plan(place, routes, route_weights, capacity, pieces, experts, groups):
+    picks, rows = routes.shape
     slots = pieces * capacity
     return pl.pallas_call(
         functools.partial(plan_kernel, capacity=capacity, pieces=pieces, experts=experts),
-        out_shape=shape_of(picks * groups, rows, slots),
-        in_specs=[scalars(), whole()],
-        out_specs=whole(),
+        out_shape=[shape_of(picks * groups, rows, slots), shape_of(rows, 128, dtype=F32)],
+        in_specs=[scalars(), whole(), whole()],
+        out_specs=[whole()] * 2,
         cost_estimate=cost(2**25, 2 * picks * groups * rows * slots),
-        compiler_params=grant(6),
+        compiler_params=grant(6, groups),
         name="plan",
-    )(place, routes)
+    )(place, routes, route_weights)
 
 
 def gather_kernel(chosen_ref, weights_ref, *refs, groups):
@@ -503,9 +537,9 @@
         ref[...] = total[:, level * width : (level + 1) * width].astype(BF16)
 
 
-def gather(chosen, route_weights, tables, levels):
+def gather(chosen, scale, tables, levels):
     groups = len(tables)
-    rows, picks = route_weights.shape
+    rows, picks = scale.shape[0], chosen.shape[0] // groups
     slots, width = tables[0].shape
     return pl.pallas_call(
         functools.partial(gather_kernel, groups=groups),
@@ -518,32 +552,27 @@
         ),
         compiler_params=grant(8),
         name="gather",
-    )(chosen, route_weights, *tables)
-
-
-def final_kernel(*refs, parts):
-    out_ref = refs[-1]
-    count = (len(refs) - 1) // parts
-    width = out_ref.shape[1] // parts
-    for part in range(parts):
-        total = refs[part * count][...].astype(F32)
-        for level in range(1, count):
-            total += refs[part * count + level][...].astype(F32)
-        out_ref[:, part * width : (part + 1) * width] = total.astype(BF16)
+    )(chosen, scale, *tables)
+
+
+def final_kernel(*refs):
+    total = refs[0][...].astype(F32)
+    for ref in refs[1:-1]:
+        total += ref[...].astype(F32)
+    refs[-1][...] = total.astype(BF16)
 
 
 def final(parts):
-    rows, width = parts[0][0].shape
-    flat = [value for part in parts for value in part]
-    return pl.pallas_call(
-        functools.partial(final_kernel, parts=len(parts)),
-        out_shape=shape_of(rows, width * len(parts)),
-        in_specs=[whole()] * len(flat),
+    rows, width = parts[0].shape
+    return pl.pallas_call(
+        final_kernel,
+        out_shape=shape_of(rows, width),
+        in_specs=[whole()] * len(parts),
         out_specs=whole(),
-        cost_estimate=cost(2**20, 2 * len(flat) * rows * width),
+        cost_estimate=cost(2**20, 2 * len(parts) * rows * width),
         compiler_params=grant(4),
         name="final",
-    )(*flat)
+    )(*parts)
 
 
 def shards(
@@ -556,7 +585,7 @@
     pieces = gate_weight.shape[0]
     experts = groups * pieces
     capacity = 3 * rows2 * picks // (2 * experts)
-    parts = parts_of(width)
+    half = levels // 2
     tp_index = lax.axis_index("tp")
     spot = jnp.stack([lax.axis_index("ep"), tp_index // CORES, tp_index % CORES])
     place = spot = spot.astype(jnp.int32)
@@ -564,45 +593,50 @@
     by_level = [tokens]
     for mask in range(1, levels):
         by_level.append(levels_flip(tokens, mask))
+    by_level[0], picked, picked_weights = fetch(tokens, routes.T, route_weights.T, mebibytes=2)
+    chosen, scale = plan(
+        place, picked, picked_weights, capacity, pieces, experts, groups
+    )
+    queries, keys, values, scale = lax.optimization_barrier((queries, keys, values, scale))
     bundles = pack(place, queries, keys, values, groups)
-    bundles = exchange(bundles)
-    chosen = plan(place, routes, capacity, pieces, experts, groups)
     own, other = [], []
     for chunk in range(2):
-        some = by_level[chunk * levels // 2 : (chunk + 1) * levels // 2]
-        tables = dispatch(place, routes, some, capacity, pieces, experts, groups)
+        some = by_level[chunk * half : (chunk + 1) * half]
+        tables = dispatch(place, picked, some, capacity, pieces, experts, groups)
         own.append(exchange(tables))
+    bundles = exchange(bundles)
     for chunk in range(2):
         swapped = []
         for table in own[chunk]:
             swapped.append(cores_flip(table))
         other.append(swapped)
+    gate_near, up_near = fetch(gate_weight, up_weight, mebibytes=FETCH_GRANT)
     hidden = hidden_units(
-        spot, own, other, expert_gain, gate_weight, up_weight, groups, capacity, width
+        spot, own, other, expert_gain, gate_near, up_near, groups, capacity, width
     )
+    halves = []
+    for first in (0, half):
+        sent, kept = down(
+            spot, hidden, down_weight, groups, capacity, width, first, half
+        )
+        halves.append((kept, cores_flip(sent)))
+    values = list(part_levels(*halves[0], half))
+    for level in range(1, half):
+        values[level] = levels_flip(values[level], level)
+    tables = add_cores(*halves[1], groups)
+    tables = exchange(tables)
+    combined = gather(chosen, scale, tables, half)
     results = []
-    for part in range(parts):
-        sent, kept = down(
-            spot, hidden, down_weight, groups, capacity, width, levels,
-            part * (width // parts), width // parts,
-        )
-        partner = cores_flip(sent)
-        tables = add_cores(kept, partner, groups)
-        tables = exchange(tables)
-        combined = gather(chosen, route_weights, tables, levels)
-        arrived = [combined[0]]
-        for mask in range(1, levels):
-            arrived.append(levels_flip(combined[mask], mask))
-        results.append(arrived)
+    for inner, value in enumerate(combined):
+        results.append(levels_flip(value, half + inner))
+    tables = sum_levels(values, groups)
+    tables = exchange(tables)
+    results += gather(chosen, scale, tables, 1)
     attended = attention(place, bundles, mix_weight, sub_gain, queries.shape[0])
     attended = exchange(attended)
     moe_out = final(results)
     attn_out = unpack(place, attended, queries.shape[1])
     return (attn_out, moe_out)
-
-
-def parts_of(width):
-    return 2 if width % 256 == 0 else 1
 
 
 def solution(mesh):

time: 115 us -> 96.5 us (0.84)
  waiting for transfers between devices: 28.9 us -> 18.1 us
  Pallas kernels: 30 us -> 23.7 us
  local copies, waits for them, and re-layouts: 8.05 us -> 3.42 us
  starting transfers between devices: 46.6 us -> 50.1 us
    ppermute x37 -> x34, waiting for transfers between devices: 28.9 us -> 18.1 us  [flip(): return lax.ppermute(value, axis, pairs)]
    pallas_call x1, Pallas kernels: 10.1 us -> 5.08 us  [hidden_units(): pl.pallas_call(functools.partial(hidden_kernel, count=len(tables), groups...]
    unnamed x30 -> x21, local copies, waits for them, and re-layouts: 7.98 us -> 3.31 us
    pallas_call x1 -> x5, Pallas kernels: 0.73 us -> 4.64 us  [the longest x2 3.69 us: fetch(): pl.pallas_call(fetch_kernel, out_shape=[shape_of(*array.shape, dtype=arra...]
    ppermute x37 -> x34, starting transfers between devices: 46.6 us -> 50.1 us  [flip(): return lax.ppermute(value, axis, pairs)]
    pallas_call x2, Pallas kernels: 5.55 us -> 3.08 us  [down(): pl.pallas_call(functools.partial(down_kernel, groups=groups, capacity=cap...]
    pallas_call x2 -> x1, Pallas kernels: 1.64 us -> 0.18 us  [add_cores(): pl.pallas_call(add_kernel, out_shape=[shape_of(rows // groups, width)] *...]
  transfers between devices with their start and end apart: 37 -> 34, of which waited for: 14 -> 8; matrix products, arithmetic and copies ran while one was open for 1% -> 1% of each run, Pallas kernels for 14% -> 17%
where the time goes in v3:
time: 96.5 us; the launch traced here: 96.3 us
  starting transfers between devices  50.1 us (52%)
  Pallas kernels  23.7 us (25%)
  waiting for transfers between devices  18.1 us (19%)
  local copies, waits for them, and re-layouts  3.42 us (4%)
    ppermute x34, starting transfers between devices, flip(): return lax.ppermute(value, axis, pairs)  50.1 us
    ppermute x34, waiting for transfers between devices, flip(): return lax.ppermute(value, axis, pairs)  18.1 us
    pallas_call x1, Pallas kernels, attention(): pl.pallas_call(functools.partial(attention_kernel, groups=groups, rows=ro...  5.19 us
    pallas_call x1, Pallas kernels, hidden_units(): pl.pallas_call(functools.partial(hidden_kernel, count=len(tables), groups...  5.08 us
    pallas_call x2, Pallas kernels, fetch(): pl.pallas_call(fetch_kernel, out_shape=[shape_of(*array.shape, dtype=arra...  3.69 us
    unnamed x21, local copies, waits for them, and re-layouts  3.31 us
    pallas_call x2, Pallas kernels, down(): pl.pallas_call(functools.partial(down_kernel, groups=groups, capacity=cap...  3.08 us
    pallas_call x2, Pallas kernels, dispatch(): pl.pallas_call(functools.partial(dispatch_kernel, capacity=capacity, piec...  2.15 us
  transfers between devices with their start and end apart: 34, of which 8 were waited for; matrix products, arithmetic and copies ran while one was open for 1% of the time, Pallas kernels for 17%

profile of v3, /device:TPU:0, one launch (start us, length us, event | category | flops | bytes accessed | tf_op | source)
XLA Modules:
  0.0 96.3 jit_solution(15586212698630306140)
XLA Ops:
  0.6 4.1 %collective-permute-start.10 = (bf16[256,256]{1,0:T(8,128)(2,1)}, bf16[256,256]{1,0:T(8,128)(2,1)S(1)}, u32[]{:S(2)}, u32[]{:S(2)}) collective-permute-start(bf16[256,256]{1,0:T(8,128)(2,1)} %refs_0_.2), channel_id=1, source_target_pairs={{0,4},{1,5},{2,6},{3,7},{4,0},{5,1},{6,2},{7,3},{8,12},{9,13},{10,... | collective-permute-start | bytes 393224 | tf_op jit(solution)/shard_map/ppermute | solution.py:53
  4.8 1.3 %collective-permute-start.11 = (bf16[256,256]{1,0:T(8,128)(2,1)}, bf16[256,256]{1,0:T(8,128)(2,1)S(1)}, u32[]{:S(2)}, u32[]{:S(2)}) collective-permute-start(bf16[256,256]{1,0:T(8,128)(2,1)} %refs_0_.2), channel_id=1, source_target_pairs={{0,6},{1,7},{2,4},{3,5},{4,2},{5,3},{6,0},{7,1},{8,14},{9,15},{10,... | collective-permute-start | bytes 393224 | tf_op jit(solution)/shard_map/ppermute | solution.py:53
  8.9 6.1 %collective-permute-done.10.refs_0_ = bf16[256,256]{1,0:T(8,128)(2,1)S(1)} collective-permute-done((bf16[256,256]{1,0:T(8,128)(2,1)}, bf16[256,256]{1,0:T(8,128)(2,1)S(1)}, u32[]{:S(2)}, u32[]{:S(2)}) %collective-permute-start.10) | collective-permute-done | bytes 131104 | tf_op jit(solution)/shard_map/ppermute | solution.py:53
  16.1 1.9 %collective-permute-start.12 = (bf16[192,512]{1,0:T(8,128)(2,1)S(1)}, bf16[192,512]{1,0:T(8,128)(2,1)S(1)}, u32[]{:S(2)}, u32[]{:S(2)}) collective-permute-start(bf16[192,512]{1,0:T(8,128)(2,1)S(1)} %get-tuple-element.67), channel_id=1, source_target_pairs={{0,8},{8,0},{16,24},{24,16},{1,9},{9,1},{17,25},{25,17},{2,10},{10... | collective-permute-start | bytes 589832 | tf_op jit(solution)/shard_map/ppermute | solution.py:53
  17.9 1.5 %collective-permute-start.13 = (bf16[192,512]{1,0:T(8,128)(2,1)S(1)}, bf16[192,512]{1,0:T(8,128)(2,1)S(1)}, u32[]{:S(2)}, u32[]{:S(2)}) collective-permute-start(bf16[192,512]{1,0:T(8,128)(2,1)S(1)} %get-tuple-element.68), channel_id=1, source_target_pairs={{0,16},{8,24},{16,0},{24,8},{1,17},{9,25},{17,1},{25,9},{2,18},{10... | collective-permute-start | bytes 589832 | tf_op jit(solution)/shard_map/ppermute | solution.py:53
  20.7 1.9 %collective-permute-start.7 = (bf16[192,512]{1,0:T(8,128)(2,1)S(1)}, bf16[192,512]{1,0:T(8,128)(2,1)S(1)}, u32[]{:S(2)}, u32[]{:S(2)}) collective-permute-start(bf16[192,512]{1,0:T(8,128)(2,1)S(1)} %get-tuple-element.63), channel_id=1, source_target_pairs={{0,8},{8,0},{16,24},{24,16},{1,9},{9,1},{17,25},{25,17},{2,10},{10... | collective-permute-start | bytes 589832 | tf_op jit(solution)/shard_map/ppermute | solution.py:53
  22.6 1.5 %collective-permute-start.8 = (bf16[192,512]{1,0:T(8,128)(2,1)S(1)}, bf16[192,512]{1,0:T(8,128)(2,1)S(1)}, u32[]{:S(2)}, u32[]{:S(2)}) collective-permute-start(bf16[192,512]{1,0:T(8,128)(2,1)S(1)} %get-tuple-element.64), channel_id=1, source_target_pairs={{0,16},{8,24},{16,0},{24,8},{1,17},{9,25},{17,1},{25,9},{2,18},{10... | collective-permute-start | bytes 589832 | tf_op jit(solution)/shard_map/ppermute | solution.py:53
  24.1 2.6 %collective-permute-start.9 = (bf16[192,512]{1,0:T(8,128)(2,1)S(1)}, bf16[192,512]{1,0:T(8,128)(2,1)S(1)}, u32[]{:S(2)}, u32[]{:S(2)}) collective-permute-start(bf16[192,512]{1,0:T(8,128)(2,1)S(1)} %get-tuple-element.65), channel_id=1, source_target_pairs={{0,24},{8,16},{16,8},{24,0},{1,25},{9,17},{17,9},{25,1},{2,26},{10... | collective-permute-start | bytes 589832 | tf_op jit(solution)/shard_map/ppermute | solution.py:53
  26.7 1.6 %collective-permute-done.13.refs_6_ = bf16[192,512]{1,0:T(8,128)(2,1)S(1)} collective-permute-done((bf16[192,512]{1,0:T(8,128)(2,1)S(1)}, bf16[192,512]{1,0:T(8,128)(2,1)S(1)}, u32[]{:S(2)}, u32[]{:S(2)}) %collective-permute-start.13) | collective-permute-done | bytes 196640 | tf_op jit(solution)/shard_map/ppermute | solution.py:53
  29.5 2.4 %collective-permute-done.7.refs_1_ = bf16[192,512]{1,0:T(8,128)(2,1)S(1)} collective-permute-done((bf16[192,512]{1,0:T(8,128)(2,1)S(1)}, bf16[192,512]{1,0:T(8,128)(2,1)S(1)}, u32[]{:S(2)}, u32[]{:S(2)}) %collective-permute-start.7) | collective-permute-done | bytes 196640 | tf_op jit(solution)/shard_map/ppermute | solution.py:53
  31.9 3.3 %collective-permute-done.8.refs_2_ = bf16[192,512]{1,0:T(8,128)(2,1)S(1)} collective-permute-done((bf16[192,512]{1,0:T(8,128)(2,1)S(1)}, bf16[192,512]{1,0:T(8,128)(2,1)S(1)}, u32[]{:S(2)}, u32[]{:S(2)}) %collective-permute-start.8) | collective-permute-done | bytes 196640 | tf_op jit(solution)/shard_map/ppermute | solution.py:53
  36.3 3.5 %shard_map.132 = (bf16[2,2048,512]{2,1,0:T(8,128)(2,1)S(1)}, bf16[2,2048,512]{2,1,0:T(8,128)(2,1)S(1)}) custom-call(bf16[2,2048,512]{2,1,0:T(8,128)(2,1)} %refs_0_.3, bf16[2,2048,512]{2,1,0:T(8,128)(2,1)} %refs_1_.1), custom_call_target="tpu_custom_call" | custom-call | flops 1048576 | bytes 16777216 | tf_op jit(solution)/shard_map/pallas_call | solution.py:299
  39.9 5.1 %hidden.1.hidden_ref = bf16[2,384,512]{2,1,0:T(8,128)(2,1)S(1)} custom-call(s32[3]{0:T(128)S(1)} %pad_add_fusion.place_ref.spot_ref, bf16[192,512]{1,0:T(8,128)(2,1)S(1)} %get-tuple-element.62.refs_0_, bf16[192,512]{1,0:T(8,128)(2,1)S(1)} %collective-permute-done.7.refs_1_, bf16[192,512]{1,0:T(8,128)(2,1)S(1)} %collective-permute-done.8.refs_2_, ...), custom_call_target="tpu_custom_call" | custom-call | flops 3221225472 | bytes 14680064 | tf_op jit(solution)/shard_map/hidden/pallas_call | solution.py:353
  45.0 1.5 %down.3 = (bf16[768,512]{1,0:T(8,128)(2,1)S(1)}, bf16[768,512]{1,0:T(8,128)(2,1)S(1)}) custom-call(s32[3]{0:T(128)S(1)} %pad_add_fusion.place_ref.spot_ref, bf16[2,384,512]{2,1,0:T(8,128)(2,1)S(1)} %hidden.1.hidden_ref, bf16[2,512,2048]{2,1,0:T(8,128)(2,1)S(1)} %copy-done), custom_call_target="tpu_custom_call" | custom-call | flops 805306368 | bytes 3670016 | tf_op jit(solution)/shard_map/down/pallas_call | solution.py:394
  47.2 1.5 %down.2 = (bf16[768,512]{1,0:T(8,128)(2,1)S(1)}, bf16[768,512]{1,0:T(8,128)(2,1)S(1)}) custom-call(s32[3]{0:T(128)S(1)} %pad_add_fusion.place_ref.spot_ref, bf16[2,384,512]{2,1,0:T(8,128)(2,1)S(1)} %hidden.1.hidden_ref, bf16[2,512,2048]{2,1,0:T(8,128)(2,1)S(1)} %copy-done), custom_call_target="tpu_custom_call" | custom-call | flops 805306368 | bytes 3670016 | tf_op jit(solution)/shard_map/down/pallas_call | solution.py:394
  52.6 1.7 %collective-permute-start.2 = (bf16[1280,128]{1,0:T(8,128)(2,1)S(1)}, bf16[1280,128]{1,0:T(8,128)(2,1)S(1)}, u32[]{:S(2)}, u32[]{:S(2)}) collective-permute-start(bf16[1280,128]{1,0:T(8,128)(2,1)S(1)} %get-tuple-element.54), channel_id=1, source_target_pairs={{0,24},{8,16},{16,8},{24,0},{1,25},{9,17},{17,9},{25,1},{2,26},{10... | collective-permute-start | bytes 983048 | tf_op jit(solution)/shard_map/ppermute | solution.py:53
  54.5 4.4 %collective-permute-start.30 = (bf16[768,256]{1,0:T(8,128)(2,1)S(1)}, bf16[768,256]{1,0:T(8,128)(2,1)S(1)}, u32[]{:S(2)}, u32[]{:S(2)}) collective-permute-start(bf16[768,256]{1,0:T(8,128)(2,1)S(1)} %get-tuple-element.83), channel_id=1, source_target_pairs={{0,2},{1,3},{2,0},{3,1},{4,6},{5,7},{6,4},{7,5},{8,10},{9,11},{10,... | collective-permute-start | bytes 1179656 | tf_op jit(solution)/shard_map/ppermute | solution.py:53
  59.1 1.3 %collective-permute-start.24 = (bf16[192,512]{1,0:T(8,128)(2,1)S(1)}, bf16[192,512]{1,0:T(8,128)(2,1)S(1)}, u32[]{:S(2)}, u32[]{:S(2)}) collective-permute-start(bf16[192,512]{1,0:T(8,128)(2,1)S(1)} %get-tuple-element.75), channel_id=1, source_target_pairs={{0,8},{8,0},{16,24},{24,16},{1,9},{9,1},{17,25},{25,17},{2,10},{10... | collective-permute-start | bytes 589832 | tf_op jit(solution)/shard_map/ppermute | solution.py:53
  62.6 8.5 %collective-permute-start.26 = (bf16[192,512]{1,0:T(8,128)(2,1)S(1)}, bf16[192,512]{1,0:T(8,128)(2,1)S(1)}, u32[]{:S(2)}, u32[]{:S(2)}) collective-permute-start(bf16[192,512]{1,0:T(8,128)(2,1)S(1)} %get-tuple-element.77), channel_id=1, source_target_pairs={{0,24},{8,16},{16,8},{24,0},{1,25},{9,17},{17,9},{25,1},{2,26},{10... | collective-permute-start | bytes 589832 | tf_op jit(solution)/shard_map/ppermute | solution.py:53
  71.1 5.2 %attention.1 = (bf16[256,128]{1,0:T(8,128)(2,1)S(1)}, bf16[256,128]{1,0:T(8,128)(2,1)S(1)}, bf16[256,128]{1,0:T(8,128)(2,1)S(1)}, bf16[256,128]{1,0:T(8,128)(2,1)S(1)}) custom-call(s32[3]{0:T(128)S(1)} %pad_add_fusion.place_ref.spot_ref, f32[2]{0:T(128)S(1)} %copy-done.5, bf16[1280,128]{1,0:T(8,128)(2,1)S(1)} %get-tuple-element.51.refs_0_, ...), custom_call_target="tpu_custom_call" | custom-call | flops 1342177280 | bytes 1310720 | tf_op jit(solution)/shard_map/attention/pallas_call | solution.py:176
  76.9 2.9 %collective-permute-start.5 = (bf16[256,128]{1,0:T(8,128)(2,1)S(1)}, bf16[256,128]{1,0:T(8,128)(2,1)S(1)}, u32[]{:S(2)}, u32[]{:S(2)}) collective-permute-start(bf16[256,128]{1,0:T(8,128)(2,1)S(1)} %get-tuple-element.58), channel_id=1, source_target_pairs={{0,24},{8,16},{16,8},{24,0},{1,25},{9,17},{17,9},{25,1},{2,26},{10... | collective-permute-start | bytes 196616 | tf_op jit(solution)/shard_map/ppermute | solution.py:53
  80.5 6.6 %collective-permute-start.27 = (bf16[256,256]{1,0:T(8,128)(2,1)S(1)}, bf16[256,256]{1,0:T(8,128)(2,1)S(1)}, u32[]{:S(2)}, u32[]{:S(2)}) collective-permute-start(bf16[256,256]{1,0:T(8,128)(2,1)S(1)} %get-tuple-element.78), channel_id=1, source_target_pairs={{0,4},{1,5},{2,6},{3,7},{4,0},{5,1},{6,2},{7,3},{8,12},{9,13},{10,... | collective-permute-start | bytes 393224 | tf_op jit(solution)/shard_map/ppermute | solution.py:53
  88.4 2.9 %collective-permute-start.33 = (bf16[192,256]{1,0:T(8,128)(2,1)S(1)}, bf16[192,256]{1,0:T(8,128)(2,1)S(1)}, u32[]{:S(2)}, u32[]{:S(2)}) collective-permute-start(bf16[192,256]{1,0:T(8,128)(2,1)S(1)} %get-tuple-element.87), channel_id=1, source_target_pairs={{0,24},{8,16},{16,8},{24,0},{1,25},{9,17},{17,9},{25,1},{2,26},{10... | collective-permute-start | bytes 294920 | tf_op jit(solution)/shard_map/ppermute | solution.py:53
  94.3 1.3 %collective-permute-done.27.refs_0_ = bf16[256,256]{1,0:T(8,128)(2,1)S(1)} collective-permute-done((bf16[256,256]{1,0:T(8,128)(2,1)S(1)}, bf16[256,256]{1,0:T(8,128)(2,1)S(1)}, u32[]{:S(2)}, u32[]{:S(2)}) %collective-permute-start.27) | collective-permute-done | bytes 131104 | tf_op jit(solution)/shard_map/ppermute | solution.py:53
  (85 shorter events, 20.8 us)
Async XLA Ops:
  0.6 14.3 %collective-permute-start.10 = (bf16[256,256]{1,0:T(8,128)(2,1)}, bf16[256,256]{1,0:T(8,128)(2,1)S(1)}, u32[]{:S(2)}, u32[]{:S(2)}) collective-permute-start(bf16[256,256]{1,0:T(8,128)(2,1)} %refs_0_.2), channel_id=1, source_target_pairs={{0,4},{1,5},{2,6},{3,7},{4,0},{5,1},{6,2},{7,3},{8,12},{9,13},{10,... | collective-permute-start | bytes 393224 | tf_op jit(solution)/shard_map/ppermute | solution.py:53
  4.8 10.2 %collective-permute-start.11 = (bf16[256,256]{1,0:T(8,128)(2,1)}, bf16[256,256]{1,0:T(8,128)(2,1)S(1)}, u32[]{:S(2)}, u32[]{:S(2)}) collective-permute-start(bf16[256,256]{1,0:T(8,128)(2,1)} %refs_0_.2), channel_id=1, source_target_pairs={{0,6},{1,7},{2,4},{3,5},{4,2},{5,3},{6,0},{7,1},{8,14},{9,15},{10,... | collective-permute-start | bytes 393224 | tf_op jit(solution)/shard_map/ppermute | solution.py:53
  6.1 13.5 %collective-permute-start.6 = (bf16[256,256]{1,0:T(8,128)(2,1)}, bf16[256,256]{1,0:T(8,128)(2,1)S(1)}, u32[]{:S(2)}, u32[]{:S(2)}) collective-permute-start(bf16[256,256]{1,0:T(8,128)(2,1)} %refs_0_.2), channel_id=1, source_target_pairs={{0,2},{1,3},{2,0},{3,1},{4,6},{5,7},{6,4},{7,5},{8,10},{9,11},{10,... | collective-permute-start | bytes 393224 | tf_op jit(solution)/shard_map/ppermute | solution.py:53
  16.1 8.0 %collective-permute-start.12 = (bf16[192,512]{1,0:T(8,128)(2,1)S(1)}, bf16[192,512]{1,0:T(8,128)(2,1)S(1)}, u32[]{:S(2)}, u32[]{:S(2)}) collective-permute-start(bf16[192,512]{1,0:T(8,128)(2,1)S(1)} %get-tuple-element.67), channel_id=1, source_target_pairs={{0,8},{8,0},{16,24},{24,16},{1,9},{9,1},{17,25},{25,17},{2,10},{10... | collective-permute-start | bytes 589832 | tf_op jit(solution)/shard_map/ppermute | solution.py:53
  17.9 10.3 %collective-permute-start.13 = (bf16[192,512]{1,0:T(8,128)(2,1)S(1)}, bf16[192,512]{1,0:T(8,128)(2,1)S(1)}, u32[]{:S(2)}, u32[]{:S(2)}) collective-permute-start(bf16[192,512]{1,0:T(8,128)(2,1)S(1)} %get-tuple-element.68), channel_id=1, source_target_pairs={{0,16},{8,24},{16,0},{24,8},{1,17},{9,25},{17,1},{25,9},{2,18},{10... | collective-permute-start | bytes 589832 | tf_op jit(solution)/shard_map/ppermute | solution.py:53
  19.5 10.0 %collective-permute-start.14 = (bf16[192,512]{1,0:T(8,128)(2,1)S(1)}, bf16[192,512]{1,0:T(8,128)(2,1)S(1)}, u32[]{:S(2)}, u32[]{:S(2)}) collective-permute-start(bf16[192,512]{1,0:T(8,128)(2,1)S(1)} %get-tuple-element.69), channel_id=1, source_target_pairs={{0,24},{8,16},{16,8},{24,0},{1,25},{9,17},{17,9},{25,1},{2,26},{10... | collective-permute-start | bytes 589832 | tf_op jit(solution)/shard_map/ppermute | solution.py:53
  20.7 11.2 %collective-permute-start.7 = (bf16[192,512]{1,0:T(8,128)(2,1)S(1)}, bf16[192,512]{1,0:T(8,128)(2,1)S(1)}, u32[]{:S(2)}, u32[]{:S(2)}) collective-permute-start(bf16[192,512]{1,0:T(8,128)(2,1)S(1)} %get-tuple-element.63), channel_id=1, source_target_pairs={{0,8},{8,0},{16,24},{24,16},{1,9},{9,1},{17,25},{25,17},{2,10},{10... | collective-permute-start | bytes 589832 | tf_op jit(solution)/shard_map/ppermute | solution.py:53
  22.6 12.6 %collective-permute-start.8 = (bf16[192,512]{1,0:T(8,128)(2,1)S(1)}, bf16[192,512]{1,0:T(8,128)(2,1)S(1)}, u32[]{:S(2)}, u32[]{:S(2)}) collective-permute-start(bf16[192,512]{1,0:T(8,128)(2,1)S(1)} %get-tuple-element.64), channel_id=1, source_target_pairs={{0,16},{8,24},{16,0},{24,8},{1,17},{9,25},{17,1},{25,9},{2,18},{10... | collective-permute-start | bytes 589832 | tf_op jit(solution)/shard_map/ppermute | solution.py:53
  24.1 11.1 %collective-permute-start.9 = (bf16[192,512]{1,0:T(8,128)(2,1)S(1)}, bf16[192,512]{1,0:T(8,128)(2,1)S(1)}, u32[]{:S(2)}, u32[]{:S(2)}) collective-permute-start(bf16[192,512]{1,0:T(8,128)(2,1)S(1)} %get-tuple-element.65), channel_id=1, source_target_pairs={{0,24},{8,16},{16,8},{24,0},{1,25},{9,17},{17,9},{25,1},{2,26},{10... | collective-permute-start | bytes 589832 | tf_op jit(solution)/shard_map/ppermute | solution.py:53
  28.3 7.5 %collective-permute-start.19 = (bf16[192,512]{1,0:T(8,128)(2,1)S(1)}, bf16[192,512]{1,0:T(8,128)(2,1)S(1)}, u32[]{:S(2)}, u32[]{:S(2)}) collective-permute-start(bf16[192,512]{1,0:T(8,128)(2,1)S(1)} %get-tuple-element.66.refs_4_), channel_id=1, source_target_pairs={{0,1},{1,0},{2,3},{3,2},{4,5},{5,4},{6,7},{7,6},{8,9},{9,8},{10,11... | collective-permute-start | bytes 589832 | tf_op jit(solution)/shard_map/ppermute | solution.py:53
  46.6 7.7 %collective-permute-start.29 = (bf16[768,512]{1,0:T(8,128)(2,1)S(1)}, bf16[768,512]{1,0:T(8,128)(2,1)S(1)}, u32[]{:S(2)}, u32[]{:S(2)}) collective-permute-start(bf16[768,512]{1,0:T(8,128)(2,1)S(1)} %get-tuple-element.81), channel_id=1, source_target_pairs={{0,1},{1,0},{2,3},{3,2},{4,5},{5,4},{6,7},{7,6},{8,9},{9,8},{10,11... | collective-permute-start | bytes 2359304 | tf_op jit(solution)/shard_map/ppermute | solution.py:53
  48.7 10.2 %collective-permute-start.23 = (bf16[768,512]{1,0:T(8,128)(2,1)S(1)}, bf16[768,512]{1,0:T(8,128)(2,1)S(1)}, u32[]{:S(2)}, u32[]{:S(2)}) collective-permute-start(bf16[768,512]{1,0:T(8,128)(2,1)S(1)} %get-tuple-element.73), channel_id=1, source_target_pairs={{0,1},{1,0},{2,3},{3,2},{4,5},{5,4},{6,7},{7,6},{8,9},{9,8},{10,11... | collective-permute-start | bytes 2359304 | tf_op jit(solution)/shard_map/ppermute | solution.py:53
  50.7 10.6 %collective-permute-start = (bf16[1280,128]{1,0:T(8,128)(2,1)S(1)}, bf16[1280,128]{1,0:T(8,128)(2,1)S(1)}, u32[]{:S(2)}, u32[]{:S(2)}) collective-permute-start(bf16[1280,128]{1,0:T(8,128)(2,1)S(1)} %get-tuple-element.52), channel_id=1, source_target_pairs={{0,8},{8,0},{16,24},{24,16},{1,9},{9,1},{17,25},{25,17},{2,10},{10... | collective-permute-start | bytes 983048 | tf_op jit(solution)/shard_map/ppermute | solution.py:53
  51.7 10.9 %collective-permute-start.1 = (bf16[1280,128]{1,0:T(8,128)(2,1)S(1)}, bf16[1280,128]{1,0:T(8,128)(2,1)S(1)}, u32[]{:S(2)}, u32[]{:S(2)}) collective-permute-start(bf16[1280,128]{1,0:T(8,128)(2,1)S(1)} %get-tuple-element.53), channel_id=1, source_target_pairs={{0,16},{8,24},{16,0},{24,8},{1,17},{9,25},{17,1},{25,9},{2,18},{10... | collective-permute-start | bytes 983048 | tf_op jit(solution)/shard_map/ppermute | solution.py:53
  52.6 18.5 %collective-permute-start.2 = (bf16[1280,128]{1,0:T(8,128)(2,1)S(1)}, bf16[1280,128]{1,0:T(8,128)(2,1)S(1)}, u32[]{:S(2)}, u32[]{:S(2)}) collective-permute-start(bf16[1280,128]{1,0:T(8,128)(2,1)S(1)} %get-tuple-element.54), channel_id=1, source_target_pairs={{0,24},{8,16},{16,8},{24,0},{1,25},{9,17},{17,9},{25,1},{2,26},{10... | collective-permute-start | bytes 983048 | tf_op jit(solution)/shard_map/ppermute | solution.py:53
  54.5 32.6 %collective-permute-start.30 = (bf16[768,256]{1,0:T(8,128)(2,1)S(1)}, bf16[768,256]{1,0:T(8,128)(2,1)S(1)}, u32[]{:S(2)}, u32[]{:S(2)}) collective-permute-start(bf16[768,256]{1,0:T(8,128)(2,1)S(1)} %get-tuple-element.83), channel_id=1, source_target_pairs={{0,2},{1,3},{2,0},{3,1},{4,6},{5,7},{6,4},{7,5},{8,10},{9,11},{10,... | collective-permute-start | bytes 1179656 | tf_op jit(solution)/shard_map/ppermute | solution.py:53
  59.1 17.3 %collective-permute-start.24 = (bf16[192,512]{1,0:T(8,128)(2,1)S(1)}, bf16[192,512]{1,0:T(8,128)(2,1)S(1)}, u32[]{:S(2)}, u32[]{:S(2)}) collective-permute-start(bf16[192,512]{1,0:T(8,128)(2,1)S(1)} %get-tuple-element.75), channel_id=1, source_target_pairs={{0,8},{8,0},{16,24},{24,16},{1,9},{9,1},{17,25},{25,17},{2,10},{10... | collective-permute-start | bytes 589832 | tf_op jit(solution)/shard_map/ppermute | solution.py:53
  61.4 15.5 %collective-permute-start.25 = (bf16[192,512]{1,0:T(8,128)(2,1)S(1)}, bf16[192,512]{1,0:T(8,128)(2,1)S(1)}, u32[]{:S(2)}, u32[]{:S(2)}) collective-permute-start(bf16[192,512]{1,0:T(8,128)(2,1)S(1)} %get-tuple-element.76), channel_id=1, source_target_pairs={{0,16},{8,24},{16,0},{24,8},{1,17},{9,25},{17,1},{25,9},{2,18},{10... | collective-permute-start | bytes 589832 | tf_op jit(solution)/shard_map/ppermute | solution.py:53
  62.6 17.3 %collective-permute-start.26 = (bf16[192,512]{1,0:T(8,128)(2,1)S(1)}, bf16[192,512]{1,0:T(8,128)(2,1)S(1)}, u32[]{:S(2)}, u32[]{:S(2)}) collective-permute-start(bf16[192,512]{1,0:T(8,128)(2,1)S(1)} %get-tuple-element.77), channel_id=1, source_target_pairs={{0,24},{8,16},{16,8},{24,0},{1,25},{9,17},{17,9},{25,1},{2,26},{10... | collective-permute-start | bytes 589832 | tf_op jit(solution)/shard_map/ppermute | solution.py:53
  76.3 11.5 %collective-permute-start.3 = (bf16[256,128]{1,0:T(8,128)(2,1)S(1)}, bf16[256,128]{1,0:T(8,128)(2,1)S(1)}, u32[]{:S(2)}, u32[]{:S(2)}) collective-permute-start(bf16[256,128]{1,0:T(8,128)(2,1)S(1)} %get-tuple-element.56), channel_id=1, source_target_pairs={{0,8},{8,0},{16,24},{24,16},{1,9},{9,1},{17,25},{25,17},{2,10},{10... | collective-permute-start | bytes 196616 | tf_op jit(solution)/shard_map/ppermute | solution.py:53
  76.4 11.5 %collective-permute-start.4 = (bf16[256,128]{1,0:T(8,128)(2,1)S(1)}, bf16[256,128]{1,0:T(8,128)(2,1)S(1)}, u32[]{:S(2)}, u32[]{:S(2)}) collective-permute-start(bf16[256,128]{1,0:T(8,128)(2,1)S(1)} %get-tuple-element.57), channel_id=1, source_target_pairs={{0,16},{8,24},{16,0},{24,8},{1,17},{9,25},{17,1},{25,9},{2,18},{10... | collective-permute-start | bytes 196616 | tf_op jit(solution)/shard_map/ppermute | solution.py:53
  76.9 11.5 %collective-permute-start.5 = (bf16[256,128]{1,0:T(8,128)(2,1)S(1)}, bf16[256,128]{1,0:T(8,128)(2,1)S(1)}, u32[]{:S(2)}, u32[]{:S(2)}) collective-permute-start(bf16[256,128]{1,0:T(8,128)(2,1)S(1)} %get-tuple-element.58), channel_id=1, source_target_pairs={{0,24},{8,16},{16,8},{24,0},{1,25},{9,17},{17,9},{25,1},{2,26},{10... | collective-permute-start | bytes 196616 | tf_op jit(solution)/shard_map/ppermute | solution.py:53
  80.5 15.1 %collective-permute-start.27 = (bf16[256,256]{1,0:T(8,128)(2,1)S(1)}, bf16[256,256]{1,0:T(8,128)(2,1)S(1)}, u32[]{:S(2)}, u32[]{:S(2)}) collective-permute-start(bf16[256,256]{1,0:T(8,128)(2,1)S(1)} %get-tuple-element.78), channel_id=1, source_target_pairs={{0,4},{1,5},{2,6},{3,7},{4,0},{5,1},{6,2},{7,3},{8,12},{9,13},{10,... | collective-permute-start | bytes 393224 | tf_op jit(solution)/shard_map/ppermute | solution.py:53
  87.1 8.5 %collective-permute-start.28 = (bf16[256,256]{1,0:T(8,128)(2,1)S(1)}, bf16[256,256]{1,0:T(8,128)(2,1)S(1)}, u32[]{:S(2)}, u32[]{:S(2)}) collective-permute-start(bf16[256,256]{1,0:T(8,128)(2,1)S(1)} %get-tuple-element.79), channel_id=1, source_target_pairs={{0,6},{1,7},{2,4},{3,5},{4,2},{5,3},{6,0},{7,1},{8,14},{9,15},{10,... | collective-permute-start | bytes 393224 | tf_op jit(solution)/shard_map/ppermute | solution.py:53
  (20 other events, 128.9 us)

commit v4 on v3

--- a/solution.py
+++ b/solution.py
@@ -17,6 +17,7 @@
 LOG2E = 1.4426950408889634
 CORES = 2
 FETCH_GRANT = 44
+SPLITS = 2
 BF16 = jnp.bfloat16
 F32 = jnp.float32
 
@@ -284,8 +285,12 @@
     arrivals = refs[-1]
     copies = []
     for source, target in zip(refs[:count], refs[count : 2 * count]):
-        parts = [()] if len(source.shape) < 3 else [(piece,) for piece in range(source.shape[0])]
-        for part in parts:
+        count = 1 if len(source.shape) < 3 else SPLITS
+        rows = source.shape[-2] // count
+        for index in range(source.shape[0] * count if count > 1 else 1):
+            part = (
+                (index // count, pl.ds(index % count * rows, rows)) if count > 1 else ()
+            )
             copies.append(
                 pltpu.make_async_copy(source.at[part], target.at[part], arrivals.at[len(copies)])
             )
@@ -301,71 +306,94 @@
         out_shape=[shape_of(*array.shape, dtype=array.dtype) for array in arrays],
         in_specs=[far()] * len(arrays),
         out_specs=[whole()] * len(arrays),
-        scratch_shapes=[pltpu.SemaphoreType.DMA((2 * len(arrays),))],
+        scratch_shapes=[pltpu.SemaphoreType.DMA((2 * SPLITS * len(arrays),))],
         cost_estimate=cost(2**20, sum(4 * array.size for array in arrays)),
         compiler_params=grant(mebibytes),
     )(*arrays)
 
 
-def hidden_kernel(spot_ref, *refs, count, groups, capacity, width):
+def hidden_kernel(spot_ref, *refs, groups, capacity, width, chunk, last):
+    count = CORES * groups
     slot_refs = refs[:count]
-    gain_ref, gate_ref, up_ref, hidden_ref, normed = refs[count:]
+    gain_ref, gate_ref, up_ref = refs[count : count + 3]
+    rest = refs[count + 3 :]
     pieces, total_width, ff = gate_ref.shape
     tile = 256 if ff % 256 == 0 else ff
-    chunks = count // groups // 2
     span = slot_refs[0].shape[1] // width
+    depth = CORES * span * width
+    first = lax.div(spot_ref[1], span)
+    base = pl.multiple_of((first if chunk == 0 else jnp.bitwise_xor(first, chunk)) * depth, depth)
+    if last:
+        sums_ref, squares_ref, hidden_ref, normed = rest
+    else:
+        sums_ref, squares_ref, normed = rest
     factors = [[None] * groups for _ in range(pieces)]
+    slots = pieces * capacity
     for group in range(groups):
-        squares = jnp.zeros((pieces * capacity, 1), F32)
+        squares = jnp.zeros((slots, 1), F32)
         for side in range(CORES):
-            for chunk in range(chunks):
-                ref = slot_refs[(side * chunks + chunk) * groups + group]
-                for inner in range(span):
-                    floats = ref[:, inner * width : (inner + 1) * width].astype(F32)
-                    squares += jnp.sum(floats * floats, axis=-1, keepdims=True)
-                    start = block_start(spot_ref, chunk * span + inner, side, width)
-                    place = pl.ds(pl.multiple_of(start, width), width)
-                    value = (floats * gain_ref[:, place]).astype(BF16)
-                    for piece in range(pieces):
-                        normed[piece, group * capacity : (group + 1) * capacity, place] = value[
-                            piece * capacity : (piece + 1) * capacity
-                        ]
-        factor = lax.rsqrt(squares / total_width + NORM_EPS)
-        for piece in range(pieces):
-            factors[piece][group] = factor[piece * capacity : (piece + 1) * capacity]
+            ref = slot_refs[side * groups + group]
+            for inner in range(span):
+                floats = ref[:, inner * width : (inner + 1) * width].astype(F32)
+                squares += jnp.sum(floats * floats, axis=-1, keepdims=True)
+                start = block_start(spot_ref, chunk * span + inner, side, width)
+                gain = gain_ref[:, pl.ds(pl.multiple_of(start, width), width)]
+                value = (floats * gain).astype(BF16)
+                place = pl.ds(pl.multiple_of(start - base, width), width)
+                for piece in range(pieces):
+                    normed[piece, group * capacity : (group + 1) * capacity, place] = value[
+                        piece * capacity : (piece + 1) * capacity
+                    ]
+        rows = slice(group * slots, (group + 1) * slots)
+        if last:
+            squares += squares_ref[rows, 0:1]
+            factor = lax.rsqrt(squares / total_width + NORM_EPS)
+            for piece in range(pieces):
+                factors[piece][group] = factor[piece * capacity : (piece + 1) * capacity]
+        else:
+            squares_ref[rows] = jnp.broadcast_to(squares, (slots, squares_ref.shape[1]))
     for piece in range(pieces):
-        factor = jnp.concatenate(factors[piece], axis=0)
+        factor = jnp.concatenate(factors[piece], axis=0) if last else None
         for start in range(0, ff, tile):
             columns = slice(start, start + tile)
-            gate = jnp.dot(normed[piece], gate_ref[piece, :, columns], preferred_element_type=F32)
-            up = jnp.dot(normed[piece], up_ref[piece, :, columns], preferred_element_type=F32)
-            gate = jnp.minimum(gate * factor, CLAMP_LIMIT)
-            up = jnp.clip(up * factor, -CLAMP_LIMIT, CLAMP_LIMIT)
-            hidden_ref[piece, :, columns] = (
-                (up + 1.0) * gate * jax.nn.sigmoid(GLU_ALPHA * gate)
-            ).astype(BF16)
-
-
-def hidden_units(spot, own, other, gain, gate_weight, up_weight, groups, capacity, width):
-    pieces, total_width, ff = gate_weight.shape
-    tables = [table for side in (own, other) for chunk in side for table in chunk]
-    rows = groups * capacity
+            pair = []
+            for kind, ref in enumerate((gate_ref, up_ref)):
+                value = jnp.dot(
+                    normed[piece],
+                    ref[piece, pl.ds(base, depth), columns],
+                    preferred_element_type=F32,
+                )
+                if last:
+                    pair.append((value + sums_ref[kind, piece, :, columns]) * factor)
+                else:
+                    sums_ref[kind, piece, :, columns] = value
+            if last:
+                gate = jnp.minimum(pair[0], CLAMP_LIMIT)
+                up = jnp.clip(pair[1], -CLAMP_LIMIT, CLAMP_LIMIT)
+                hidden_ref[piece, :, columns] = (
+                    (up + 1.0) * gate * jax.nn.sigmoid(GLU_ALPHA * gate)
+                ).astype(BF16)
+
+
+def hidden_units(spot, tables, prior, gain, gate, up, groups, capacity, width, chunk):
+    pieces, _, ff = gate.shape
+    rows, depth = groups * capacity, CORES * tables[0].shape[1]
+    last = prior is not None
+    sums = [shape_of(2, pieces, rows, ff, dtype=F32), shape_of(pieces * rows, 128, dtype=F32)]
+    inputs = list(tables) + [gain[None, :], gate, up] + (list(prior) if last else [])
     return pl.pallas_call(
         functools.partial(
-            hidden_kernel, count=len(tables), groups=groups, capacity=capacity, width=width
+            hidden_kernel, groups=groups, capacity=capacity, width=width, chunk=chunk, last=last
         ),
-        out_shape=shape_of(pieces, rows, ff),
-        in_specs=[scalars()] + [whole()] * (len(tables) + 3),
-        out_specs=whole(),
-        scratch_shapes=[pltpu.VMEM((pieces, rows, total_width), BF16)],
+        out_shape=shape_of(pieces, rows, ff) if last else sums,
+        in_specs=[scalars()] + [whole()] * len(inputs),
+        out_specs=whole() if last else [whole()] * 2,
+        scratch_shapes=[pltpu.VMEM((pieces, rows, depth), BF16)],
         cost_estimate=cost(
-            4 * pieces * rows * total_width * ff,
-            4 * pieces * total_width * (ff + rows),
-            pieces * rows * ff,
+            4 * pieces * rows * depth * ff, 4 * pieces * depth * (ff + rows), pieces * rows * ff
         ),
-        compiler_params=grant(20),
-        name="hidden",
-    )(spot, *tables, gain[None, :], gate_weight, up_weight)
+        compiler_params=grant(14),
+    )(spot, *inputs)
 
 
 def down_kernel(
@@ -517,12 +545,10 @@
     )(place, routes, route_weights)
 
 
-def gather_kernel(chosen_ref, weights_ref, *refs, groups):
-    table_refs, out_refs = refs[:groups], refs[groups:]
-    picks = chosen_ref.shape[0] // groups
-    width = out_refs[0].shape[1]
+def gather_rows(chosen_ref, scale_ref, table_refs):
+    groups = len(table_refs)
     total = None
-    for pick in range(picks):
+    for pick in range(chosen_ref.shape[0] // groups):
         picked = None
         for group in range(groups):
             part = jnp.dot(
@@ -531,8 +557,15 @@
                 preferred_element_type=F32,
             )
             picked = part if picked is None else picked + part
-        picked = picked * weights_ref[:, pick : pick + 1]
+        picked = picked * scale_ref[:, pick : pick + 1]
         total = picked if total is None else total + picked
+    return total
+
+
+def gather_kernel(chosen_ref, scale_ref, *refs, groups):
+    total = gather_rows(chosen_ref, scale_ref, refs[:groups])
+    out_refs = refs[groups:]
+    width = out_refs[0].shape[1]
     for level, ref in enumerate(out_refs):
         ref[...] = total[:, level * width : (level + 1) * width].astype(BF16)
 
@@ -555,24 +588,25 @@
     )(chosen, scale, *tables)
 
 
-def final_kernel(*refs):
-    total = refs[0][...].astype(F32)
-    for ref in refs[1:-1]:
+def final_kernel(chosen_ref, scale_ref, *refs, groups):
+    total = gather_rows(chosen_ref, scale_ref, refs[:groups])
+    for ref in refs[groups:-1]:
         total += ref[...].astype(F32)
     refs[-1][...] = total.astype(BF16)
 
 
-def final(parts):
+def final(chosen, scale, tables, parts):
     rows, width = parts[0].shape
-    return pl.pallas_call(
-        final_kernel,
+    groups = len(tables)
+    return pl.pallas_call(
+        functools.partial(final_kernel, groups=groups),
         out_shape=shape_of(rows, width),
-        in_specs=[whole()] * len(parts),
+        in_specs=[whole()] * (2 + groups + len(parts)),
         out_specs=whole(),
-        cost_estimate=cost(2**20, 2 * len(parts) * rows * width),
-        compiler_params=grant(4),
+        cost_estimate=cost(2**28, 2 * (groups + len(parts)) * rows * width),
+        compiler_params=grant(8),
         name="final",
-    )(*parts)
+    )(chosen, scale, *tables, *parts)
 
 
 def shards(
@@ -593,6 +627,7 @@
     by_level = [tokens]
     for mask in range(1, levels):
         by_level.append(levels_flip(tokens, mask))
+    (gate_near,) = fetch(gate_weight, mebibytes=FETCH_GRANT)
     by_level[0], picked, picked_weights = fetch(tokens, routes.T, route_weights.T, mebibytes=2)
     chosen, scale = plan(
         place, picked, picked_weights, capacity, pieces, experts, groups
@@ -610,10 +645,13 @@
         for table in own[chunk]:
             swapped.append(cores_flip(table))
         other.append(swapped)
-    gate_near, up_near = fetch(gate_weight, up_weight, mebibytes=FETCH_GRANT)
-    hidden = hidden_units(
-        spot, own, other, expert_gain, gate_near, up_near, groups, capacity, width
-    )
+    (up_near,) = fetch(up_weight, mebibytes=FETCH_GRANT)
+    hidden = None
+    for chunk in range(2):
+        hidden = hidden_units(
+            spot, own[chunk] + other[chunk], hidden, expert_gain, gate_near, up_near,
+            groups, capacity, width, chunk,
+        )
     halves = []
     for first in (0, half):
         sent, kept = down(
@@ -631,10 +669,9 @@
         results.append(levels_flip(value, half + inner))
     tables = sum_levels(values, groups)
     tables = exchange(tables)
-    results += gather(chosen, scale, tables, 1)
     attended = attention(place, bundles, mix_weight, sub_gain, queries.shape[0])
     attended = exchange(attended)
-    moe_out = final(results)
+    moe_out = final(chosen, scale, tables, results)
     attn_out = unpack(place, attended, queries.shape[1])
     return (attn_out, moe_out)
 

time: 96.5 us -> 89.7 us (0.930)
  starting transfers between devices: 50.1 us -> 37 us
  local copies, waits for them, and re-layouts: 3.42 us -> 7.85 us
  waiting for transfers between devices: 18.1 us -> 21.6 us
  Pallas kernels: 23.7 us -> 21.9 us
    ppermute x34, starting transfers between devices: 50.1 us -> 37 us  [flip(): return lax.ppermute(value, axis, pairs)]
    unnamed x21 -> x25, local copies, waits for them, and re-layouts: 3.31 us -> 7.74 us
    ppermute x34, waiting for transfers between devices: 18.1 us -> 21.6 us  [flip(): return lax.ppermute(value, axis, pairs)]
    pallas_call x2 -> x3, Pallas kernels: 3.69 us -> 0.89 us  [fetch(): pl.pallas_call(fetch_kernel, out_shape=[shape_of(*array.shape, dtype=arra...]
    pallas_call x2 -> x3, Pallas kernels: 5.79 us -> 7.18 us  [the longest x2 6.08 us: hidden_units(): pl.pallas_call(functools.partial(hidden_kernel, groups=groups, capacity=c...]
  transfers between devices with their start and end apart: 34 -> 34, of which waited for: 8 -> 7; matrix products, arithmetic and copies ran while one was open for 1% -> 1% of each run, Pallas kernels for 17% -> 18%
where the time goes in v4:
time: 89.7 us; the launch traced here: 89.4 us
  starting transfers between devices  37 us (41%)
  Pallas kernels  21.9 us (24%)
  waiting for transfers between devices  21.6 us (24%)
  local copies, waits for them, and re-layouts  7.85 us (9%)
  between operations  0.95 us (1%)
    ppermute x34, starting transfers between devices, flip(): return lax.ppermute(value, axis, pairs)  37 us
    ppermute x34, waiting for transfers between devices, flip(): return lax.ppermute(value, axis, pairs)  21.6 us
    unnamed x25, local copies, waits for them, and re-layouts  7.74 us
    pallas_call x2, Pallas kernels, hidden_units(): pl.pallas_call(functools.partial(hidden_kernel, groups=groups, capacity=c...  6.08 us
    pallas_call x1, Pallas kernels, attention(): pl.pallas_call(functools.partial(attention_kernel, groups=groups, rows=ro...  5.19 us
    pallas_call x2, Pallas kernels, down(): pl.pallas_call(functools.partial(down_kernel, groups=groups, capacity=cap...  3.08 us
    pallas_call x2, Pallas kernels, dispatch(): pl.pallas_call(functools.partial(dispatch_kernel, capacity=capacity, piec...  2.15 us
  transfers between devices with their start and end apart: 34, of which 7 were waited for; matrix products, arithmetic and copies ran while one was open for 1% of the time, Pallas kernels for 18%

profile of v4, /device:TPU:0, one launch (start us, length us, event | category | flops | bytes accessed | tf_op | source)
XLA Modules:
  0.0 89.4 jit_solution(13263965668433051733)
XLA Ops:
  0.6 3.1 %collective-permute-start.15 = (bf16[256,256]{1,0:T(8,128)(2,1)}, bf16[256,256]{1,0:T(8,128)(2,1)S(1)}, u32[]{:S(2)}, u32[]{:S(2)}) collective-permute-start(bf16[256,256]{1,0:T(8,128)(2,1)} %refs_0_.3), channel_id=1, source_target_pairs={{0,2},{1,3},{2,0},{3,1},{4,6},{5,7},{6,4},{7,5},{8,10},{9,11},{10,... | collective-permute-start | bytes 393224 | tf_op jit(solution)/shard_map/ppermute | solution.py:54
  3.7 2.6 %collective-permute-start.6 = (bf16[256,256]{1,0:T(8,128)(2,1)}, bf16[256,256]{1,0:T(8,128)(2,1)S(1)}, u32[]{:S(2)}, u32[]{:S(2)}) collective-permute-start(bf16[256,256]{1,0:T(8,128)(2,1)} %refs_0_.3), channel_id=1, source_target_pairs={{0,4},{1,5},{2,6},{3,7},{4,0},{5,1},{6,2},{7,3},{8,12},{9,13},{10,... | collective-permute-start | bytes 393224 | tf_op jit(solution)/shard_map/ppermute | solution.py:54
  10.1 1.8 %collective-permute-start.16 = (bf16[192,512]{1,0:T(8,128)(2,1)S(1)}, bf16[192,512]{1,0:T(8,128)(2,1)S(1)}, u32[]{:S(2)}, u32[]{:S(2)}) collective-permute-start(bf16[192,512]{1,0:T(8,128)(2,1)S(1)} %get-tuple-element.67), channel_id=1, source_target_pairs={{0,8},{8,0},{16,24},{24,16},{1,9},{9,1},{17,25},{25,17},{2,10},{10... | collective-permute-start | bytes 589832 | tf_op jit(solution)/shard_map/ppermute | solution.py:54
  11.9 1.5 %collective-permute-start.17 = (bf16[192,512]{1,0:T(8,128)(2,1)S(1)}, bf16[192,512]{1,0:T(8,128)(2,1)S(1)}, u32[]{:S(2)}, u32[]{:S(2)}) collective-permute-start(bf16[192,512]{1,0:T(8,128)(2,1)S(1)} %get-tuple-element.68), channel_id=1, source_target_pairs={{0,16},{8,24},{16,0},{24,8},{1,17},{9,25},{17,1},{25,9},{2,18},{10... | collective-permute-start | bytes 589832 | tf_op jit(solution)/shard_map/ppermute | solution.py:54
  13.7 3.2 %collective-permute-done.6.refs_0_ = bf16[256,256]{1,0:T(8,128)(2,1)S(1)} collective-permute-done((bf16[256,256]{1,0:T(8,128)(2,1)}, bf16[256,256]{1,0:T(8,128)(2,1)S(1)}, u32[]{:S(2)}, u32[]{:S(2)}) %collective-permute-start.6) | collective-permute-done | bytes 131104 | tf_op jit(solution)/shard_map/ppermute | solution.py:54
  17.9 1.6 %collective-permute-start.8 = (bf16[192,512]{1,0:T(8,128)(2,1)S(1)}, bf16[192,512]{1,0:T(8,128)(2,1)S(1)}, u32[]{:S(2)}, u32[]{:S(2)}) collective-permute-start(bf16[192,512]{1,0:T(8,128)(2,1)S(1)} %get-tuple-element.62), channel_id=1, source_target_pairs={{0,8},{8,0},{16,24},{24,16},{1,9},{9,1},{17,25},{25,17},{2,10},{10... | collective-permute-start | bytes 589832 | tf_op jit(solution)/shard_map/ppermute | solution.py:54
  19.5 1.5 %collective-permute-start.9 = (bf16[192,512]{1,0:T(8,128)(2,1)S(1)}, bf16[192,512]{1,0:T(8,128)(2,1)S(1)}, u32[]{:S(2)}, u32[]{:S(2)}) collective-permute-start(bf16[192,512]{1,0:T(8,128)(2,1)S(1)} %get-tuple-element.63), channel_id=1, source_target_pairs={{0,16},{8,24},{16,0},{24,8},{1,17},{9,25},{17,1},{25,9},{2,18},{10... | collective-permute-start | bytes 589832 | tf_op jit(solution)/shard_map/ppermute | solution.py:54
  23.7 2.1 %collective-permute-done.8.refs_1_ = bf16[192,512]{1,0:T(8,128)(2,1)S(1)} collective-permute-done((bf16[192,512]{1,0:T(8,128)(2,1)S(1)}, bf16[192,512]{1,0:T(8,128)(2,1)S(1)}, u32[]{:S(2)}, u32[]{:S(2)}) %collective-permute-start.8) | collective-permute-done | bytes 196640 | tf_op jit(solution)/shard_map/ppermute | solution.py:54
  25.8 5.0 %collective-permute-done.9.refs_2_ = bf16[192,512]{1,0:T(8,128)(2,1)S(1)} collective-permute-done((bf16[192,512]{1,0:T(8,128)(2,1)S(1)}, bf16[192,512]{1,0:T(8,128)(2,1)S(1)}, u32[]{:S(2)}, u32[]{:S(2)}) %collective-permute-start.9) | collective-permute-done | bytes 196640 | tf_op jit(solution)/shard_map/ppermute | solution.py:54
  31.8 2.2 %copy-done.1 = bf16[2,2048,512]{2,1,0:T(8,128)(2,1)S(1)} copy-done((bf16[2,2048,512]{2,1,0:T(8,128)(2,1)S(1)}, bf16[2,2048,512]{2,1,0:T(8,128)(2,1)}, u32[]{:S(2)}) %copy-start.1) | copy-done | bytes 4194328
  34.3 1.9 %copy-done.2 = bf16[2,2048,512]{2,1,0:T(8,128)(2,1)S(1)} copy-done((bf16[2,2048,512]{2,1,0:T(8,128)(2,1)S(1)}, bf16[2,2048,512]{2,1,0:T(8,128)(2,1)}, u32[]{:S(2)}) %copy-start.2) | copy-done | bytes 4194328
  36.9 2.7 %shard_map.134 = (f32[2,2,384,512]{3,2,1,0:T(8,128)S(1)}, f32[768,128]{1,0:T(8,128)S(1)}) custom-call(s32[3]{0:T(128)S(1)} %pad_add_fusion.place_ref.spot_ref, bf16[192,512]{1,0:T(8,128)(2,1)S(1)} %get-tuple-element.66.refs_0_, bf16[192,512]{1,0:T(8,128)(2,1)S(1)} %collective-permute-done.16.refs_1_, bf16[192,512]{1,0:T(8,128)(2,1)S(1)} %collective-permute-done.17.refs_2_, ...), custom_call_target="tpu_custom_call" | custom-call | flops 1610612736 | bytes 7340032 | tf_op jit(solution)/shard_map/pallas_call | solution.py:384
  39.6 3.4 %shard_map.135.hidden_ref = bf16[2,384,512]{2,1,0:T(8,128)(2,1)S(1)} custom-call(s32[3]{0:T(128)S(1)} %pad_add_fusion.place_ref.spot_ref, bf16[192,512]{1,0:T(8,128)(2,1)S(1)} %get-tuple-element.61.refs_0_, bf16[192,512]{1,0:T(8,128)(2,1)S(1)} %collective-permute-done.8.refs_1_, bf16[192,512]{1,0:T(8,128)(2,1)S(1)} %collective-permute-done.9.refs_2_, ...), custom_call_target="tpu_custom_call" | custom-call | flops 1610612736 | bytes 7340032 | tf_op jit(solution)/shard_map/pallas_call | solution.py:384
  43.0 1.5 %down.2 = (bf16[768,512]{1,0:T(8,128)(2,1)S(1)}, bf16[768,512]{1,0:T(8,128)(2,1)S(1)}) custom-call(s32[3]{0:T(128)S(1)} %pad_add_fusion.place_ref.spot_ref, bf16[2,384,512]{2,1,0:T(8,128)(2,1)S(1)} %shard_map.135.hidden_ref, bf16[2,512,2048]{2,1,0:T(8,128)(2,1)S(1)} %copy-done), custom_call_target="tpu_custom_call" | custom-call | flops 805306368 | bytes 3670016 | tf_op jit(solution)/shard_map/down/pallas_call | solution.py:422
  44.8 1.5 %down.3 = (bf16[768,512]{1,0:T(8,128)(2,1)S(1)}, bf16[768,512]{1,0:T(8,128)(2,1)S(1)}) custom-call(s32[3]{0:T(128)S(1)} %pad_add_fusion.place_ref.spot_ref, bf16[2,384,512]{2,1,0:T(8,128)(2,1)S(1)} %shard_map.135.hidden_ref, bf16[2,512,2048]{2,1,0:T(8,128)(2,1)S(1)} %copy-done), custom_call_target="tpu_custom_call" | custom-call | flops 805306368 | bytes 3670016 | tf_op jit(solution)/shard_map/down/pallas_call | solution.py:422
  53.8 5.5 %collective-permute-done.refs_1_ = bf16[1280,128]{1,0:T(8,128)(2,1)S(1)} collective-permute-done((bf16[1280,128]{1,0:T(8,128)(2,1)S(1)}, bf16[1280,128]{1,0:T(8,128)(2,1)S(1)}, u32[]{:S(2)}, u32[]{:S(2)}) %collective-permute-start) | collective-permute-done | bytes 327712 | tf_op jit(solution)/shard_map/ppermute | solution.py:54
  59.4 1.5 %collective-permute-start.30 = (bf16[192,512]{1,0:T(8,128)(2,1)S(1)}, bf16[192,512]{1,0:T(8,128)(2,1)S(1)}, u32[]{:S(2)}, u32[]{:S(2)}) collective-permute-start(bf16[192,512]{1,0:T(8,128)(2,1)S(1)} %get-tuple-element.84), channel_id=1, source_target_pairs={{0,16},{8,24},{16,0},{24,8},{1,17},{9,25},{17,1},{25,9},{2,18},{10... | collective-permute-start | bytes 589832 | tf_op jit(solution)/shard_map/ppermute | solution.py:54
  60.9 3.2 %collective-permute-done.1.refs_2_ = bf16[1280,128]{1,0:T(8,128)(2,1)S(1)} collective-permute-done((bf16[1280,128]{1,0:T(8,128)(2,1)S(1)}, bf16[1280,128]{1,0:T(8,128)(2,1)S(1)}, u32[]{:S(2)}, u32[]{:S(2)}) %collective-permute-start.1) | collective-permute-done | bytes 327712 | tf_op jit(solution)/shard_map/ppermute | solution.py:54
  64.1 4.6 %collective-permute-start.31 = (bf16[192,512]{1,0:T(8,128)(2,1)S(1)}, bf16[192,512]{1,0:T(8,128)(2,1)S(1)}, u32[]{:S(2)}, u32[]{:S(2)}) collective-permute-start(bf16[192,512]{1,0:T(8,128)(2,1)S(1)} %get-tuple-element.85), channel_id=1, source_target_pairs={{0,24},{8,16},{16,8},{24,0},{1,25},{9,17},{17,9},{25,1},{2,26},{10... | collective-permute-start | bytes 589832 | tf_op jit(solution)/shard_map/ppermute | solution.py:54
  68.8 5.2 %attention.1 = (bf16[256,128]{1,0:T(8,128)(2,1)S(1)}, bf16[256,128]{1,0:T(8,128)(2,1)S(1)}, bf16[256,128]{1,0:T(8,128)(2,1)S(1)}, bf16[256,128]{1,0:T(8,128)(2,1)S(1)}) custom-call(s32[3]{0:T(128)S(1)} %pad_add_fusion.place_ref.spot_ref, f32[2]{0:T(128)S(1)} %copy-done.7, bf16[1280,128]{1,0:T(8,128)(2,1)S(1)} %get-tuple-element.51.refs_0_, ...), custom_call_target="tpu_custom_call" | custom-call | flops 1342177280 | bytes 1310720 | tf_op jit(solution)/shard_map/attention/pallas_call | solution.py:177
  74.6 2.9 %collective-permute-start.5 = (bf16[256,128]{1,0:T(8,128)(2,1)S(1)}, bf16[256,128]{1,0:T(8,128)(2,1)S(1)}, u32[]{:S(2)}, u32[]{:S(2)}) collective-permute-start(bf16[256,128]{1,0:T(8,128)(2,1)S(1)} %get-tuple-element.58), channel_id=1, source_target_pairs={{0,24},{8,16},{16,8},{24,0},{1,25},{9,17},{17,9},{25,1},{2,26},{10... | collective-permute-start | bytes 196616 | tf_op jit(solution)/shard_map/ppermute | solution.py:54
  79.7 1.5 %collective-permute-start.33 = (bf16[256,256]{1,0:T(8,128)(2,1)S(1)}, bf16[256,256]{1,0:T(8,128)(2,1)S(1)}, u32[]{:S(2)}, u32[]{:S(2)}) collective-permute-start(bf16[256,256]{1,0:T(8,128)(2,1)S(1)} %get-tuple-element.87), channel_id=1, source_target_pairs={{0,6},{1,7},{2,4},{3,5},{4,2},{5,3},{6,0},{7,1},{8,14},{9,15},{10,... | collective-permute-start | bytes 393224 | tf_op jit(solution)/shard_map/ppermute | solution.py:54
  82.0 2.9 %collective-permute-start.27 = (bf16[192,256]{1,0:T(8,128)(2,1)S(1)}, bf16[192,256]{1,0:T(8,128)(2,1)S(1)}, u32[]{:S(2)}, u32[]{:S(2)}) collective-permute-start(bf16[192,256]{1,0:T(8,128)(2,1)S(1)} %get-tuple-element.79), channel_id=1, source_target_pairs={{0,24},{8,16},{16,8},{24,0},{1,25},{9,17},{17,9},{25,1},{2,26},{10... | collective-permute-start | bytes 294920 | tf_op jit(solution)/shard_map/ppermute | solution.py:54
  86.4 1.8 %collective-permute-done.32.refs_4_ = bf16[256,256]{1,0:T(8,128)(2,1)S(1)} collective-permute-done((bf16[256,256]{1,0:T(8,128)(2,1)S(1)}, bf16[256,256]{1,0:T(8,128)(2,1)S(1)}, u32[]{:S(2)}, u32[]{:S(2)}) %collective-permute-start.32) | collective-permute-done | bytes 131104 | tf_op jit(solution)/shard_map/ppermute | solution.py:54
  (90 shorter events, 23.6 us)
Async XLA Ops:
  0.6 8.4 %collective-permute-start.15 = (bf16[256,256]{1,0:T(8,128)(2,1)}, bf16[256,256]{1,0:T(8,128)(2,1)S(1)}, u32[]{:S(2)}, u32[]{:S(2)}) collective-permute-start(bf16[256,256]{1,0:T(8,128)(2,1)} %refs_0_.3), channel_id=1, source_target_pairs={{0,2},{1,3},{2,0},{3,1},{4,6},{5,7},{6,4},{7,5},{8,10},{9,11},{10,... | collective-permute-start | bytes 393224 | tf_op jit(solution)/shard_map/ppermute | solution.py:54
  3.7 13.1 %collective-permute-start.6 = (bf16[256,256]{1,0:T(8,128)(2,1)}, bf16[256,256]{1,0:T(8,128)(2,1)S(1)}, u32[]{:S(2)}, u32[]{:S(2)}) collective-permute-start(bf16[256,256]{1,0:T(8,128)(2,1)} %refs_0_.3), channel_id=1, source_target_pairs={{0,4},{1,5},{2,6},{3,7},{4,0},{5,1},{6,2},{7,3},{8,12},{9,13},{10,... | collective-permute-start | bytes 393224 | tf_op jit(solution)/shard_map/ppermute | solution.py:54
  6.3 10.5 %collective-permute-start.7 = (bf16[256,256]{1,0:T(8,128)(2,1)}, bf16[256,256]{1,0:T(8,128)(2,1)S(1)}, u32[]{:S(2)}, u32[]{:S(2)}) collective-permute-start(bf16[256,256]{1,0:T(8,128)(2,1)} %refs_0_.3), channel_id=1, source_target_pairs={{0,6},{1,7},{2,4},{3,5},{4,2},{5,3},{6,0},{7,1},{8,14},{9,15},{10,... | collective-permute-start | bytes 393224 | tf_op jit(solution)/shard_map/ppermute | solution.py:54
  10.1 9.4 %collective-permute-start.16 = (bf16[192,512]{1,0:T(8,128)(2,1)S(1)}, bf16[192,512]{1,0:T(8,128)(2,1)S(1)}, u32[]{:S(2)}, u32[]{:S(2)}) collective-permute-start(bf16[192,512]{1,0:T(8,128)(2,1)S(1)} %get-tuple-element.67), channel_id=1, source_target_pairs={{0,8},{8,0},{16,24},{24,16},{1,9},{9,1},{17,25},{25,17},{2,10},{10... | collective-permute-start | bytes 589832 | tf_op jit(solution)/shard_map/ppermute | solution.py:54
  11.9 9.8 %collective-permute-start.17 = (bf16[192,512]{1,0:T(8,128)(2,1)S(1)}, bf16[192,512]{1,0:T(8,128)(2,1)S(1)}, u32[]{:S(2)}, u32[]{:S(2)}) collective-permute-start(bf16[192,512]{1,0:T(8,128)(2,1)S(1)} %get-tuple-element.68), channel_id=1, source_target_pairs={{0,16},{8,24},{16,0},{24,8},{1,17},{9,25},{17,1},{25,9},{2,18},{10... | collective-permute-start | bytes 589832 | tf_op jit(solution)/shard_map/ppermute | solution.py:54
  13.4 9.8 %collective-permute-start.18 = (bf16[192,512]{1,0:T(8,128)(2,1)S(1)}, bf16[192,512]{1,0:T(8,128)(2,1)S(1)}, u32[]{:S(2)}, u32[]{:S(2)}) collective-permute-start(bf16[192,512]{1,0:T(8,128)(2,1)S(1)} %get-tuple-element.69), channel_id=1, source_target_pairs={{0,24},{8,16},{16,8},{24,0},{1,25},{9,17},{17,9},{25,1},{2,26},{10... | collective-permute-start | bytes 589832 | tf_op jit(solution)/shard_map/ppermute | solution.py:54
  19.5 11.2 %collective-permute-start.9 = (bf16[192,512]{1,0:T(8,128)(2,1)S(1)}, bf16[192,512]{1,0:T(8,128)(2,1)S(1)}, u32[]{:S(2)}, u32[]{:S(2)}) collective-permute-start(bf16[192,512]{1,0:T(8,128)(2,1)S(1)} %get-tuple-element.63), channel_id=1, source_target_pairs={{0,16},{8,24},{16,0},{24,8},{1,17},{9,25},{17,1},{25,9},{2,18},{10... | collective-permute-start | bytes 589832 | tf_op jit(solution)/shard_map/ppermute | solution.py:54
  21.7 9.0 %collective-permute-start.10 = (bf16[192,512]{1,0:T(8,128)(2,1)S(1)}, bf16[192,512]{1,0:T(8,128)(2,1)S(1)}, u32[]{:S(2)}, u32[]{:S(2)}) collective-permute-start(bf16[192,512]{1,0:T(8,128)(2,1)S(1)} %get-tuple-element.64), channel_id=1, source_target_pairs={{0,24},{8,16},{16,8},{24,0},{1,25},{9,17},{17,9},{25,1},{2,26},{10... | collective-permute-start | bytes 589832 | tf_op jit(solution)/shard_map/ppermute | solution.py:54
  23.2 8.1 %collective-permute-start.20 = (bf16[192,512]{1,0:T(8,128)(2,1)S(1)}, bf16[192,512]{1,0:T(8,128)(2,1)S(1)}, u32[]{:S(2)}, u32[]{:S(2)}) collective-permute-start(bf16[192,512]{1,0:T(8,128)(2,1)S(1)} %collective-permute-done.16.refs_1_), channel_id=1, source_target_pairs={{0,1},{1,0},{2,3},{3,2},{4,5},{5,4},{6,7},{7,6},{8,9},{9,8},{10,11... | collective-permute-start | bytes 589832 | tf_op jit(solution)/shard_map/ppermute | solution.py:54
  23.2 8.2 %collective-permute-start.21 = (bf16[192,512]{1,0:T(8,128)(2,1)S(1)}, bf16[192,512]{1,0:T(8,128)(2,1)S(1)}, u32[]{:S(2)}, u32[]{:S(2)}) collective-permute-start(bf16[192,512]{1,0:T(8,128)(2,1)S(1)} %collective-permute-done.17.refs_2_), channel_id=1, source_target_pairs={{0,1},{1,0},{2,3},{3,2},{4,5},{5,4},{6,7},{7,6},{8,9},{9,8},{10,11... | collective-permute-start | bytes 589832 | tf_op jit(solution)/shard_map/ppermute | solution.py:54
  25.8 10.7 %collective-permute-start.22 = (bf16[192,512]{1,0:T(8,128)(2,1)S(1)}, bf16[192,512]{1,0:T(8,128)(2,1)S(1)}, u32[]{:S(2)}, u32[]{:S(2)}) collective-permute-start(bf16[192,512]{1,0:T(8,128)(2,1)S(1)} %collective-permute-done.18.refs_3_), channel_id=1, source_target_pairs={{0,1},{1,0},{2,3},{3,2},{4,5},{5,4},{6,7},{7,6},{8,9},{9,8},{10,11... | collective-permute-start | bytes 589832 | tf_op jit(solution)/shard_map/ppermute | solution.py:54
  30.7 8.8 %collective-permute-start.11 = (bf16[192,512]{1,0:T(8,128)(2,1)S(1)}, bf16[192,512]{1,0:T(8,128)(2,1)S(1)}, u32[]{:S(2)}, u32[]{:S(2)}) collective-permute-start(bf16[192,512]{1,0:T(8,128)(2,1)S(1)} %get-tuple-element.61.refs_0_), channel_id=1, source_target_pairs={{0,1},{1,0},{2,3},{3,2},{4,5},{5,4},{6,7},{7,6},{8,9},{9,8},{10,11... | collective-permute-start | bytes 589832 | tf_op jit(solution)/shard_map/ppermute | solution.py:54
  30.8 8.8 %collective-permute-start.12 = (bf16[192,512]{1,0:T(8,128)(2,1)S(1)}, bf16[192,512]{1,0:T(8,128)(2,1)S(1)}, u32[]{:S(2)}, u32[]{:S(2)}) collective-permute-start(bf16[192,512]{1,0:T(8,128)(2,1)S(1)} %collective-permute-done.8.refs_1_), channel_id=1, source_target_pairs={{0,1},{1,0},{2,3},{3,2},{4,5},{5,4},{6,7},{7,6},{8,9},{9,8},{10,11... | collective-permute-start | bytes 589832 | tf_op jit(solution)/shard_map/ppermute | solution.py:54
  31.3 8.3 %collective-permute-start.13 = (bf16[192,512]{1,0:T(8,128)(2,1)S(1)}, bf16[192,512]{1,0:T(8,128)(2,1)S(1)}, u32[]{:S(2)}, u32[]{:S(2)}) collective-permute-start(bf16[192,512]{1,0:T(8,128)(2,1)S(1)} %collective-permute-done.9.refs_2_), channel_id=1, source_target_pairs={{0,1},{1,0},{2,3},{3,2},{4,5},{5,4},{6,7},{7,6},{8,9},{9,8},{10,11... | collective-permute-start | bytes 589832 | tf_op jit(solution)/shard_map/ppermute | solution.py:54
  31.3 8.2 %collective-permute-start.14 = (bf16[192,512]{1,0:T(8,128)(2,1)S(1)}, bf16[192,512]{1,0:T(8,128)(2,1)S(1)}, u32[]{:S(2)}, u32[]{:S(2)}) collective-permute-start(bf16[192,512]{1,0:T(8,128)(2,1)S(1)} %collective-permute-done.10.refs_3_), channel_id=1, source_target_pairs={{0,1},{1,0},{2,3},{3,2},{4,5},{5,4},{6,7},{7,6},{8,9},{9,8},{10,11... | collective-permute-start | bytes 589832 | tf_op jit(solution)/shard_map/ppermute | solution.py:54
  48.7 10.6 %collective-permute-start = (bf16[1280,128]{1,0:T(8,128)(2,1)S(1)}, bf16[1280,128]{1,0:T(8,128)(2,1)S(1)}, u32[]{:S(2)}, u32[]{:S(2)}) collective-permute-start(bf16[1280,128]{1,0:T(8,128)(2,1)S(1)} %get-tuple-element.52), channel_id=1, source_target_pairs={{0,8},{8,0},{16,24},{24,16},{1,9},{9,1},{17,25},{25,17},{2,10},{10... | collective-permute-start | bytes 983048 | tf_op jit(solution)/shard_map/ppermute | solution.py:54
  49.6 14.5 %collective-permute-start.1 = (bf16[1280,128]{1,0:T(8,128)(2,1)S(1)}, bf16[1280,128]{1,0:T(8,128)(2,1)S(1)}, u32[]{:S(2)}, u32[]{:S(2)}) collective-permute-start(bf16[1280,128]{1,0:T(8,128)(2,1)S(1)} %get-tuple-element.53), channel_id=1, source_target_pairs={{0,16},{8,24},{16,0},{24,8},{1,17},{9,25},{17,1},{25,9},{2,18},{10... | collective-permute-start | bytes 983048 | tf_op jit(solution)/shard_map/ppermute | solution.py:54
  50.8 17.9 %collective-permute-start.2 = (bf16[1280,128]{1,0:T(8,128)(2,1)S(1)}, bf16[1280,128]{1,0:T(8,128)(2,1)S(1)}, u32[]{:S(2)}, u32[]{:S(2)}) collective-permute-start(bf16[1280,128]{1,0:T(8,128)(2,1)S(1)} %get-tuple-element.54), channel_id=1, source_target_pairs={{0,24},{8,16},{16,8},{24,0},{1,25},{9,17},{17,9},{25,1},{2,26},{10... | collective-permute-start | bytes 983048 | tf_op jit(solution)/shard_map/ppermute | solution.py:54
  52.5 27.3 %collective-permute-start.24 = (bf16[768,256]{1,0:T(8,128)(2,1)S(1)}, bf16[768,256]{1,0:T(8,128)(2,1)S(1)}, u32[]{:S(2)}, u32[]{:S(2)}) collective-permute-start(bf16[768,256]{1,0:T(8,128)(2,1)S(1)} %get-tuple-element.75), channel_id=1, source_target_pairs={{0,2},{1,3},{2,0},{3,1},{4,6},{5,7},{6,4},{7,5},{8,10},{9,11},{10,... | collective-permute-start | bytes 1179656 | tf_op jit(solution)/shard_map/ppermute | solution.py:54
  53.2 20.9 %collective-permute-start.29 = (bf16[192,512]{1,0:T(8,128)(2,1)S(1)}, bf16[192,512]{1,0:T(8,128)(2,1)S(1)}, u32[]{:S(2)}, u32[]{:S(2)}) collective-permute-start(bf16[192,512]{1,0:T(8,128)(2,1)S(1)} %get-tuple-element.83), channel_id=1, source_target_pairs={{0,8},{8,0},{16,24},{24,16},{1,9},{9,1},{17,25},{25,17},{2,10},{10... | collective-permute-start | bytes 589832 | tf_op jit(solution)/shard_map/ppermute | solution.py:54
  59.4 15.2 %collective-permute-start.30 = (bf16[192,512]{1,0:T(8,128)(2,1)S(1)}, bf16[192,512]{1,0:T(8,128)(2,1)S(1)}, u32[]{:S(2)}, u32[]{:S(2)}) collective-permute-start(bf16[192,512]{1,0:T(8,128)(2,1)S(1)} %get-tuple-element.84), channel_id=1, source_target_pairs={{0,16},{8,24},{16,0},{24,8},{1,17},{9,25},{17,1},{25,9},{2,18},{10... | collective-permute-start | bytes 589832 | tf_op jit(solution)/shard_map/ppermute | solution.py:54
  64.1 13.4 %collective-permute-start.31 = (bf16[192,512]{1,0:T(8,128)(2,1)S(1)}, bf16[192,512]{1,0:T(8,128)(2,1)S(1)}, u32[]{:S(2)}, u32[]{:S(2)}) collective-permute-start(bf16[192,512]{1,0:T(8,128)(2,1)S(1)} %get-tuple-element.85), channel_id=1, source_target_pairs={{0,24},{8,16},{16,8},{24,0},{1,25},{9,17},{17,9},{25,1},{2,26},{10... | collective-permute-start | bytes 589832 | tf_op jit(solution)/shard_map/ppermute | solution.py:54
  78.2 10.0 %collective-permute-start.32 = (bf16[256,256]{1,0:T(8,128)(2,1)S(1)}, bf16[256,256]{1,0:T(8,128)(2,1)S(1)}, u32[]{:S(2)}, u32[]{:S(2)}) collective-permute-start(bf16[256,256]{1,0:T(8,128)(2,1)S(1)} %get-tuple-element.86), channel_id=1, source_target_pairs={{0,4},{1,5},{2,6},{3,7},{4,0},{5,1},{6,2},{7,3},{8,12},{9,13},{10,... | collective-permute-start | bytes 393224 | tf_op jit(solution)/shard_map/ppermute | solution.py:54
  79.7 8.5 %collective-permute-start.33 = (bf16[256,256]{1,0:T(8,128)(2,1)S(1)}, bf16[256,256]{1,0:T(8,128)(2,1)S(1)}, u32[]{:S(2)}, u32[]{:S(2)}) collective-permute-start(bf16[256,256]{1,0:T(8,128)(2,1)S(1)} %get-tuple-element.87), channel_id=1, source_target_pairs={{0,6},{1,7},{2,4},{3,5},{4,2},{5,3},{6,0},{7,1},{8,14},{9,15},{10,... | collective-permute-start | bytes 393224 | tf_op jit(solution)/shard_map/ppermute | solution.py:54
  (22 other events, 144.6 us)

commit v5 on v4

--- a/solution.py
+++ b/solution.py
@@ -16,7 +16,8 @@
 OUT_SCALE = 0.8
 LOG2E = 1.4426950408889634
 CORES = 2
-FETCH_GRANT = 44
+GATE_GRANT = 46
+UP_GRANT = 44
 SPLITS = 2
 BF16 = jnp.bfloat16
 F32 = jnp.float32
@@ -104,7 +105,7 @@
 def attention_kernel(place_ref, mix_ref, *refs, groups, rows, heads, scale):
     bundle_refs, gain_ref = refs[:groups], refs[groups]
     out_refs = refs[groups + 1 : 2 * groups + 1]
-    bundle, outputs, scores, arrivals = refs[2 * groups + 1 :]
+    bundle, outputs, scores, turned, arrivals = refs[2 * groups + 1 :]
     place = place_ref[0]
     copies = []
     for mask in range(groups):
@@ -123,10 +124,11 @@
     lane = lax.broadcasted_iota(jnp.int32, (share, width), 1)
     row = lax.broadcasted_iota(jnp.int32, (share, rows), 0)
     column = lax.broadcasted_iota(jnp.int32, (share, rows), 1)
-    contract = (((1,), (1,)), ((), ()))
     factor = scale * LOG2E
     for copy in copies:
         copy.wait()
+    for block in range(groups):
+        turned[block] = bundle[block, :rows, :].T
     tops = [None, None]
     for block in range(groups):
         visible = column <= row + (part if block % 2 == 0 else splits - 1 - part) * share
@@ -136,9 +138,7 @@
             query = jnp.where((lane < half) if side == 0 else (lane >= half), queries, empty)
             top = jnp.full((share, width), NEG_FILL, F32)
             for other in range(block + 1):
-                score = lax.dot_general(
-                    query, bundle[other, :rows, :], contract, preferred_element_type=F32
-                )
+                score = jnp.dot(query, turned[other], preferred_element_type=F32)
                 if other == block:
                     score = jnp.where(visible, score, NEG_FILL)
                 scores[side, :, other * rows : (other + 1) * rows] = score
@@ -185,6 +185,7 @@
             pltpu.VMEM((groups, tall, width), BF16),
             pltpu.VMEM((groups, share, width), BF16),
             pltpu.VMEM((2, share, groups * rows), F32),
+            pltpu.VMEM((groups, width, rows), BF16),
             pltpu.SemaphoreType.DMA((groups,)),
         ],
         cost_estimate=cost(pairs * 4 * width, 2 * groups * tall * width, pairs),
@@ -324,7 +325,7 @@
     first = lax.div(spot_ref[1], span)
     base = pl.multiple_of((first if chunk == 0 else jnp.bitwise_xor(first, chunk)) * depth, depth)
     if last:
-        sums_ref, squares_ref, hidden_ref, normed = rest
+        sums_ref, squares_ref, down_ref, hidden_ref, sent_ref, kept_ref, normed = rest
     else:
         sums_ref, squares_ref, normed = rest
     factors = [[None] * groups for _ in range(pieces)]
@@ -373,6 +374,11 @@
                 hidden_ref[piece, :, columns] = (
                     (up + 1.0) * gate * jax.nn.sigmoid(GLU_ALPHA * gate)
                 ).astype(BF16)
+    if last:
+        down_kernel(
+            spot_ref, hidden_ref, down_ref, sent_ref, kept_ref,
+            groups=groups, capacity=capacity, width=width, first=span,
+        )
 
 
 def hidden_units(spot, tables, prior, gain, gate, up, groups, capacity, width, chunk):
@@ -380,19 +386,20 @@
     rows, depth = groups * capacity, CORES * tables[0].shape[1]
     last = prior is not None
     sums = [shape_of(2, pieces, rows, ff, dtype=F32), shape_of(pieces * rows, 128, dtype=F32)]
+    outs = [shape_of(pieces, rows, ff)] + [shape_of(pieces * rows, depth // CORES)] * 2
     inputs = list(tables) + [gain[None, :], gate, up] + (list(prior) if last else [])
     return pl.pallas_call(
         functools.partial(
             hidden_kernel, groups=groups, capacity=capacity, width=width, chunk=chunk, last=last
         ),
-        out_shape=shape_of(pieces, rows, ff) if last else sums,
+        out_shape=outs if last else sums,
         in_specs=[scalars()] + [whole()] * len(inputs),
-        out_specs=whole() if last else [whole()] * 2,
+        out_specs=[whole()] * len(outs if last else sums),
         scratch_shapes=[pltpu.VMEM((pieces, rows, depth), BF16)],
         cost_estimate=cost(
             4 * pieces * rows * depth * ff, 4 * pieces * depth * (ff + rows), pieces * rows * ff
         ),
-        compiler_params=grant(14),
+        compiler_params=grant(16),
     )(spot, *inputs)
 
 
@@ -627,7 +634,7 @@
     by_level = [tokens]
     for mask in range(1, levels):
         by_level.append(levels_flip(tokens, mask))
-    (gate_near,) = fetch(gate_weight, mebibytes=FETCH_GRANT)
+    (gate_near,) = fetch(gate_weight, mebibytes=GATE_GRANT)
     by_level[0], picked, picked_weights = fetch(tokens, routes.T, route_weights.T, mebibytes=2)
     chosen, scale = plan(
         place, picked, picked_weights, capacity, pieces, experts, groups
@@ -645,19 +652,19 @@
         for table in own[chunk]:
             swapped.append(cores_flip(table))
         other.append(swapped)
-    (up_near,) = fetch(up_weight, mebibytes=FETCH_GRANT)
+    (up_near,) = fetch(up_weight, mebibytes=UP_GRANT)
     hidden = None
     for chunk in range(2):
+        if chunk == 1:
+            hidden = list(hidden) + [down_weight]
         hidden = hidden_units(
             spot, own[chunk] + other[chunk], hidden, expert_gain, gate_near, up_near,
             groups, capacity, width, chunk,
         )
-    halves = []
-    for first in (0, half):
-        sent, kept = down(
-            spot, hidden, down_weight, groups, capacity, width, first, half
-        )
-        halves.append((kept, cores_flip(sent)))
+    hidden, sent, kept = hidden
+    halves = [(kept, cores_flip(sent))]
+    sent, kept = down(spot, hidden, down_weight, groups, capacity, width, 0, half)
+    halves.insert(0, (kept, cores_flip(sent)))
     values = list(part_levels(*halves[0], half))
     for level in range(1, half):
         values[level] = levels_flip(values[level], level)

time: 89.7 us -> 86.7 us (0.967)
  local copies, waits for them, and re-layouts: 7.85 us -> 3.8 us
  Pallas kernels: 21.9 us -> 23.1 us
    unnamed x25 -> x23, local copies, waits for them, and re-layouts: 7.74 us -> 3.69 us
    pallas_call x3, Pallas kernels: 0.89 us -> 3.01 us  [fetch(): pl.pallas_call(fetch_kernel, out_shape=[shape_of(*array.shape, dtype=arra...]
    pallas_call x2 -> x1, Pallas kernels: 3.08 us -> 1.54 us  [down(): pl.pallas_call(functools.partial(down_kernel, groups=groups, capacity=cap...]
  transfers between devices with their start and end apart: 34 -> 34, of which waited for: 7 -> 7; matrix products, arithmetic and copies ran while one was open for 1% -> 1% of each run, Pallas kernels for 18% -> 19%
where the time goes in v5:
time: 86.7 us; the launch traced here: 86.4 us
  starting transfers between devices  36.9 us (43%)
  Pallas kernels  23.1 us (27%)
  waiting for transfers between devices  21.6 us (25%)
  local copies, waits for them, and re-layouts  3.8 us (4%)
  between operations  0.97 us (1%)
    ppermute x34, starting transfers between devices, flip(): return lax.ppermute(value, axis, pairs)  36.9 us
    ppermute x34, waiting for transfers between devices, flip(): return lax.ppermute(value, axis, pairs)  21.6 us
    pallas_call x2, Pallas kernels, hidden_units(): pl.pallas_call(functools.partial(hidden_kernel, groups=groups, capacity=c...  6.74 us
    pallas_call x1, Pallas kernels, attention(): pl.pallas_call(functools.partial(attention_kernel, groups=groups, rows=ro...  5.18 us
    unnamed x23, local copies, waits for them, and re-layouts  3.69 us
    pallas_call x3, Pallas kernels, fetch(): pl.pallas_call(fetch_kernel, out_shape=[shape_of(*array.shape, dtype=arra...  3.01 us
    pallas_call x2, Pallas kernels, dispatch(): pl.pallas_call(functools.partial(dispatch_kernel, capacity=capacity, piec...  2.16 us
  transfers between devices with their start and end apart: 34, of which 7 were waited for; matrix products, arithmetic and copies ran while one was open for 1% of the time, Pallas kernels for 19%

profile of v5, /device:TPU:0, one launch (start us, length us, event | category | flops | bytes accessed | tf_op | source)
XLA Modules:
  0.0 86.4 jit_solution(17247008050646949192)
XLA Ops:
  0.6 3.1 %collective-permute-start.15 = (bf16[256,256]{1,0:T(8,128)(2,1)}, bf16[256,256]{1,0:T(8,128)(2,1)S(1)}, u32[]{:S(2)}, u32[]{:S(2)}) collective-permute-start(bf16[256,256]{1,0:T(8,128)(2,1)} %refs_0_.3), channel_id=1, source_target_pairs={{0,2},{1,3},{2,0},{3,1},{4,6},{5,7},{6,4},{7,5},{8,10},{9,11},{10,... | collective-permute-start | bytes 393224 | tf_op jit(solution)/shard_map/ppermute | solution.py:55
  3.7 2.6 %collective-permute-start.6 = (bf16[256,256]{1,0:T(8,128)(2,1)}, bf16[256,256]{1,0:T(8,128)(2,1)S(1)}, u32[]{:S(2)}, u32[]{:S(2)}) collective-permute-start(bf16[256,256]{1,0:T(8,128)(2,1)} %refs_0_.3), channel_id=1, source_target_pairs={{0,4},{1,5},{2,6},{3,7},{4,0},{5,1},{6,2},{7,3},{8,12},{9,13},{10,... | collective-permute-start | bytes 393224 | tf_op jit(solution)/shard_map/ppermute | solution.py:55
  10.1 1.8 %collective-permute-start.16 = (bf16[192,512]{1,0:T(8,128)(2,1)S(1)}, bf16[192,512]{1,0:T(8,128)(2,1)S(1)}, u32[]{:S(2)}, u32[]{:S(2)}) collective-permute-start(bf16[192,512]{1,0:T(8,128)(2,1)S(1)} %get-tuple-element.68), channel_id=1, source_target_pairs={{0,8},{8,0},{16,24},{24,16},{1,9},{9,1},{17,25},{25,17},{2,10},{10... | collective-permute-start | bytes 589832 | tf_op jit(solution)/shard_map/ppermute | solution.py:55
  11.9 1.5 %collective-permute-start.17 = (bf16[192,512]{1,0:T(8,128)(2,1)S(1)}, bf16[192,512]{1,0:T(8,128)(2,1)S(1)}, u32[]{:S(2)}, u32[]{:S(2)}) collective-permute-start(bf16[192,512]{1,0:T(8,128)(2,1)S(1)} %get-tuple-element.69), channel_id=1, source_target_pairs={{0,16},{8,24},{16,0},{24,8},{1,17},{9,25},{17,1},{25,9},{2,18},{10... | collective-permute-start | bytes 589832 | tf_op jit(solution)/shard_map/ppermute | solution.py:55
  13.7 3.2 %collective-permute-done.6.refs_0_ = bf16[256,256]{1,0:T(8,128)(2,1)S(1)} collective-permute-done((bf16[256,256]{1,0:T(8,128)(2,1)}, bf16[256,256]{1,0:T(8,128)(2,1)S(1)}, u32[]{:S(2)}, u32[]{:S(2)}) %collective-permute-start.6) | collective-permute-done | bytes 131104 | tf_op jit(solution)/shard_map/ppermute | solution.py:55
  17.9 1.6 %collective-permute-start.8 = (bf16[192,512]{1,0:T(8,128)(2,1)S(1)}, bf16[192,512]{1,0:T(8,128)(2,1)S(1)}, u32[]{:S(2)}, u32[]{:S(2)}) collective-permute-start(bf16[192,512]{1,0:T(8,128)(2,1)S(1)} %get-tuple-element.63), channel_id=1, source_target_pairs={{0,8},{8,0},{16,24},{24,16},{1,9},{9,1},{17,25},{25,17},{2,10},{10... | collective-permute-start | bytes 589832 | tf_op jit(solution)/shard_map/ppermute | solution.py:55
  19.5 1.5 %collective-permute-start.9 = (bf16[192,512]{1,0:T(8,128)(2,1)S(1)}, bf16[192,512]{1,0:T(8,128)(2,1)S(1)}, u32[]{:S(2)}, u32[]{:S(2)}) collective-permute-start(bf16[192,512]{1,0:T(8,128)(2,1)S(1)} %get-tuple-element.64), channel_id=1, source_target_pairs={{0,16},{8,24},{16,0},{24,8},{1,17},{9,25},{17,1},{25,9},{2,18},{10... | collective-permute-start | bytes 589832 | tf_op jit(solution)/shard_map/ppermute | solution.py:55
  23.7 2.1 %collective-permute-done.8.refs_1_ = bf16[192,512]{1,0:T(8,128)(2,1)S(1)} collective-permute-done((bf16[192,512]{1,0:T(8,128)(2,1)S(1)}, bf16[192,512]{1,0:T(8,128)(2,1)S(1)}, u32[]{:S(2)}, u32[]{:S(2)}) %collective-permute-start.8) | collective-permute-done | bytes 196640 | tf_op jit(solution)/shard_map/ppermute | solution.py:55
  25.8 5.0 %collective-permute-done.9.refs_2_ = bf16[192,512]{1,0:T(8,128)(2,1)S(1)} collective-permute-done((bf16[192,512]{1,0:T(8,128)(2,1)S(1)}, bf16[192,512]{1,0:T(8,128)(2,1)S(1)}, u32[]{:S(2)}, u32[]{:S(2)}) %collective-permute-start.9) | collective-permute-done | bytes 196640 | tf_op jit(solution)/shard_map/ppermute | solution.py:55
  31.8 2.4 %shard_map.132.refs_9_ = bf16[2,2048,512]{2,1,0:T(8,128)(2,1)S(1)} custom-call(bf16[2,2048,512]{2,1,0:T(8,128)(2,1)} %refs_0_.4), custom_call_target="tpu_custom_call" | custom-call | flops 1048576 | bytes 8388608 | tf_op jit(solution)/shard_map/pallas_call | solution.py:305
  34.9 2.7 %shard_map.134 = (f32[2,2,384,512]{3,2,1,0:T(8,128)S(1)}, f32[768,128]{1,0:T(8,128)S(1)}) custom-call(s32[3]{0:T(128)S(1)} %pad_add_fusion.place_ref.spot_ref, bf16[192,512]{1,0:T(8,128)(2,1)S(1)} %get-tuple-element.67.refs_0_, bf16[192,512]{1,0:T(8,128)(2,1)S(1)} %collective-permute-done.16.refs_1_, bf16[192,512]{1,0:T(8,128)(2,1)S(1)} %collective-permute-done.17.refs_2_, ...), custom_call_target="tpu_custom_call" | custom-call | flops 1610612736 | bytes 7340032 | tf_op jit(solution)/shard_map/pallas_call | solution.py:391
  37.7 4.0 %shard_map.135 = (bf16[2,384,512]{2,1,0:T(8,128)(2,1)S(1)}, bf16[768,512]{1,0:T(8,128)(2,1)S(1)}, bf16[768,512]{1,0:T(8,128)(2,1)S(1)}) custom-call(s32[3]{0:T(128)S(1)} %pad_add_fusion.place_ref.spot_ref, bf16[192,512]{1,0:T(8,128)(2,1)S(1)} %get-tuple-element.62.refs_0_, bf16[192,512]{1,0:T(8,128)(2,1)S(1)} %collective-permute-done.8.refs_1_, ...), custom_call_target="tpu_custom_call" | custom-call | flops 1610612736 | bytes 7340032 | tf_op jit(solution)/shard_map/pallas_call | solution.py:391
  41.8 1.5 %down.1 = (bf16[768,512]{1,0:T(8,128)(2,1)S(1)}, bf16[768,512]{1,0:T(8,128)(2,1)S(1)}) custom-call(s32[3]{0:T(128)S(1)} %pad_add_fusion.place_ref.spot_ref, bf16[2,384,512]{2,1,0:T(8,128)(2,1)S(1)} %get-tuple-element.73.hidden_ref, bf16[2,512,2048]{2,1,0:T(8,128)(2,1)S(1)} %copy-done), custom_call_target="tpu_custom_call" | custom-call | flops 805306368 | bytes 3670016 | tf_op jit(solution)/shard_map/down/pallas_call | solution.py:429
  46.5 1.4 %collective-permute-start.1 = (bf16[1280,128]{1,0:T(8,128)(2,1)S(1)}, bf16[1280,128]{1,0:T(8,128)(2,1)S(1)}, u32[]{:S(2)}, u32[]{:S(2)}) collective-permute-start(bf16[1280,128]{1,0:T(8,128)(2,1)S(1)} %get-tuple-element.54), channel_id=1, source_target_pairs={{0,16},{8,24},{16,0},{24,8},{1,17},{9,25},{17,1},{25,9},{2,18},{10... | collective-permute-start | bytes 983048 | tf_op jit(solution)/shard_map/ppermute | solution.py:55
  50.8 5.7 %collective-permute-done.refs_1_ = bf16[1280,128]{1,0:T(8,128)(2,1)S(1)} collective-permute-done((bf16[1280,128]{1,0:T(8,128)(2,1)S(1)}, bf16[1280,128]{1,0:T(8,128)(2,1)S(1)}, u32[]{:S(2)}, u32[]{:S(2)}) %collective-permute-start) | collective-permute-done | bytes 327712 | tf_op jit(solution)/shard_map/ppermute | solution.py:55
  56.5 1.5 %collective-permute-start.30 = (bf16[192,512]{1,0:T(8,128)(2,1)S(1)}, bf16[192,512]{1,0:T(8,128)(2,1)S(1)}, u32[]{:S(2)}, u32[]{:S(2)}) collective-permute-start(bf16[192,512]{1,0:T(8,128)(2,1)S(1)} %get-tuple-element.86), channel_id=1, source_target_pairs={{0,16},{8,24},{16,0},{24,8},{1,17},{9,25},{17,1},{25,9},{2,18},{10... | collective-permute-start | bytes 589832 | tf_op jit(solution)/shard_map/ppermute | solution.py:55
  58.0 3.2 %collective-permute-done.1.refs_2_ = bf16[1280,128]{1,0:T(8,128)(2,1)S(1)} collective-permute-done((bf16[1280,128]{1,0:T(8,128)(2,1)S(1)}, bf16[1280,128]{1,0:T(8,128)(2,1)S(1)}, u32[]{:S(2)}, u32[]{:S(2)}) %collective-permute-start.1) | collective-permute-done | bytes 327712 | tf_op jit(solution)/shard_map/ppermute | solution.py:55
  61.2 4.8 %collective-permute-start.31 = (bf16[192,512]{1,0:T(8,128)(2,1)S(1)}, bf16[192,512]{1,0:T(8,128)(2,1)S(1)}, u32[]{:S(2)}, u32[]{:S(2)}) collective-permute-start(bf16[192,512]{1,0:T(8,128)(2,1)S(1)} %get-tuple-element.87), channel_id=1, source_target_pairs={{0,24},{8,16},{16,8},{24,0},{1,25},{9,17},{17,9},{25,1},{2,26},{10... | collective-permute-start | bytes 589832 | tf_op jit(solution)/shard_map/ppermute | solution.py:55
  66.0 5.2 %attention.1 = (bf16[256,128]{1,0:T(8,128)(2,1)S(1)}, bf16[256,128]{1,0:T(8,128)(2,1)S(1)}, bf16[256,128]{1,0:T(8,128)(2,1)S(1)}, bf16[256,128]{1,0:T(8,128)(2,1)S(1)}) custom-call(s32[3]{0:T(128)S(1)} %pad_add_fusion.place_ref.spot_ref, f32[2]{0:T(128)S(1)} %copy-done.6, bf16[1280,128]{1,0:T(8,128)(2,1)S(1)} %get-tuple-element.52.refs_0_, ...), custom_call_target="tpu_custom_call" | custom-call | flops 1342177280 | bytes 1310720 | tf_op jit(solution)/shard_map/attention/pallas_call | solution.py:177
  71.9 2.9 %collective-permute-start.5 = (bf16[256,128]{1,0:T(8,128)(2,1)S(1)}, bf16[256,128]{1,0:T(8,128)(2,1)S(1)}, u32[]{:S(2)}, u32[]{:S(2)}) collective-permute-start(bf16[256,128]{1,0:T(8,128)(2,1)S(1)} %get-tuple-element.59), channel_id=1, source_target_pairs={{0,24},{8,16},{16,8},{24,0},{1,25},{9,17},{17,9},{25,1},{2,26},{10... | collective-permute-start | bytes 196616 | tf_op jit(solution)/shard_map/ppermute | solution.py:55
  75.5 1.5 %collective-permute-start.32 = (bf16[256,256]{1,0:T(8,128)(2,1)S(1)}, bf16[256,256]{1,0:T(8,128)(2,1)S(1)}, u32[]{:S(2)}, u32[]{:S(2)}) collective-permute-start(bf16[256,256]{1,0:T(8,128)(2,1)S(1)} %get-tuple-element.88), channel_id=1, source_target_pairs={{0,4},{1,5},{2,6},{3,7},{4,0},{5,1},{6,2},{7,3},{8,12},{9,13},{10,... | collective-permute-start | bytes 393224 | tf_op jit(solution)/shard_map/ppermute | solution.py:55
  77.0 1.5 %collective-permute-start.33 = (bf16[256,256]{1,0:T(8,128)(2,1)S(1)}, bf16[256,256]{1,0:T(8,128)(2,1)S(1)}, u32[]{:S(2)}, u32[]{:S(2)}) collective-permute-start(bf16[256,256]{1,0:T(8,128)(2,1)S(1)} %get-tuple-element.89), channel_id=1, source_target_pairs={{0,6},{1,7},{2,4},{3,5},{4,2},{5,3},{6,0},{7,1},{8,14},{9,15},{10,... | collective-permute-start | bytes 393224 | tf_op jit(solution)/shard_map/ppermute | solution.py:55
  79.2 2.9 %collective-permute-start.27 = (bf16[192,256]{1,0:T(8,128)(2,1)S(1)}, bf16[192,256]{1,0:T(8,128)(2,1)S(1)}, u32[]{:S(2)}, u32[]{:S(2)}) collective-permute-start(bf16[192,256]{1,0:T(8,128)(2,1)S(1)} %get-tuple-element.81), channel_id=1, source_target_pairs={{0,24},{8,16},{16,8},{24,0},{1,25},{9,17},{17,9},{25,1},{2,26},{10... | collective-permute-start | bytes 294920 | tf_op jit(solution)/shard_map/ppermute | solution.py:55
  83.7 1.6 %collective-permute-done.32.refs_4_ = bf16[256,256]{1,0:T(8,128)(2,1)S(1)} collective-permute-done((bf16[256,256]{1,0:T(8,128)(2,1)S(1)}, bf16[256,256]{1,0:T(8,128)(2,1)S(1)}, u32[]{:S(2)}, u32[]{:S(2)}) %collective-permute-start.32) | collective-permute-done | bytes 131104 | tf_op jit(solution)/shard_map/ppermute | solution.py:55
  (87 shorter events, 20.1 us)
Async XLA Ops:
  0.6 8.4 %collective-permute-start.15 = (bf16[256,256]{1,0:T(8,128)(2,1)}, bf16[256,256]{1,0:T(8,128)(2,1)S(1)}, u32[]{:S(2)}, u32[]{:S(2)}) collective-permute-start(bf16[256,256]{1,0:T(8,128)(2,1)} %refs_0_.3), channel_id=1, source_target_pairs={{0,2},{1,3},{2,0},{3,1},{4,6},{5,7},{6,4},{7,5},{8,10},{9,11},{10,... | collective-permute-start | bytes 393224 | tf_op jit(solution)/shard_map/ppermute | solution.py:55
  3.7 13.1 %collective-permute-start.6 = (bf16[256,256]{1,0:T(8,128)(2,1)}, bf16[256,256]{1,0:T(8,128)(2,1)S(1)}, u32[]{:S(2)}, u32[]{:S(2)}) collective-permute-start(bf16[256,256]{1,0:T(8,128)(2,1)} %refs_0_.3), channel_id=1, source_target_pairs={{0,4},{1,5},{2,6},{3,7},{4,0},{5,1},{6,2},{7,3},{8,12},{9,13},{10,... | collective-permute-start | bytes 393224 | tf_op jit(solution)/shard_map/ppermute | solution.py:55
  6.3 10.5 %collective-permute-start.7 = (bf16[256,256]{1,0:T(8,128)(2,1)}, bf16[256,256]{1,0:T(8,128)(2,1)S(1)}, u32[]{:S(2)}, u32[]{:S(2)}) collective-permute-start(bf16[256,256]{1,0:T(8,128)(2,1)} %refs_0_.3), channel_id=1, source_target_pairs={{0,6},{1,7},{2,4},{3,5},{4,2},{5,3},{6,0},{7,1},{8,14},{9,15},{10,... | collective-permute-start | bytes 393224 | tf_op jit(solution)/shard_map/ppermute | solution.py:55
  10.1 9.4 %collective-permute-start.16 = (bf16[192,512]{1,0:T(8,128)(2,1)S(1)}, bf16[192,512]{1,0:T(8,128)(2,1)S(1)}, u32[]{:S(2)}, u32[]{:S(2)}) collective-permute-start(bf16[192,512]{1,0:T(8,128)(2,1)S(1)} %get-tuple-element.68), channel_id=1, source_target_pairs={{0,8},{8,0},{16,24},{24,16},{1,9},{9,1},{17,25},{25,17},{2,10},{10... | collective-permute-start | bytes 589832 | tf_op jit(solution)/shard_map/ppermute | solution.py:55
  11.9 9.8 %collective-permute-start.17 = (bf16[192,512]{1,0:T(8,128)(2,1)S(1)}, bf16[192,512]{1,0:T(8,128)(2,1)S(1)}, u32[]{:S(2)}, u32[]{:S(2)}) collective-permute-start(bf16[192,512]{1,0:T(8,128)(2,1)S(1)} %get-tuple-element.69), channel_id=1, source_target_pairs={{0,16},{8,24},{16,0},{24,8},{1,17},{9,25},{17,1},{25,9},{2,18},{10... | collective-permute-start | bytes 589832 | tf_op jit(solution)/shard_map/ppermute | solution.py:55
  13.4 9.8 %collective-permute-start.18 = (bf16[192,512]{1,0:T(8,128)(2,1)S(1)}, bf16[192,512]{1,0:T(8,128)(2,1)S(1)}, u32[]{:S(2)}, u32[]{:S(2)}) collective-permute-start(bf16[192,512]{1,0:T(8,128)(2,1)S(1)} %get-tuple-element.70), channel_id=1, source_target_pairs={{0,24},{8,16},{16,8},{24,0},{1,25},{9,17},{17,9},{25,1},{2,26},{10... | collective-permute-start | bytes 589832 | tf_op jit(solution)/shard_map/ppermute | solution.py:55
  17.9 7.8 %collective-permute-start.8 = (bf16[192,512]{1,0:T(8,128)(2,1)S(1)}, bf16[192,512]{1,0:T(8,128)(2,1)S(1)}, u32[]{:S(2)}, u32[]{:S(2)}) collective-permute-start(bf16[192,512]{1,0:T(8,128)(2,1)S(1)} %get-tuple-element.63), channel_id=1, source_target_pairs={{0,8},{8,0},{16,24},{24,16},{1,9},{9,1},{17,25},{25,17},{2,10},{10... | collective-permute-start | bytes 589832 | tf_op jit(solution)/shard_map/ppermute | solution.py:55
  19.5 11.2 %collective-permute-start.9 = (bf16[192,512]{1,0:T(8,128)(2,1)S(1)}, bf16[192,512]{1,0:T(8,128)(2,1)S(1)}, u32[]{:S(2)}, u32[]{:S(2)}) collective-permute-start(bf16[192,512]{1,0:T(8,128)(2,1)S(1)} %get-tuple-element.64), channel_id=1, source_target_pairs={{0,16},{8,24},{16,0},{24,8},{1,17},{9,25},{17,1},{25,9},{2,18},{10... | collective-permute-start | bytes 589832 | tf_op jit(solution)/shard_map/ppermute | solution.py:55
  21.7 9.0 %collective-permute-start.10 = (bf16[192,512]{1,0:T(8,128)(2,1)S(1)}, bf16[192,512]{1,0:T(8,128)(2,1)S(1)}, u32[]{:S(2)}, u32[]{:S(2)}) collective-permute-start(bf16[192,512]{1,0:T(8,128)(2,1)S(1)} %get-tuple-element.65), channel_id=1, source_target_pairs={{0,24},{8,16},{16,8},{24,0},{1,25},{9,17},{17,9},{25,1},{2,26},{10... | collective-permute-start | bytes 589832 | tf_op jit(solution)/shard_map/ppermute | solution.py:55
  23.2 8.1 %collective-permute-start.20 = (bf16[192,512]{1,0:T(8,128)(2,1)S(1)}, bf16[192,512]{1,0:T(8,128)(2,1)S(1)}, u32[]{:S(2)}, u32[]{:S(2)}) collective-permute-start(bf16[192,512]{1,0:T(8,128)(2,1)S(1)} %collective-permute-done.16.refs_1_), channel_id=1, source_target_pairs={{0,1},{1,0},{2,3},{3,2},{4,5},{5,4},{6,7},{7,6},{8,9},{9,8},{10,11... | collective-permute-start | bytes 589832 | tf_op jit(solution)/shard_map/ppermute | solution.py:55
  23.2 8.2 %collective-permute-start.21 = (bf16[192,512]{1,0:T(8,128)(2,1)S(1)}, bf16[192,512]{1,0:T(8,128)(2,1)S(1)}, u32[]{:S(2)}, u32[]{:S(2)}) collective-permute-start(bf16[192,512]{1,0:T(8,128)(2,1)S(1)} %collective-permute-done.17.refs_2_), channel_id=1, source_target_pairs={{0,1},{1,0},{2,3},{3,2},{4,5},{5,4},{6,7},{7,6},{8,9},{9,8},{10,11... | collective-permute-start | bytes 589832 | tf_op jit(solution)/shard_map/ppermute | solution.py:55
  25.8 8.8 %collective-permute-start.22 = (bf16[192,512]{1,0:T(8,128)(2,1)S(1)}, bf16[192,512]{1,0:T(8,128)(2,1)S(1)}, u32[]{:S(2)}, u32[]{:S(2)}) collective-permute-start(bf16[192,512]{1,0:T(8,128)(2,1)S(1)} %collective-permute-done.18.refs_3_), channel_id=1, source_target_pairs={{0,1},{1,0},{2,3},{3,2},{4,5},{5,4},{6,7},{7,6},{8,9},{9,8},{10,11... | collective-permute-start | bytes 589832 | tf_op jit(solution)/shard_map/ppermute | solution.py:55
  45.8 10.6 %collective-permute-start = (bf16[1280,128]{1,0:T(8,128)(2,1)S(1)}, bf16[1280,128]{1,0:T(8,128)(2,1)S(1)}, u32[]{:S(2)}, u32[]{:S(2)}) collective-permute-start(bf16[1280,128]{1,0:T(8,128)(2,1)S(1)} %get-tuple-element.53), channel_id=1, source_target_pairs={{0,8},{8,0},{16,24},{24,16},{1,9},{9,1},{17,25},{25,17},{2,10},{10... | collective-permute-start | bytes 983048 | tf_op jit(solution)/shard_map/ppermute | solution.py:55
  46.5 14.7 %collective-permute-start.1 = (bf16[1280,128]{1,0:T(8,128)(2,1)S(1)}, bf16[1280,128]{1,0:T(8,128)(2,1)S(1)}, u32[]{:S(2)}, u32[]{:S(2)}) collective-permute-start(bf16[1280,128]{1,0:T(8,128)(2,1)S(1)} %get-tuple-element.54), channel_id=1, source_target_pairs={{0,16},{8,24},{16,0},{24,8},{1,17},{9,25},{17,1},{25,9},{2,18},{10... | collective-permute-start | bytes 983048 | tf_op jit(solution)/shard_map/ppermute | solution.py:55
  47.9 18.1 %collective-permute-start.2 = (bf16[1280,128]{1,0:T(8,128)(2,1)S(1)}, bf16[1280,128]{1,0:T(8,128)(2,1)S(1)}, u32[]{:S(2)}, u32[]{:S(2)}) collective-permute-start(bf16[1280,128]{1,0:T(8,128)(2,1)S(1)} %get-tuple-element.55), channel_id=1, source_target_pairs={{0,24},{8,16},{16,8},{24,0},{1,25},{9,17},{17,9},{25,1},{2,26},{10... | collective-permute-start | bytes 983048 | tf_op jit(solution)/shard_map/ppermute | solution.py:55
  49.5 27.4 %collective-permute-start.24 = (bf16[768,256]{1,0:T(8,128)(2,1)S(1)}, bf16[768,256]{1,0:T(8,128)(2,1)S(1)}, u32[]{:S(2)}, u32[]{:S(2)}) collective-permute-start(bf16[768,256]{1,0:T(8,128)(2,1)S(1)} %get-tuple-element.77), channel_id=1, source_target_pairs={{0,2},{1,3},{2,0},{3,1},{4,6},{5,7},{6,4},{7,5},{8,10},{9,11},{10,... | collective-permute-start | bytes 1179656 | tf_op jit(solution)/shard_map/ppermute | solution.py:55
  50.3 21.0 %collective-permute-start.29 = (bf16[192,512]{1,0:T(8,128)(2,1)S(1)}, bf16[192,512]{1,0:T(8,128)(2,1)S(1)}, u32[]{:S(2)}, u32[]{:S(2)}) collective-permute-start(bf16[192,512]{1,0:T(8,128)(2,1)S(1)} %get-tuple-element.85), channel_id=1, source_target_pairs={{0,8},{8,0},{16,24},{24,16},{1,9},{9,1},{17,25},{25,17},{2,10},{10... | collective-permute-start | bytes 589832 | tf_op jit(solution)/shard_map/ppermute | solution.py:55
  56.5 15.4 %collective-permute-start.30 = (bf16[192,512]{1,0:T(8,128)(2,1)S(1)}, bf16[192,512]{1,0:T(8,128)(2,1)S(1)}, u32[]{:S(2)}, u32[]{:S(2)}) collective-permute-start(bf16[192,512]{1,0:T(8,128)(2,1)S(1)} %get-tuple-element.86), channel_id=1, source_target_pairs={{0,16},{8,24},{16,0},{24,8},{1,17},{9,25},{17,1},{25,9},{2,18},{10... | collective-permute-start | bytes 589832 | tf_op jit(solution)/shard_map/ppermute | solution.py:55
  61.2 13.6 %collective-permute-start.31 = (bf16[192,512]{1,0:T(8,128)(2,1)S(1)}, bf16[192,512]{1,0:T(8,128)(2,1)S(1)}, u32[]{:S(2)}, u32[]{:S(2)}) collective-permute-start(bf16[192,512]{1,0:T(8,128)(2,1)S(1)} %get-tuple-element.87), channel_id=1, source_target_pairs={{0,24},{8,16},{16,8},{24,0},{1,25},{9,17},{17,9},{25,1},{2,26},{10... | collective-permute-start | bytes 589832 | tf_op jit(solution)/shard_map/ppermute | solution.py:55
  71.2 7.3 %collective-permute-start.3 = (bf16[256,128]{1,0:T(8,128)(2,1)S(1)}, bf16[256,128]{1,0:T(8,128)(2,1)S(1)}, u32[]{:S(2)}, u32[]{:S(2)}) collective-permute-start(bf16[256,128]{1,0:T(8,128)(2,1)S(1)} %get-tuple-element.57), channel_id=1, source_target_pairs={{0,8},{8,0},{16,24},{24,16},{1,9},{9,1},{17,25},{25,17},{2,10},{10... | collective-permute-start | bytes 196616 | tf_op jit(solution)/shard_map/ppermute | solution.py:55
  71.3 7.4 %collective-permute-start.4 = (bf16[256,128]{1,0:T(8,128)(2,1)S(1)}, bf16[256,128]{1,0:T(8,128)(2,1)S(1)}, u32[]{:S(2)}, u32[]{:S(2)}) collective-permute-start(bf16[256,128]{1,0:T(8,128)(2,1)S(1)} %get-tuple-element.58), channel_id=1, source_target_pairs={{0,16},{8,24},{16,0},{24,8},{1,17},{9,25},{17,1},{25,9},{2,18},{10... | collective-permute-start | bytes 196616 | tf_op jit(solution)/shard_map/ppermute | solution.py:55
  71.9 7.4 %collective-permute-start.5 = (bf16[256,128]{1,0:T(8,128)(2,1)S(1)}, bf16[256,128]{1,0:T(8,128)(2,1)S(1)}, u32[]{:S(2)}, u32[]{:S(2)}) collective-permute-start(bf16[256,128]{1,0:T(8,128)(2,1)S(1)} %get-tuple-element.59), channel_id=1, source_target_pairs={{0,24},{8,16},{16,8},{24,0},{1,25},{9,17},{17,9},{25,1},{2,26},{10... | collective-permute-start | bytes 196616 | tf_op jit(solution)/shard_map/ppermute | solution.py:55
  75.5 9.8 %collective-permute-start.32 = (bf16[256,256]{1,0:T(8,128)(2,1)S(1)}, bf16[256,256]{1,0:T(8,128)(2,1)S(1)}, u32[]{:S(2)}, u32[]{:S(2)}) collective-permute-start(bf16[256,256]{1,0:T(8,128)(2,1)S(1)} %get-tuple-element.88), channel_id=1, source_target_pairs={{0,4},{1,5},{2,6},{3,7},{4,0},{5,1},{6,2},{7,3},{8,12},{9,13},{10,... | collective-permute-start | bytes 393224 | tf_op jit(solution)/shard_map/ppermute | solution.py:55
  77.0 8.4 %collective-permute-start.33 = (bf16[256,256]{1,0:T(8,128)(2,1)S(1)}, bf16[256,256]{1,0:T(8,128)(2,1)S(1)}, u32[]{:S(2)}, u32[]{:S(2)}) collective-permute-start(bf16[256,256]{1,0:T(8,128)(2,1)S(1)} %get-tuple-element.89), channel_id=1, source_target_pairs={{0,6},{1,7},{2,4},{3,5},{4,2},{5,3},{6,0},{7,1},{8,14},{9,15},{10,... | collective-permute-start | bytes 393224 | tf_op jit(solution)/shard_map/ppermute | solution.py:55
  (21 other events, 132.7 us)
